TPU v7x, 512 devices: a whole 4x8x8 slice. The times are simulated.
512 devices in a mesh: sp: 64 (over z, y), tp: 8 (over x, core).
Axes of the slice: x: 4, y: 8, z: 8, core: 2. Of those that a mesh axis runs over, the one named last changes fastest.
Arguments:
- resid: bfloat16 [8192, 2048], P('sp'), may hold values from -6 to 6
- queries: bfloat16 [8192, 1024], P('sp', 'tp'), may hold values from -6 to 6
- keys: bfloat16 [8192, 1024], P('sp', 'tp'), may hold values from -6 to 6
- values: bfloat16 [8192, 2048], P('sp', 'tp'), may hold values from -6 to 6
- decay_pre: float32 [8192, 1024], P('sp', 'tp'), may hold values from -4 to 11.5
- out_gate: bfloat16 [8192, 2048], P('sp', 'tp'), may hold values from -6 to 6
- head_gain: float32 [256], replicated, may hold values from 0.1 to 1.9
- out_proj: bfloat16 [2048, 2048], P('tp'), may hold values from -0.25 to 0.25
- mix_gain: float32 [2048], replicated, may hold values from 0.1 to 1.9
- mix_shift: float32 [2048], replicated, may hold values from -3 to 3
- gate_in: bfloat16 [2048, 5632], P('sp', 'tp'), may hold values from -0.125 to 0.125
- up_in: bfloat16 [2048, 5632], P('sp', 'tp'), may hold values from -0.125 to 0.125
- down_out: bfloat16 [5632, 2048], P('tp', 'sp'), may hold values from -0.25 to 0.25
- out_gain: float32 [2048], replicated, may hold values from 0.1 to 1.9
- out_shift: float32 [2048], replicated, may hold values from -2 to 2
Outputs:
- result: bfloat16 [8192, 2048], P('sp')
All inputs are finite; a program needn't handle non-finite values.
Results may differ from a plain program's by a relative error of at most 0.02.
Values may be sent and summed in bfloat16 or wider, within the bound.
No kernel may reach another device: no remote copies, remote signals or barrier semaphores. Data moves between devices by JAX's collectives and lax.ppermute only.
A program may use at most 64 MiB of HBM per device.

v0:
```python
import jax
import jax.numpy as jnp
from jax import lax
from jax.sharding import Mesh
from jax.sharding import PartitionSpec as P

HK = 128
HV = 256
SPAN = 64
SP = ("sp_0", "sp_1")


ALPHA = 2.0**0.25
LN_EPS = 1e-05
RMS_EPS = 1e-06
TAU = 16.0


def nothing_yet(array, identity):
    return jax.tree.map(
        lambda part, zero: jnp.zeros_like(part) + jnp.asarray(zero, part.dtype), array, identity
    )


def carried_in(array, axes, combine, identity):
    before = start = nothing_yet(array, identity)
    running = array
    for axis in reversed(axes):
        count, place = (lax.axis_size(axis), lax.axis_index(axis))
        pieces = jax.tree.map(
            lambda part, kind: lax.all_gather(part.astype(kind), axis),
            running,
            (jnp.bfloat16, jnp.bfloat16),
        )
        inside, running = (start, start)
        for k in range(count):
            passed = k < place
            running = combine(
                running, jax.tree.map(lambda part, own: part[k].astype(own.dtype), pieces, array)
            )
            inside = jax.tree.map(lambda new, old: jnp.where(passed, new, old), running, inside)
        before = combine(inside, before)
    return before


def turned_gather(arrays, axis, dims):
    turned = [jnp.moveaxis(a, dim, 0) for a, dim in zip(arrays, dims)]
    both = jnp.concatenate([t.reshape(len(t), -1) for t in turned], axis=1)
    out, at, done = (lax.all_gather(both, axis, axis=0, tiled=True), 0, [])
    for t, dim in zip(turned, dims):
        share = out[:, at : at + t[0].size].reshape(-1, *t.shape[1:])
        done.append(jnp.moveaxis(share, 0, dim))
        at += t[0].size
    return tuple(done)


def split_up(array, dim, count):
    before, after = (array.shape[:dim], array.shape[dim + 1 :])
    return jnp.moveaxis(array.reshape(*before, count, -1, *after), dim, 0)


def sent_and_summed(array, axis, dim):
    blocks = split_up(array, dim, lax.axis_size(axis))
    arrived = lax.all_to_all(blocks, axis, split_axis=0, concat_axis=0, tiled=True)
    return arrived.astype(jnp.float32).sum(axis=0)


def from_everyone(array, axis):
    copies = jnp.broadcast_to(array, (lax.axis_size(axis), *array.shape))
    return lax.all_to_all(copies, axis, split_axis=0, concat_axis=0, tiled=True)


def in_order(blocks, dim):
    lengths = list(blocks.shape[1:])
    lengths[dim] *= blocks.shape[0]
    return jnp.moveaxis(blocks, 0, dim).reshape(lengths)


def gather_directly(array, axis, dim):
    blocks = from_everyone(array, axis)
    return in_order(blocks, dim)


def layer_norm(inputs, gain, shift):
    center = inputs - jnp.mean(inputs, axis=-1, keepdims=True)
    spread = jnp.mean(center * center, axis=-1, keepdims=True)
    return center * lax.rsqrt(spread + LN_EPS) * gain + shift


def combine_states(earlier, later):
    return (earlier[0] * later[0], later[0][..., None] * earlier[1] + later[1])


def mix_tokens(queries, keys, values, decay_pre, out_gate, head_gain):
    tok_rows = queries.shape[0]
    local_heads = queries.shape[1] // HK
    blocks = tok_rows // SPAN
    logdecay = jax.nn.log_sigmoid(decay_pre) / TAU
    scaled_q = queries.astype(jnp.float32).reshape(blocks, SPAN, local_heads, HK) * HK ** (-0.5)
    key_block = keys.astype(jnp.float32).reshape(blocks, SPAN, local_heads, HK)
    value_block = values.astype(jnp.float32).reshape(blocks, SPAN, local_heads, HV)
    cumul = jnp.cumsum(logdecay.reshape(blocks, SPAN, local_heads, HK), axis=1)
    last = cumul[:, -1]
    key_decayed = key_block * jnp.exp(last[:, None] - cumul)
    updates = jnp.einsum(
        "nchk,nchv->nhkv", key_decayed, value_block, precision=lax.Precision.HIGHEST
    )

    def advance(running_state, inputs):
        decay_end, state_increment, current_query = inputs
        running_state = jnp.exp(decay_end)[..., None] * running_state + state_increment
        return (
            running_state,
            jnp.einsum(
                "qpy,pyr->qpr", current_query, running_state, precision=lax.Precision.HIGHEST
            ),
        )

    own_state, local_read = lax.scan(
        advance, jnp.zeros((local_heads, HK, HV), jnp.float32), (last, updates, scaled_q)
    )
    block_ends = jnp.cumsum(last, axis=0)
    own_decay = jnp.exp(block_ends[-1])
    identity = (jnp.ones_like(own_decay), jnp.zeros_like(own_state))
    _, incoming = carried_in((own_decay, own_state), SP, combine_states, identity)
    carried = jnp.einsum(
        "xepj,pjw->xepw",
        scaled_q * jnp.exp(block_ends)[:, None],
        incoming,
        precision=lax.Precision.HIGHEST,
    )
    state_readout = (local_read + carried).reshape(tok_rows, local_heads, HV)
    normed = (
        state_readout
        * lax.rsqrt(jnp.mean(state_readout * state_readout, axis=-1, keepdims=True) + RMS_EPS)
        * head_gain
    )
    return (
        normed.reshape(tok_rows, local_heads * HV) * jax.nn.silu(out_gate.astype(jnp.float32))
    ).astype(jnp.bfloat16)


def expand_rows(mid_rows, gate_whole, up_whole):
    gate = jnp.dot(mid_rows, gate_whole, preferred_element_type=jnp.float32)
    upward = jnp.dot(mid_rows, up_whole, preferred_element_type=jnp.float32)
    return (jax.nn.silu(gate) * upward).astype(jnp.bfloat16)


def body(
    resid,
    queries,
    keys,
    values,
    decay_pre,
    out_gate,
    head_gain,
    out_proj,
    mix_gain,
    mix_shift,
    gate_in,
    up_in,
    down_out,
    out_gain,
    out_shift,
):
    tp_count = lax.axis_size("tp")
    tok_rows = queries.shape[0]
    own_count = tok_rows // tp_count
    gate_whole, up_whole, down_whole = turned_gather((gate_in, up_in, down_out), SP, (0, 0, 1))
    gated = mix_tokens(queries, keys, values, decay_pre, out_gate, head_gain)
    mixed = sent_and_summed(
        jnp.dot(gated, out_proj, preferred_element_type=jnp.float32).astype(jnp.bfloat16), "tp", 0
    )
    own_resid = lax.dynamic_slice_in_dim(resid, lax.axis_index("tp") * own_count, own_count, 0)
    mid = layer_norm(ALPHA * own_resid.astype(jnp.float32) + mixed, mix_gain, mix_shift).astype(
        jnp.bfloat16
    )
    hidden = expand_rows(gather_directly(mid, "tp", 0), gate_whole, up_whole)
    ffn = sent_and_summed(
        jnp.dot(hidden, down_whole, preferred_element_type=jnp.float32).astype(jnp.bfloat16),
        "tp",
        0,
    )
    finished = layer_norm(ALPHA * mid.astype(jnp.float32) + 0.5 * ffn, out_gain, out_shift).astype(
        jnp.bfloat16
    )
    return gather_directly(finished, "tp", 0)


def solution(mesh):
    finer = Mesh(mesh.devices.reshape(8, 8, mesh.shape["tp"]), ("sp_0", "sp_1", "tp"))
    placed = (
        P(SP, None),
        P(SP, "tp"),
        P(SP, "tp"),
        P(SP, "tp"),
        P(SP, "tp"),
        P(SP, "tp"),
        P(),
        P("tp", None),
        P(),
        P(),
        P(SP, "tp"),
        P(SP, "tp"),
        P("tp", SP),
        P(),
        P(),
    )
    return jax.shard_map(body, mesh=finer, in_specs=placed, out_specs=P(SP, None), check_vma=False)
```

profile of v0, /device:TPU:1, one launch (start us, length us, event | category | flops | bytes accessed | tf_op | source)
XLA Modules:
  0.0 182.2 jit_solution(2570630741148802236)
XLA Ops:
  6.6 1.7 concatenate.3
  8.4 0.9 fusion.102
  9.4 0.8 convert_multiply_fusion.2
  10.2 1.2 convolution_bitcast_fusion.1
  11.4 0.8 while.13
  11.4 0.1 bitcast_add_fusion.2
  11.5 0.2 fusion.184
  11.8 0.1 bitcast_add_fusion.2
  11.9 0.2 fusion.184
  12.2 13.8 %all_gather.21 = bf16[8,1,128]{2,1,0:T(2,128)(2,1)S(1)} all-gather(bf16[1,1,128]{2,1,0:T(2,128)(2,1)S(1)} %convert_bitcast_fusion.16), channel_id=1, replica_groups=mesh['sp_0'=8,'sp_1'=8,'tp'=8] {'sp_1'}, dimensions={0}, use_global_device_ids=true | all-gather | bytes 2304 | tf_op jit(solution)/shard_map/all_gather | solution.py:31
  26.0 18.6 %all_gather.22 = bf16[8,1,128]{2,1,0:T(2,128)(2,1)S(1)} all-gather(bf16[1,1,128]{2,1,0:T(2,128)(2,1)S(1)} %multiply_convert_fusion), channel_id=1, replica_groups=mesh['sp_0'=8,'sp_1'=8,'tp'=8] {'sp_0'}, dimensions={0}, use_global_device_ids=true | all-gather | bytes 2304 | tf_op jit(solution)/shard_map/all_gather | solution.py:31
  44.6 20.8 %all-gather = bf16[8,128,256]{2,1,0:T(8,128)(2,1)S(1)} all-gather(bf16[1,128,256]{2,1,0:T(8,128)(2,1)S(1)} %convert_element_type.740), channel_id=2, replica_groups=mesh['sp_0'=8,'sp_1'=8,'tp'=8] {'sp_1'}, dimensions={0}, use_global_device_ids=true | all-gather | bytes 589824 | tf_op jit(solution)/shard_map/all_gather | solution.py:31
  65.4 0.2 fusion.100
  65.6 22.4 %all_gather.25 = bf16[8,1,128,256]{3,2,1,0:T(8,128)(2,1)S(1)} all-gather(bf16[1,1,128,256]{3,2,1,0:T(8,128)(2,1)S(1)} %fusion.100), channel_id=1, replica_groups=mesh['sp_0'=8,'sp_1'=8,'tp'=8] {'sp_0'}, dimensions={0}, use_global_device_ids=true | all-gather | bytes 589824 | tf_op jit(solution)/shard_map/all_gather | solution.py:31
  88.0 0.8 multiply_reduce_fusion.2
  88.8 0.1 rsqrt.28
  88.9 0.1 fusion.99
  89.0 1.1 convolution_convert_fusion
  90.1 22.7 %all-to-all-start = ((bf16[8,16,2048]{2,1,0:T(8,128)(2,1)}), bf16[8,16,2048]{2,1,0:T(8,128)(2,1)S(1)}, u32[]{:S(2)}, u32[]{:S(2)}) async-start(bf16[8,16,2048]{2,1,0:T(8,128)(2,1)} %bitcast.61), calls=%async_computation | async-start | bytes 1048576 | tf_op jit(solution)/shard_map/all_to_all | solution.py:64
  112.8 9.3 %all-to-all-done = bf16[8,16,2048]{2,1,0:T(8,128)(2,1)S(1)} async-done(((bf16[8,16,2048]{2,1,0:T(8,128)(2,1)}), bf16[8,16,2048]{2,1,0:T(8,128)(2,1)S(1)}, u32[]{:S(2)}, u32[]{:S(2)}) %all-to-all-start) | async-done | bytes 524320 | tf_op jit(solution)/shard_map/all_to_all | solution.py:64
  122.2 1.0 fusion.149
  123.2 1.0 multiply_reduce_fusion.1
  124.3 0.9 add_convert_fusion.1
  125.3 12.7 %all_to_all.20 = bf16[8,16,2048]{2,1,0:T(8,128)(2,1)S(1)} all-to-all(bf16[8,16,2048]{2,1,0:T(8,128)(2,1)S(1)} %broadcast_in_dim.15), channel_id=1, replica_groups=mesh['sp_0'=8,'sp_1'=8,'tp'=8] {'tp'}, dimensions={0} | all-to-all | bytes 1048576 | tf_op jit(solution)/shard_map/all_to_all | solution.py:70
  138.0 3.2 %fusion.8 = f32[128,704]{0,1:T(8,128)S(1)} fusion(bf16[128,2048]{1,0:T(8,128)(2,1)S(1)} %bitcast.399, bf16[2048,2112]{1,0:T(8,128)(2,1)} %all-gather.3.cloned.1.call-done), kind=kOutput, calls=%fused_computation.13 | convolution fusion | flops 369098752 | bytes 4030464 | tf_op jit(solution)/shard_map/dot_general | solution.py:144
  141.2 7.2 %fusion.10 = bf16[128,2048]{1,0:T(8,128)(2,1)S(1)} fusion(bf16[2048,2112]{1,0:T(8,128)(2,1)} %all-gather.3.cloned.1.call-done, bf16[128,2048]{1,0:T(8,128)(2,1)S(1)} %bitcast.400, f32[128,704]{0,1:T(8,128)S(1)} %fusion.8), kind=kOutput, calls=%fused_computation.15 | convolution fusion | flops 739000320 | bytes 7700480 | tf_op jit(solution)/shard_map/dot_general | solution.py:180
  148.4 12.8 %all_to_all.21 = bf16[8,16,2048]{2,1,0:T(8,128)(2,1)S(1)} all-to-all(bf16[8,16,2048]{2,1,0:T(8,128)(2,1)S(1)} %bitcast.401), channel_id=1, replica_groups=mesh['sp_0'=8,'sp_1'=8,'tp'=8] {'tp'}, dimensions={0} | all-to-all | bytes 1048576 | tf_op jit(solution)/shard_map/all_to_all | solution.py:64
  161.3 0.1 fusion.148
  161.4 0.2 multiply_reduce_fusion
  161.7 0.1 add_convert_fusion
  161.8 12.8 %all_to_all.22 = bf16[8,16,2048]{2,1,0:T(8,128)(2,1)S(1)} all-to-all(bf16[8,16,2048]{2,1,0:T(8,128)(2,1)S(1)} %broadcast_in_dim.16), channel_id=1, replica_groups=mesh['sp_0'=8,'sp_1'=8,'tp'=8] {'tp'}, dimensions={0} | all-to-all | bytes 1048576 | tf_op jit(solution)/shard_map/all_to_all | solution.py:70
  174.6 0.8 copy.36
  (43 shorter events, 0.6 us)
Async XLA Ops:
  6.5 82.4 %copy-start = (bf16[256,2048]{1,0:T(8,128)(2,1)S(1)}, bf16[256,2048]{1,0:T(8,128)(2,1)}, u32[]{:S(2)}) copy-start(bf16[256,2048]{1,0:T(8,128)(2,1)} %param.24) | copy-start | bytes 3145732
  6.5 82.3 %copy-start.6 = (f32[256]{0:T(256)S(1)}, f32[256]{0:T(256)}, u32[]{:S(2)}) copy-start(f32[256]{0:T(256)} %param.23) | copy-start | bytes 3076
  6.5 82.3 %copy-start.1 = (bf16[128,256]{1,0:T(8,128)(2,1)S(1)}, bf16[128,256]{1,0:T(8,128)(2,1)}, u32[]{:S(2)}) copy-start(bf16[128,256]{1,0:T(8,128)(2,1)} %param.22) | copy-start | bytes 196612
  6.5 117.7 %copy-start.2 = (f32[2048]{0:T(1024)S(1)}, f32[2048]{0:T(1024)}, u32[]{:S(2)}) copy-start(f32[2048]{0:T(1024)} %param.26) | copy-start | bytes 24580
  6.5 117.7 %copy-start.3 = (f32[2048]{0:T(1024)S(1)}, f32[2048]{0:T(1024)}, u32[]{:S(2)}) copy-start(f32[2048]{0:T(1024)} %param.25) | copy-start | bytes 24580
  6.5 131.5 %all-gather.3.cloned.1.call-start = ((), (), s32[]{:S(2)}) async-start(), calls=%async_computation.4 | async-start | bytes 9052160 | tf_op jit(solution)/shard_map/all_gather | solution.py:49
  90.1 32.1 %all-to-all-start = ((bf16[8,16,2048]{2,1,0:T(8,128)(2,1)}), bf16[8,16,2048]{2,1,0:T(8,128)(2,1)S(1)}, u32[]{:S(2)}, u32[]{:S(2)}) async-start(bf16[8,16,2048]{2,1,0:T(8,128)(2,1)} %bitcast.61), calls=%async_computation | async-start | bytes 1048576 | tf_op jit(solution)/shard_map/all_to_all | solution.py:64
  125.3 36.4 %copy-start.4 = (f32[2048]{0:T(1024)S(1)}, f32[2048]{0:T(1024)}, u32[]{:S(2)}) copy-start(f32[2048]{0:T(1024)} %param.31) | copy-start | bytes 24580
  125.3 36.4 %copy-start.5 = (f32[2048]{0:T(1024)S(1)}, f32[2048]{0:T(1024)}, u32[]{:S(2)}) copy-start(f32[2048]{0:T(1024)} %param.30) | copy-start | bytes 24580
Sparse Core Ops, SparseCore 0:
  10.4 110.9 all-gather.2
where the time goes:
time: 183 us; the launch traced here: 182 us
  blocking collectives  114 us (62%)
  starting transfers between devices  22.8 us (12%)
  matrix products  13.9 us (8%)
  between operations  13.6 us (7%)
  waiting for transfers between devices  9.37 us (5%)
  other arithmetic  5.9 us (3%)
  local copies, waits for them, and re-layouts  2.73 us (1%)
    all_gather x4, blocking collectives, carried_in(): lax.all_gather(part.astype(kind), axis)  75.5 us
    all_to_all x2, blocking collectives, from_everyone(): return lax.all_to_all(copies, axis, split_axis=0, concat_axis=0, tiled=True)  25.5 us
    all_to_all x1, starting transfers between devices, sent_and_summed(): lax.all_to_all(blocks, axis, split_axis=0, concat_axis=0, tiled=True)  22.7 us
    all_to_all x1, blocking collectives, sent_and_summed(): lax.all_to_all(blocks, axis, split_axis=0, concat_axis=0, tiled=True)  12.8 us
    all_to_all x1, waiting for transfers between devices, sent_and_summed(): lax.all_to_all(blocks, axis, split_axis=0, concat_axis=0, tiled=True)  9.35 us
    dot_general x1, matrix products, body(): jnp.dot(hidden, down_whole, preferred_element_type=jnp.float32)  7.24 us
  transfers between devices with their start and end apart: 2, of which 1 were waited for; matrix products, arithmetic and copies ran while one was open for 5% of the time, Pallas kernels for 0%

commit v1 on v0

--- a/solution.py
+++ b/solution.py
@@ -1,6 +1,10 @@
+import functools
+
 import jax
 import jax.numpy as jnp
 from jax import lax
+from jax.experimental import pallas as pl
+from jax.experimental.pallas import tpu as pltpu
 from jax.sharding import Mesh
 from jax.sharding import PartitionSpec as P
 
@@ -16,42 +20,48 @@
 TAU = 16.0
 
 
-def nothing_yet(array, identity):
-    return jax.tree.map(
-        lambda part, zero: jnp.zeros_like(part) + jnp.asarray(zero, part.dtype), array, identity
-    )
-
-
-def carried_in(array, axes, combine, identity):
-    before = start = nothing_yet(array, identity)
-    running = array
-    for axis in reversed(axes):
-        count, place = (lax.axis_size(axis), lax.axis_index(axis))
-        pieces = jax.tree.map(
-            lambda part, kind: lax.all_gather(part.astype(kind), axis),
-            running,
-            (jnp.bfloat16, jnp.bfloat16),
-        )
-        inside, running = (start, start)
-        for k in range(count):
-            passed = k < place
-            running = combine(
-                running, jax.tree.map(lambda part, own: part[k].astype(own.dtype), pieces, array)
-            )
-            inside = jax.tree.map(lambda new, old: jnp.where(passed, new, old), running, inside)
-        before = combine(inside, before)
-    return before
-
-
-def turned_gather(arrays, axis, dims):
-    turned = [jnp.moveaxis(a, dim, 0) for a, dim in zip(arrays, dims)]
-    both = jnp.concatenate([t.reshape(len(t), -1) for t in turned], axis=1)
-    out, at, done = (lax.all_gather(both, axis, axis=0, tiled=True), 0, [])
-    for t, dim in zip(turned, dims):
-        share = out[:, at : at + t[0].size].reshape(-1, *t.shape[1:])
-        done.append(jnp.moveaxis(share, 0, dim))
-        at += t[0].size
-    return tuple(done)
+def with_decay(state, logs):
+    coarse = lax.reduce_precision(logs, 8, 7)
+    lane = lax.broadcasted_iota(jnp.int32, (*logs.shape, 128), logs.ndim)
+    extra = jnp.where(
+        lane == 0, coarse[..., None], jnp.where(lane == 1, (logs - coarse)[..., None], 0.0)
+    )
+    return jnp.concatenate([state, extra], axis=-1).astype(jnp.bfloat16)
+
+
+def apart(packed):
+    whole = packed.astype(jnp.float32)
+    return whole[..., :HV], whole[..., HV:].sum(axis=-1)
+
+
+def incoming_state(own_state, own_log):
+    row, col = SP
+    count = lax.axis_size(col)
+    packed = with_decay(own_state, own_log).reshape(count, -1, HV + 128)
+    states, logs = apart(
+        lax.all_to_all(packed, col, split_axis=0, concat_axis=0, tiled=True)
+    )
+    before, passed = [jnp.zeros_like(states[0])], [jnp.zeros_like(logs[0])]
+    for k in range(count):
+        before.append(jnp.exp(logs[k])[:, None] * before[-1] + states[k])
+        passed.append(passed[-1] + logs[k])
+    totals, total_logs = apart(from_everyone(with_decay(before[-1], passed[-1]), row))
+    earlier = jnp.zeros_like(totals[0])
+    for k in range(lax.axis_size(row)):
+        earlier = jnp.where(
+            k < lax.axis_index(row), jnp.exp(total_logs[k])[:, None] * earlier + totals[k], earlier
+        )
+    entering = jnp.stack(
+        [jnp.exp(passed[k])[:, None] * earlier + before[k] for k in range(count)]
+    ).astype(jnp.bfloat16)
+    back = lax.all_to_all(entering, col, split_axis=0, concat_axis=0, tiled=True)
+    return back.reshape(own_state.shape).astype(jnp.float32)
+
+
+def gathered_weights(gate_in, up_in, down_out):
+    return lax.all_gather(
+        jnp.concatenate([gate_in, up_in, down_out.T], axis=1), SP, axis=0, tiled=True
+    )
 
 
 def split_up(array, dim, count):
@@ -85,10 +95,6 @@
     center = inputs - jnp.mean(inputs, axis=-1, keepdims=True)
     spread = jnp.mean(center * center, axis=-1, keepdims=True)
     return center * lax.rsqrt(spread + LN_EPS) * gain + shift
-
-
-def combine_states(earlier, later):
-    return (earlier[0] * later[0], later[0][..., None] * earlier[1] + later[1])
 
 
 def mix_tokens(queries, keys, values, decay_pre, out_gate, head_gain):
@@ -120,9 +126,7 @@
         advance, jnp.zeros((local_heads, HK, HV), jnp.float32), (last, updates, scaled_q)
     )
     block_ends = jnp.cumsum(last, axis=0)
-    own_decay = jnp.exp(block_ends[-1])
-    identity = (jnp.ones_like(own_decay), jnp.zeros_like(own_state))
-    _, incoming = carried_in((own_decay, own_state), SP, combine_states, identity)
+    incoming = incoming_state(own_state[0], block_ends[-1, 0])[None]
     carried = jnp.einsum(
         "xepj,pjw->xepw",
         scaled_q * jnp.exp(block_ends)[:, None],
@@ -140,10 +144,64 @@
     ).astype(jnp.bfloat16)
 
 
-def expand_rows(mid_rows, gate_whole, up_whole):
-    gate = jnp.dot(mid_rows, gate_whole, preferred_element_type=jnp.float32)
-    upward = jnp.dot(mid_rows, up_whole, preferred_element_type=jnp.float32)
-    return (jax.nn.silu(gate) * upward).astype(jnp.bfloat16)
+def mixer_kernel(units, depth, mid_ref, weights_ref, out_ref, held, total, sems):
+    steps = mid_ref.shape[1] // depth
+    wide = 2 * units
+
+    def fetch(step, part):
+        rows = pl.ds(step * depth, depth)
+        columns = pl.ds(0, wide) if part == 0 else pl.ds(wide, units)
+        return pltpu.make_async_copy(
+            weights_ref.at[rows, columns], held.at[rows, columns], sems.at[part, step]
+        )
+
+    for part in range(2):
+        for step in range(steps):
+            fetch(step, part).start()
+    for step in range(steps):
+        fetch(step, 0).wait()
+        rows = pl.ds(step * depth, depth)
+        product = jnp.dot(
+            mid_ref[:, rows], held[rows, pl.ds(0, wide)], preferred_element_type=jnp.float32
+        )
+        if step == 0:
+            total[...] = product
+        else:
+            total[...] += product
+    hidden = (jax.nn.silu(total[:, :units]) * total[:, units:]).astype(jnp.bfloat16)
+    for step in range(steps):
+        fetch(step, 1).wait()
+        rows = pl.ds(step * depth, depth)
+        out_ref[:, rows] = lax.dot_general(
+            hidden,
+            held[rows, pl.ds(wide, units)],
+            (((1,), (1,)), ((), ())),
+            preferred_element_type=jnp.float32,
+        ).astype(jnp.bfloat16)
+
+
+def mix_channels(mid_rows, weights):
+    units, depth = weights.shape[1] // 3, 256
+    steps = weights.shape[0] // depth
+    return pl.pallas_call(
+        functools.partial(mixer_kernel, units, depth),
+        out_shape=jax.ShapeDtypeStruct(mid_rows.shape, jnp.bfloat16),
+        in_specs=[
+            pl.BlockSpec(memory_space=pltpu.VMEM),
+            pl.BlockSpec(memory_space=pl.ANY),
+        ],
+        out_specs=pl.BlockSpec(memory_space=pltpu.VMEM),
+        scratch_shapes=[
+            pltpu.VMEM(weights.shape, jnp.bfloat16),
+            pltpu.VMEM((mid_rows.shape[0], 2 * units), jnp.float32),
+            pltpu.SemaphoreType.DMA((2, steps)),
+        ],
+        compiler_params=pltpu.CompilerParams(vmem_limit_bytes=24 << 20),
+        cost_estimate=pl.CostEstimate(
+            flops=6 * mid_rows.size * units, bytes_accessed=2 * weights.size, transcendentals=0
+        ),
+        name="mix_channels",
+    )(mid_rows, weights)
 
 
 def body(
@@ -166,7 +224,7 @@
     tp_count = lax.axis_size("tp")
     tok_rows = queries.shape[0]
     own_count = tok_rows // tp_count
-    gate_whole, up_whole, down_whole = turned_gather((gate_in, up_in, down_out), SP, (0, 0, 1))
+    weights = gathered_weights(gate_in, up_in, down_out)
     gated = mix_tokens(queries, keys, values, decay_pre, out_gate, head_gain)
     mixed = sent_and_summed(
         jnp.dot(gated, out_proj, preferred_element_type=jnp.float32).astype(jnp.bfloat16), "tp", 0
@@ -175,12 +233,7 @@
     mid = layer_norm(ALPHA * own_resid.astype(jnp.float32) + mixed, mix_gain, mix_shift).astype(
         jnp.bfloat16
     )
-    hidden = expand_rows(gather_directly(mid, "tp", 0), gate_whole, up_whole)
-    ffn = sent_and_summed(
-        jnp.dot(hidden, down_whole, preferred_element_type=jnp.float32).astype(jnp.bfloat16),
-        "tp",
-        0,
-    )
+    ffn = sent_and_summed(mix_channels(gather_directly(mid, "tp", 0), weights), "tp", 0)
     finished = layer_norm(ALPHA * mid.astype(jnp.float32) + 0.5 * ffn, out_gain, out_shift).astype(
         jnp.bfloat16
     )

time: 183 us -> 163 us (0.89)
  blocking collectives: 114 us -> 64.4 us
  waiting for transfers between devices: 9.37 us -> 41.8 us
  matrix products: 13.9 us -> 3.01 us
  Pallas kernels: 0 us -> 5.87 us
  local copies, waits for them, and re-layouts: 2.73 us -> 7.01 us
  starting transfers between devices: 22.8 us -> 18.9 us
    all_gather x4 -> x0, blocking collectives: 75.5 us -> none  [carried_in(): lax.all_gather(part.astype(kind), axis)]
    all_to_all x0 -> x2, blocking collectives: none -> 24.7 us  [the longest x1 15.1 us: incoming_state(): lax.all_to_all(packed, col, split_axis=0, concat_axis=0, tiled=True)]
    all_gather x1, waiting for transfers between devices: 0.01 us -> 24.5 us  [gathered_weights(): lax.all_gather(jnp.concatenate([gate_in, up_in, down_out.T], axis=1), SP,...]
    all_to_all x1, starting transfers between devices: 22.7 us -> 8.89 us  [sent_and_summed(): lax.all_to_all(blocks, axis, split_axis=0, concat_axis=0, tiled=True)]
    dot_general x2 -> x0, matrix products: 10.4 us -> none  [the longest x1 7.24 us: body(): jnp.dot(hidden, down_whole, preferred_element_type=jnp.float32)]
    all_to_all x0 -> x1, starting transfers between devices: none -> 10 us  [from_everyone(): return lax.all_to_all(copies, axis, split_axis=0, concat_axis=0, tiled=True)]
    all_to_all x0 -> x1, waiting for transfers between devices: none -> 7.94 us  [from_everyone(): return lax.all_to_all(copies, axis, split_axis=0, concat_axis=0, tiled=True)]
    pallas_call x0 -> x1, Pallas kernels: none -> 5.87 us  [mix_channels(): pl.pallas_call(functools.partial(mixer_kernel, units, depth), out_shape=j...]
  transfers between devices with their start and end apart: 2 -> 3, of which waited for: 1 -> 3; matrix products, arithmetic and copies ran while one was open for 5% -> 7% of each run, Pallas kernels for 0% -> 0%
where the time goes in v1:
time: 163 us; the launch traced here: 162 us
  blocking collectives  64.4 us (40%)
  waiting for transfers between devices  41.8 us (26%)
  starting transfers between devices  18.9 us (12%)
  between operations  13.7 us (8%)
  other arithmetic  7.69 us (5%)
  local copies, waits for them, and re-layouts  7.01 us (4%)
  Pallas kernels  5.87 us (4%)
  matrix products  3.01 us (2%)
    all_to_all x2, blocking collectives, from_everyone(): return lax.all_to_all(copies, axis, split_axis=0, concat_axis=0, tiled=True)  25.5 us
    all_gather x1, waiting for transfers between devices, gathered_weights(): lax.all_gather(jnp.concatenate([gate_in, up_in, down_out.T], axis=1), SP,...  24.5 us
    all_to_all x1, blocking collectives, incoming_state(): lax.all_to_all(packed, col, split_axis=0, concat_axis=0, tiled=True)  15.1 us
    all_to_all x1, blocking collectives, sent_and_summed(): lax.all_to_all(blocks, axis, split_axis=0, concat_axis=0, tiled=True)  14.2 us
    all_to_all x1, starting transfers between devices, from_everyone(): return lax.all_to_all(copies, axis, split_axis=0, concat_axis=0, tiled=True)  10 us
    all_to_all x1, blocking collectives, incoming_state(): lax.all_to_all(entering, col, split_axis=0, concat_axis=0, tiled=True)  9.65 us
    all_to_all x1, waiting for transfers between devices, sent_and_summed(): lax.all_to_all(blocks, axis, split_axis=0, concat_axis=0, tiled=True)  9.35 us
    all_to_all x1, starting transfers between devices, sent_and_summed(): lax.all_to_all(blocks, axis, split_axis=0, concat_axis=0, tiled=True)  8.89 us
  transfers between devices with their start and end apart: 3, of which 3 were waited for; matrix products, arithmetic and copies ran while one was open for 7% of the time, Pallas kernels for 0%

profile of v1, /device:TPU:1, one launch (start us, length us, event | category | flops | bytes accessed | tf_op | source)
XLA Modules:
  0.0 162.5 jit_solution(4104594621051203479)
XLA Ops:
  6.5 1.7 %concatenate.17 = bf16[32,2112]{1,0:T(8,128)(2,1)} concatenate(bf16[32,704]{1,0:T(8,128)(2,1)} %param.27, bf16[32,704]{1,0:T(8,128)(2,1)} %param.28, bf16[32,704]{1,0:T(8,128)(2,1)} %bitcast.192), dimensions={1} | concatenate | bytes 270336 | tf_op jit(solution)/shard_map/concatenate | solution.py:63
  8.3 0.9 fusion.12
  9.4 0.8 convert_multiply_fusion.1
  10.2 1.2 convolution_bitcast_fusion.1
  11.4 0.8 while.13
  11.5 0.2 fusion.52
  11.9 0.2 fusion.52
  12.2 0.1 select_convert_fusion
  12.3 15.1 %all_to_all.35 = bf16[8,16,384]{2,1,0:T(8,128)(2,1)S(1)} all-to-all(bf16[8,16,384]{2,1,0:T(8,128)(2,1)S(1)} %pad_maximum_fusion), channel_id=1, replica_groups=mesh['sp_0'=8,'sp_1'=8,'tp'=8] {'sp_1'}, dimensions={0} | all-to-all | bytes 196608 | tf_op jit(solution)/shard_map/all_to_all | solution.py:42
  27.7 0.7 broadcast_in_dim.60
  28.4 10.0 %all-to-all-start.1 = ((bf16[8,16,384]{2,1,0:T(8,128)(2,1)}), bf16[8,16,384]{2,1,0:T(8,128)(2,1)S(1)}, u32[]{:S(2)}, u32[]{:S(2)}) async-start(bf16[8,16,384]{2,1,0:T(8,128)(2,1)} %broadcast_in_dim.60), calls=%async_computation.1 | async-start | bytes 196608 | tf_op jit(solution)/shard_map/all_to_all | solution.py:80
  38.4 7.9 %all-to-all-done.1 = bf16[8,16,384]{2,1,0:T(8,128)(2,1)S(1)} async-done(((bf16[8,16,384]{2,1,0:T(8,128)(2,1)}), bf16[8,16,384]{2,1,0:T(8,128)(2,1)S(1)}, u32[]{:S(2)}, u32[]{:S(2)}) %all-to-all-start.1) | async-done | bytes 98336 | tf_op jit(solution)/shard_map/all_to_all | solution.py:80
  46.5 0.1 constant_dynamic-update-slice_fusion.7
  47.1 9.6 %all_to_all.36 = bf16[8,16,256]{2,1,0:T(8,128)(2,1)S(1)} all-to-all(bf16[8,16,256]{2,1,0:T(8,128)(2,1)S(1)} %constant_dynamic-update-slice_fusion), channel_id=1, replica_groups=mesh['sp_0'=8,'sp_1'=8,'tp'=8] {'sp_1'}, dimensions={0} | all-to-all | bytes 131072 | tf_op jit(solution)/shard_map/all_to_all | solution.py:57
  56.8 0.3 multiply_reduce_fusion.2
  57.2 0.9 fusion.10
  58.2 1.1 convolution_convert_fusion
  59.3 8.9 %all-to-all-start.3 = ((bf16[8,16,2048]{2,1,0:T(8,128)(2,1)}), bf16[8,16,2048]{2,1,0:T(8,128)(2,1)S(1)}, u32[]{:S(2)}, u32[]{:S(2)}) async-start(bf16[8,16,2048]{2,1,0:T(8,128)(2,1)} %bitcast.52), calls=%async_computation.3 | async-start | bytes 1048576 | tf_op jit(solution)/shard_map/all_to_all | solution.py:74
  68.2 9.3 %all-to-all-done.3 = bf16[8,16,2048]{2,1,0:T(8,128)(2,1)S(1)} async-done(((bf16[8,16,2048]{2,1,0:T(8,128)(2,1)}), bf16[8,16,2048]{2,1,0:T(8,128)(2,1)S(1)}, u32[]{:S(2)}, u32[]{:S(2)}) %all-to-all-start.3) | async-done | bytes 524320 | tf_op jit(solution)/shard_map/all_to_all | solution.py:74
  77.6 1.0 fusion.17
  78.6 1.0 multiply_reduce_fusion.1
  79.6 0.9 add_convert_fusion.1
  80.6 12.8 %all_to_all.37 = bf16[8,16,2048]{2,1,0:T(8,128)(2,1)S(1)} all-to-all(bf16[8,16,2048]{2,1,0:T(8,128)(2,1)S(1)} %broadcast_in_dim.61), channel_id=1, replica_groups=mesh['sp_0'=8,'sp_1'=8,'tp'=8] {'tp'}, dimensions={0} | all-to-all | bytes 1048576 | tf_op jit(solution)/shard_map/all_to_all | solution.py:80
  93.4 24.5 %all-gather.2.cloned.1.call-done.weights_ref = bf16[2048,2112]{1,0:T(8,128)(2,1)} async-done(((bf16[32,2112]{1,0:T(8,128)(2,1)}), bf16[2048,2112]{1,0:T(8,128)(2,1)}) %all-gather.2.cloned.1.call-update) | async-done | bytes 8650768 | tf_op jit(solution)/shard_map/all_gather | solution.py:62
  117.8 3.5 %copy-done.1 = bf16[2048,2112]{1,0:T(8,128)(2,1)S(1)} copy-done((bf16[2048,2112]{1,0:T(8,128)(2,1)S(1)}, bf16[2048,2112]{1,0:T(8,128)(2,1)}, u32[]{:S(2)}) %copy-start.1) | copy-done | bytes 8650776
  121.4 5.9 %mix_channels.1 = bf16[128,2048]{1,0:T(8,128)(2,1)S(1)} custom-call(bf16[128,2048]{1,0:T(8,128)(2,1)S(1)} %bitcast.181, bf16[2048,2112]{1,0:T(8,128)(2,1)S(1)} %copy-done.1), custom_call_target="tpu_custom_call" | custom-call | flops 1107296256 | bytes 8650752 | tf_op jit(solution)/shard_map/mix_channels/pallas_call | solution.py:186
  127.3 14.2 %all_to_all.38 = bf16[8,16,2048]{2,1,0:T(8,128)(2,1)S(1)} all-to-all(bf16[8,16,2048]{2,1,0:T(8,128)(2,1)S(1)} %bitcast.182), channel_id=1, replica_groups=mesh['sp_0'=8,'sp_1'=8,'tp'=8] {'tp'}, dimensions={0} | all-to-all | bytes 1048576 | tf_op jit(solution)/shard_map/all_to_all | solution.py:74
  141.5 0.1 fusion.16
  141.7 0.2 multiply_reduce_fusion
  141.9 0.1 add_convert_fusion
  142.1 12.8 %all_to_all.39 = bf16[8,16,2048]{2,1,0:T(8,128)(2,1)S(1)} all-to-all(bf16[8,16,2048]{2,1,0:T(8,128)(2,1)S(1)} %broadcast_in_dim.62), channel_id=1, replica_groups=mesh['sp_0'=8,'sp_1'=8,'tp'=8] {'tp'}, dimensions={0} | all-to-all | bytes 1048576 | tf_op jit(solution)/shard_map/all_to_all | solution.py:80
  154.8 0.8 copy.38
  (60 shorter events, 1.8 us)
Async XLA Ops:
  6.5 51.6 %copy-start = (bf16[256,2048]{1,0:T(8,128)(2,1)S(1)}, bf16[256,2048]{1,0:T(8,128)(2,1)}, u32[]{:S(2)}) copy-start(bf16[256,2048]{1,0:T(8,128)(2,1)} %param.24) | copy-start | bytes 3145732
  6.5 73.1 %copy-start.3 = (f32[2048]{0:T(1024)S(1)}, f32[2048]{0:T(1024)}, u32[]{:S(2)}) copy-start(f32[2048]{0:T(1024)} %param.25) | copy-start | bytes 24580
  6.5 73.1 %copy-start.2 = (f32[2048]{0:T(1024)S(1)}, f32[2048]{0:T(1024)}, u32[]{:S(2)}) copy-start(f32[2048]{0:T(1024)} %param.26) | copy-start | bytes 24580
  6.5 111.3 %all-gather.2.cloned.1.call-start = ((), (), s32[]{:S(2)}) async-start(), calls=%async_computation.7 | async-start | bytes 9052160 | tf_op jit(solution)/shard_map/all_gather | solution.py:62
  28.4 18.0 %all-to-all-start.1 = ((bf16[8,16,384]{2,1,0:T(8,128)(2,1)}), bf16[8,16,384]{2,1,0:T(8,128)(2,1)S(1)}, u32[]{:S(2)}, u32[]{:S(2)}) async-start(bf16[8,16,384]{2,1,0:T(8,128)(2,1)} %broadcast_in_dim.60), calls=%async_computation.1 | async-start | bytes 196608 | tf_op jit(solution)/shard_map/all_to_all | solution.py:80
  58.1 83.8 %copy-start.4 = (f32[2048]{0:T(1024)S(1)}, f32[2048]{0:T(1024)}, u32[]{:S(2)}) copy-start(f32[2048]{0:T(1024)} %param.31) | copy-start | bytes 24580
  58.1 83.8 %copy-start.5 = (f32[2048]{0:T(1024)S(1)}, f32[2048]{0:T(1024)}, u32[]{:S(2)}) copy-start(f32[2048]{0:T(1024)} %param.30) | copy-start | bytes 24580
  59.3 18.2 %all-to-all-start.3 = ((bf16[8,16,2048]{2,1,0:T(8,128)(2,1)}), bf16[8,16,2048]{2,1,0:T(8,128)(2,1)S(1)}, u32[]{:S(2)}, u32[]{:S(2)}) async-start(bf16[8,16,2048]{2,1,0:T(8,128)(2,1)} %bitcast.52), calls=%async_computation.3 | async-start | bytes 1048576 | tf_op jit(solution)/shard_map/all_to_all | solution.py:74
  117.8 3.5 %copy-start.1 = (bf16[2048,2112]{1,0:T(8,128)(2,1)S(1)}, bf16[2048,2112]{1,0:T(8,128)(2,1)}, u32[]{:S(2)}) copy-start(bf16[2048,2112]{1,0:T(8,128)(2,1)} %all-gather.2.cloned.1.call-done.weights_ref) | copy-start | bytes 25952260
Sparse Core Ops, SparseCore 0:
  10.3 107.4 all-gather.1

commit v2 on v1

--- a/solution.py
+++ b/solution.py
@@ -29,75 +29,154 @@
     return jnp.concatenate([state, extra], axis=-1).astype(jnp.bfloat16)
 
 
-def apart(packed):
-    whole = packed.astype(jnp.float32)
-    return whole[..., :HV], whole[..., HV:].sum(axis=-1)
-
-
-def incoming_state(own_state, own_log):
-    row, col = SP
-    count = lax.axis_size(col)
-    packed = with_decay(own_state, own_log).reshape(count, -1, HV + 128)
-    states, logs = apart(
-        lax.all_to_all(packed, col, split_axis=0, concat_axis=0, tiled=True)
-    )
-    before, passed = [jnp.zeros_like(states[0])], [jnp.zeros_like(logs[0])]
-    for k in range(count):
-        before.append(jnp.exp(logs[k])[:, None] * before[-1] + states[k])
-        passed.append(passed[-1] + logs[k])
-    totals, total_logs = apart(from_everyone(with_decay(before[-1], passed[-1]), row))
-    earlier = jnp.zeros_like(totals[0])
-    for k in range(lax.axis_size(row)):
-        earlier = jnp.where(
-            k < lax.axis_index(row), jnp.exp(total_logs[k])[:, None] * earlier + totals[k], earlier
+def prefix_kernel(packed_ref, out_ref):
+    count = packed_ref.shape[0]
+    row = lax.broadcasted_iota(jnp.int32, (count, count), 0)
+    col = lax.broadcasted_iota(jnp.int32, (count, count), 1)
+    earlier = (col < row).astype(jnp.float32)
+    for k in range(packed_ref.shape[1] // (HV + 128)):
+        at = k * (HV + 128)
+        logs = packed_ref[:, at + HV : at + HV + 128].astype(jnp.float32)
+        ends = jnp.dot(earlier, logs, precision=lax.Precision.HIGHEST)
+        ends = jnp.sum(ends, axis=1, keepdims=True)
+        across = lax.dot_general(
+            jnp.ones((8, 128), jnp.float32),
+            logs,
+            (((1,), (1,)), ((), ())),
+            precision=lax.Precision.HIGHEST,
         )
-    entering = jnp.stack(
-        [jnp.exp(passed[k])[:, None] * earlier + before[k] for k in range(count)]
-    ).astype(jnp.bfloat16)
-    back = lax.all_to_all(entering, col, split_axis=0, concat_axis=0, tiled=True)
-    return back.reshape(own_state.shape).astype(jnp.float32)
-
-
-def gathered_weights(gate_in, up_in, down_out):
+        starts = lax.dot_general(
+            across,
+            (col <= row).astype(jnp.float32),
+            (((1,), (1,)), ((), ())),
+            precision=lax.Precision.HIGHEST,
+        )[:1]
+        decay = jnp.where(col < row, jnp.exp(jnp.minimum(ends - starts, 0.0)), 0.0)
+        out_ref[:, k * HV : (k + 1) * HV] = jnp.dot(
+            decay,
+            packed_ref[:, at : at + HV].astype(jnp.float32),
+            precision=lax.Precision.HIGHEST,
+        ).astype(jnp.bfloat16)
+
+
+def incoming_state(arrived, shape):
+    count, channels = arrived.shape[:2]
+    entering = pl.pallas_call(
+        prefix_kernel,
+        out_shape=jax.ShapeDtypeStruct((count, channels * HV), jnp.bfloat16),
+        in_specs=[pl.BlockSpec(memory_space=pltpu.VMEM)],
+        out_specs=pl.BlockSpec(memory_space=pltpu.VMEM),
+        compiler_params=pltpu.CompilerParams(vmem_limit_bytes=8 << 20),
+        name="prefix",
+    )(arrived.reshape(count, -1))
+    entering = entering.reshape(count, channels, HV)
+    back = lax.all_to_all(entering, SP, split_axis=0, concat_axis=0, tiled=True)
+    return back.reshape(shape).astype(jnp.float32)
+
+
+def ring_groups(first):
+    rows, cols, parts = (lax.axis_size(axis) for axis in (*SP, "tp"))
+    place = lambda row, col, part: (row * cols + col) * parts + part
+    along_cols = lambda part: [
+        [place(row, col, part) for col in range(cols)] for row in range(rows)
+    ]
+    along_rows = lambda part: [
+        [place(row, col, part) for row in range(rows)] for col in range(cols)
+    ]
+    return [
+        group
+        for part in range(parts)
+        for group in (along_cols if (part % 2 == 0) == first else along_rows)(part)
+    ]
+
+
+def nearby_weights(gate_in, up_in, down_out):
+    own = jnp.concatenate([gate_in, up_in, down_out.T], axis=1)
+    copies = jnp.broadcast_to(own, (lax.axis_size(SP[0]), *own.shape))
+    arrived = lax.all_to_all(
+        copies,
+        (*SP, "tp"),
+        split_axis=0,
+        concat_axis=0,
+        tiled=True,
+        axis_index_groups=ring_groups(True),
+    )
+    return arrived.reshape(-1, own.shape[1])
+
+
+def gathered_weights(nearby):
     return lax.all_gather(
-        jnp.concatenate([gate_in, up_in, down_out.T], axis=1), SP, axis=0, tiled=True
-    )
-
-
-def split_up(array, dim, count):
-    before, after = (array.shape[:dim], array.shape[dim + 1 :])
-    return jnp.moveaxis(array.reshape(*before, count, -1, *after), dim, 0)
-
-
-def sent_and_summed(array, axis, dim):
-    blocks = split_up(array, dim, lax.axis_size(axis))
-    arrived = lax.all_to_all(blocks, axis, split_axis=0, concat_axis=0, tiled=True)
-    return arrived.astype(jnp.float32).sum(axis=0)
-
-
-def from_everyone(array, axis):
-    copies = jnp.broadcast_to(array, (lax.axis_size(axis), *array.shape))
-    return lax.all_to_all(copies, axis, split_axis=0, concat_axis=0, tiled=True)
-
-
-def in_order(blocks, dim):
-    lengths = list(blocks.shape[1:])
-    lengths[dim] *= blocks.shape[0]
-    return jnp.moveaxis(blocks, 0, dim).reshape(lengths)
-
-
-def gather_directly(array, axis, dim):
-    blocks = from_everyone(array, axis)
-    return in_order(blocks, dim)
-
-
-def layer_norm(inputs, gain, shift):
+        nearby, (*SP, "tp"), axis=0, tiled=True, axis_index_groups=ring_groups(False)
+    )
+
+
+def swapped(rows, outer, width):
+    lanes = 128
+    inner = rows.shape[1] // (outer * width)
+    lane = lax.broadcasted_iota(jnp.int32, (rows.shape[0], lanes), 1) // width
+    tiles = []
+    for tile in range(rows.shape[1] // lanes):
+        made = None
+        for k in range(lanes // width):
+            new = tile * (lanes // width) + k
+            old = (new % outer) * inner + new // outer
+            source, offset = divmod(old * width, lanes)
+            piece = rows[:, source * lanes : (source + 1) * lanes]
+            shift = (k * width - offset) % lanes
+            if shift:
+                piece = pltpu.roll(piece, shift, 1)
+            made = piece if made is None else jnp.where(lane == k, piece, made)
+        tiles.append(made)
+    return jnp.concatenate(tiles, axis=1)
+
+
+def settle_kernel(
+    scale, outer, width, back, forth, arrived_ref, before_ref, gain_ref, shift_ref, *out_refs
+):
+    parts = arrived_ref.shape[0]
+    even, odd = (
+        sum(arrived_ref[k].astype(jnp.float32) for k in range(start, parts, 2))
+        for start in range(2)
+    )
+    if back:
+        odd = swapped(odd, outer, width)
+    inputs = ALPHA * before_ref[...].astype(jnp.float32) + scale * (even + odd)
     center = inputs - jnp.mean(inputs, axis=-1, keepdims=True)
     spread = jnp.mean(center * center, axis=-1, keepdims=True)
-    return center * lax.rsqrt(spread + LN_EPS) * gain + shift
-
-
-def mix_tokens(queries, keys, values, decay_pre, out_gate, head_gain):
+    rows = center * lax.rsqrt(spread + LN_EPS) * gain_ref[...] + shift_ref[...]
+    rows = rows.astype(jnp.bfloat16)
+    turned = rows
+    if forth:
+        turned = swapped(rows.astype(jnp.float32), outer, width).astype(jnp.bfloat16)
+        out_refs[1][...] = rows
+    for k in range(parts):
+        out_refs[0][k] = turned if k % 2 else rows
+
+
+def settle(arrived, before, gain, shift, scale, back, forth):
+    outer = lax.axis_size(SP[0])
+    width = before.shape[1] // (outer * lax.axis_size(SP[1]))
+    copies = jax.ShapeDtypeStruct(arrived.shape, jnp.bfloat16)
+    kept = jax.ShapeDtypeStruct(before.shape, jnp.bfloat16)
+    vmem = pl.BlockSpec(memory_space=pltpu.VMEM)
+    out = pl.pallas_call(
+        functools.partial(settle_kernel, scale, outer, width, back, forth),
+        out_shape=(copies, kept) if forth else (copies,),
+        in_specs=[vmem] * 4,
+        out_specs=(vmem, vmem) if forth else (vmem,),
+        compiler_params=pltpu.CompilerParams(vmem_limit_bytes=8 << 20),
+        name="settle",
+    )(arrived, before, gain[None], shift[None])
+    return out
+
+
+def sent(array, axis):
+    count = lax.axis_size(axis)
+    blocks = array.reshape(count, -1, array.shape[-1])
+    return lax.all_to_all(blocks, axis, split_axis=0, concat_axis=0, tiled=True)
+
+
+def mix_tokens(queries, keys, values, decay_pre, out_gate, head_gain, nearby):
     tok_rows = queries.shape[0]
     local_heads = queries.shape[1] // HK
     blocks = tok_rows // SPAN
@@ -126,7 +205,11 @@
         advance, jnp.zeros((local_heads, HK, HV), jnp.float32), (last, updates, scaled_q)
     )
     block_ends = jnp.cumsum(last, axis=0)
-    incoming = incoming_state(own_state[0], block_ends[-1, 0])[None]
+    packed = with_decay(own_state[0], block_ends[-1, 0]).reshape(lax.axis_size(SP), -1, HV + 128)
+    packed, nearby = lax.optimization_barrier((packed, nearby))
+    weights = gathered_weights(nearby)
+    arrived = lax.all_to_all(packed, SP, split_axis=0, concat_axis=0, tiled=True)
+    incoming = incoming_state(arrived, own_state.shape)
     carried = jnp.einsum(
         "xepj,pjw->xepw",
         scaled_q * jnp.exp(block_ends)[:, None],
@@ -139,9 +222,10 @@
         * lax.rsqrt(jnp.mean(state_readout * state_readout, axis=-1, keepdims=True) + RMS_EPS)
         * head_gain
     )
-    return (
+    gated = (
         normed.reshape(tok_rows, local_heads * HV) * jax.nn.silu(out_gate.astype(jnp.float32))
     ).astype(jnp.bfloat16)
+    return gated, weights
 
 
 def mixer_kernel(units, depth, mid_ref, weights_ref, out_ref, held, total, sems):
@@ -188,7 +272,7 @@
         out_shape=jax.ShapeDtypeStruct(mid_rows.shape, jnp.bfloat16),
         in_specs=[
             pl.BlockSpec(memory_space=pltpu.VMEM),
-            pl.BlockSpec(memory_space=pl.ANY),
+            pl.BlockSpec(memory_space=pltpu.HBM),
         ],
         out_specs=pl.BlockSpec(memory_space=pltpu.VMEM),
         scratch_shapes=[
@@ -196,7 +280,7 @@
             pltpu.VMEM((mid_rows.shape[0], 2 * units), jnp.float32),
             pltpu.SemaphoreType.DMA((2, steps)),
         ],
-        compiler_params=pltpu.CompilerParams(vmem_limit_bytes=24 << 20),
+        compiler_params=pltpu.CompilerParams(vmem_limit_bytes=56 << 20),
         cost_estimate=pl.CostEstimate(
             flops=6 * mid_rows.size * units, bytes_accessed=2 * weights.size, transcendentals=0
         ),
@@ -221,23 +305,18 @@
     out_gain,
     out_shift,
 ):
-    tp_count = lax.axis_size("tp")
-    tok_rows = queries.shape[0]
-    own_count = tok_rows // tp_count
-    weights = gathered_weights(gate_in, up_in, down_out)
-    gated = mix_tokens(queries, keys, values, decay_pre, out_gate, head_gain)
-    mixed = sent_and_summed(
-        jnp.dot(gated, out_proj, preferred_element_type=jnp.float32).astype(jnp.bfloat16), "tp", 0
-    )
+    own_count = queries.shape[0] // lax.axis_size("tp")
+    nearby = nearby_weights(gate_in, up_in, down_out)
+    gated, weights = mix_tokens(queries, keys, values, decay_pre, out_gate, head_gain, nearby)
+    mixed = jnp.dot(gated, out_proj, preferred_element_type=jnp.float32).astype(jnp.bfloat16)
     own_resid = lax.dynamic_slice_in_dim(resid, lax.axis_index("tp") * own_count, own_count, 0)
-    mid = layer_norm(ALPHA * own_resid.astype(jnp.float32) + mixed, mix_gain, mix_shift).astype(
-        jnp.bfloat16
-    )
-    ffn = sent_and_summed(mix_channels(gather_directly(mid, "tp", 0), weights), "tp", 0)
-    finished = layer_norm(ALPHA * mid.astype(jnp.float32) + 0.5 * ffn, out_gain, out_shift).astype(
-        jnp.bfloat16
-    )
-    return gather_directly(finished, "tp", 0)
+    copies, mid = settle(
+        sent(mixed, "tp"), own_resid, mix_gain, mix_shift, 1.0, back=False, forth=True
+    )
+    mid_rows = sent(copies, "tp").reshape(resid.shape)
+    ffn = sent(mix_channels(mid_rows, weights), "tp")
+    (finished,) = settle(ffn, mid, out_gain, out_shift, 0.5, back=True, forth=False)
+    return sent(finished, "tp").reshape(resid.shape)
 
 
 def solution(mesh):

time: 163 us -> 152 us (0.933)
  waiting for transfers between devices: 41.8 us -> 25.3 us
  blocking collectives: 64.4 us -> 74.1 us
  other arithmetic: 7.69 us -> 0.79 us
  Pallas kernels: 5.87 us -> 10.1 us
  local copies, waits for them, and re-layouts: 7.01 us -> 5.18 us
    all_gather x1, waiting for transfers between devices: 24.5 us -> 0.01 us  [gathered_weights(): lax.all_gather(nearby, (*SP, 'tp'), axis=0, tiled=True, axis_index_groups...]
    all_to_all x5, blocking collectives: 64.4 us -> 74.1 us  [the longest x3 39.9 us: sent(): return lax.all_to_all(blocks, axis, split_axis=0, concat_axis=0, tiled=True)]
    all_to_all x2, waiting for transfers between devices: 17.3 us -> 25.3 us  [the longest x1 16.8 us: nearby_weights(): lax.all_to_all(copies, (*SP, 'tp'), split_axis=0, concat_axis=0, tiled=Tr...]
    reduce_sum x8 -> x0, other arithmetic: 2.68 us -> none  [the longest x2 1.24 us: layer_norm(): spread = jnp.mean(center * center, axis=-1, keepdims=True)]
    unnamed x14 -> x27, local copies, waits for them, and re-layouts: 4.35 us -> 1.85 us
    pallas_call x1, Pallas kernels: 5.87 us -> 8.17 us  [mix_channels(): pl.pallas_call(functools.partial(mixer_kernel, units, depth), out_shape=j...]
    pallas_call x0 -> x3, Pallas kernels: none -> 1.96 us  [the longest x1 1.17 us: incoming_state(): pl.pallas_call(prefix_kernel, out_shape=jax.ShapeDtypeStruct((count, chan...]
    convert_element_type x5 -> x1, other arithmetic: 2 us -> 0.1 us  [mix_tokens(): gated = (normed.reshape(tok_rows, local_heads * HV) * jax.nn.silu(out_gat...]
  transfers between devices with their start and end apart: 3 -> 3, of which waited for: 3 -> 2; matrix products, arithmetic and copies ran while one was open for 7% -> 3% of each run, Pallas kernels for 0% -> 1%
where the time goes in v2:
time: 152 us; the launch traced here: 151 us
  blocking collectives  74.1 us (49%)
  waiting for transfers between devices  25.3 us (17%)
  starting transfers between devices  19.9 us (13%)
  between operations  13.6 us (9%)
  Pallas kernels  10.1 us (7%)
  local copies, waits for them, and re-layouts  5.18 us (3%)
  matrix products  2.16 us (1%)
    all_to_all x3, blocking collectives, sent(): return lax.all_to_all(blocks, axis, split_axis=0, concat_axis=0, tiled=True)  39.9 us
    all_to_all x1, blocking collectives, mix_tokens(): lax.all_to_all(packed, SP, split_axis=0, concat_axis=0, tiled=True)  19 us
    all_to_all x1, waiting for transfers between devices, nearby_weights(): lax.all_to_all(copies, (*SP, 'tp'), split_axis=0, concat_axis=0, tiled=Tr...  16.8 us
    all_to_all x1, blocking collectives, incoming_state(): back = lax.all_to_all(entering, SP, split_axis=0, concat_axis=0, tiled=True)  15.2 us
    all_to_all x1, starting transfers between devices, nearby_weights(): lax.all_to_all(copies, (*SP, 'tp'), split_axis=0, concat_axis=0, tiled=Tr...  11 us
    all_to_all x1, starting transfers between devices, sent(): return lax.all_to_all(blocks, axis, split_axis=0, concat_axis=0, tiled=True)  8.86 us
    all_to_all x1, waiting for transfers between devices, sent(): return lax.all_to_all(blocks, axis, split_axis=0, concat_axis=0, tiled=True)  8.5 us
    pallas_call x1, Pallas kernels, mix_channels(): pl.pallas_call(functools.partial(mixer_kernel, units, depth), out_shape=j...  8.17 us
  transfers between devices with their start and end apart: 3, of which 2 were waited for; matrix products, arithmetic and copies ran while one was open for 3% of the time, Pallas kernels for 1%

profile of v2, /device:TPU:1, one launch (start us, length us, event | category | flops | bytes accessed | tf_op | source)
XLA Modules:
  0.0 151.3 jit_solution(5874584676957630389)
XLA Ops:
  6.5 1.0 concatenate.12
  7.6 1.1 broadcast_in_dim.53
  8.7 11.0 %all-to-all-start = ((bf16[8,32,2112]{2,1,0:T(8,128)(2,1)}), bf16[8,32,2112]{2,1,0:T(8,128)(2,1)S(1)}, u32[]{:S(2)}, u32[]{:S(2)}) async-start(bf16[8,32,2112]{2,1,0:T(8,128)(2,1)} %broadcast_in_dim.53), calls=%async_computation | async-start | bytes 2228224 | tf_op jit(solution)/shard_map/all_to_all | solution.py:96
  19.8 0.1 fusion.17
  19.9 0.1 squeeze.16
  20.1 0.3 convolution_bitcast_fusion.1
  20.5 0.8 while.13
  20.5 0.1 bitcast_add_fusion.2
  20.6 0.2 fusion.32
  20.9 0.1 bitcast_add_fusion.2
  21.0 0.2 fusion.32
  21.3 0.2 select_convert_fusion
  21.5 0.1 pad_maximum_fusion
  21.6 16.8 %all-to-all-done = bf16[8,32,2112]{2,1,0:T(8,128)(2,1)S(1)} async-done(((bf16[8,32,2112]{2,1,0:T(8,128)(2,1)}), bf16[8,32,2112]{2,1,0:T(8,128)(2,1)S(1)}, u32[]{:S(2)}, u32[]{:S(2)}) %all-to-all-start) | async-done | bytes 1081376 | tf_op jit(solution)/shard_map/all_to_all | solution.py:96
  38.4 1.0 copy-done.5
  39.4 19.0 %all_to_all.35 = bf16[64,2,384]{2,1,0:T(2,128)(2,1)S(1)} all-to-all(bf16[64,2,384]{2,1,0:T(2,128)(2,1)S(1)} %pad_maximum_fusion), channel_id=1, replica_groups=mesh['sp_0'=8,'sp_1'=8,'tp'=8] {'sp_0','sp_1'}, dimensions={0} | all-to-all | bytes 196608 | tf_op jit(solution)/shard_map/all_to_all | solution.py:211
  58.4 1.2 prefix.1
  59.6 15.2 %all_to_all.36 = bf16[64,2,256]{2,1,0:T(2,128)(2,1)S(1)} all-to-all(bf16[64,2,256]{2,1,0:T(2,128)(2,1)S(1)} %reshape.196), channel_id=1, replica_groups=mesh['sp_0'=8,'sp_1'=8,'tp'=8] {'sp_0','sp_1'}, dimensions={0} | all-to-all | bytes 131072 | tf_op jit(solution)/shard_map/all_to_all | solution.py:73
  74.9 0.3 multiply_reduce_fusion
  75.2 0.1 rsqrt.12
  75.3 0.1 fusion.10
  75.4 1.1 convolution_convert_fusion
  76.5 8.9 %all-to-all-start.3 = ((bf16[8,16,2048]{2,1,0:T(8,128)(2,1)}), bf16[8,16,2048]{2,1,0:T(8,128)(2,1)S(1)}, u32[]{:S(2)}, u32[]{:S(2)}) async-start(bf16[8,16,2048]{2,1,0:T(8,128)(2,1)} %bitcast.20), calls=%async_computation.3 | async-start | bytes 1048576 | tf_op jit(solution)/shard_map/all_to_all | solution.py:176
  85.4 0.8 constant_dynamic-slice_fusion.2.before_ref
  86.2 8.5 %all-to-all-done.3.arrived_ref = bf16[8,16,2048]{2,1,0:T(8,128)(2,1)S(1)} async-done(((bf16[8,16,2048]{2,1,0:T(8,128)(2,1)}), bf16[8,16,2048]{2,1,0:T(8,128)(2,1)S(1)}, u32[]{:S(2)}, u32[]{:S(2)}) %all-to-all-start.3) | async-done | bytes 524320 | tf_op jit(solution)/shard_map/all_to_all | solution.py:176
  94.7 0.4 settle.2
  95.1 13.4 %all_to_all.37 = bf16[8,16,2048]{2,1,0:T(8,128)(2,1)} all-to-all(bf16[8,16,2048]{2,1,0:T(8,128)(2,1)S(1)} %get-tuple-element.45), channel_id=1, replica_groups=mesh['sp_0'=8,'sp_1'=8,'tp'=8] {'tp'}, dimensions={0} | all-to-all | bytes 1048576 | tf_op jit(solution)/shard_map/all_to_all | solution.py:176
  108.5 8.2 %mix_channels.1 = bf16[128,2048]{1,0:T(8,128)(2,1)} custom-call(bf16[128,2048]{1,0:T(8,128)(2,1)} %bitcast.92, bf16[2048,2112]{1,0:T(8,128)(2,1)} %all-gather.2.cloned.1.call-done.weights_ref), custom_call_target="tpu_custom_call" | custom-call | flops 1107296256 | bytes 8650752 | tf_op jit(solution)/shard_map/mix_channels/pallas_call | solution.py:270
  116.7 13.8 %all_to_all.38.arrived_ref = bf16[8,16,2048]{2,1,0:T(8,128)(2,1)S(1)} all-to-all(bf16[8,16,2048]{2,1,0:T(8,128)(2,1)} %bitcast.93), channel_id=1, replica_groups=mesh['sp_0'=8,'sp_1'=8,'tp'=8] {'tp'}, dimensions={0} | all-to-all | bytes 1048576 | tf_op jit(solution)/shard_map/all_to_all | solution.py:176
  130.5 0.4 settle.3
  130.9 12.8 %all_to_all.39 = bf16[8,16,2048]{2,1,0:T(8,128)(2,1)S(1)} all-to-all(bf16[8,16,2048]{2,1,0:T(8,128)(2,1)S(1)} %settle.3), channel_id=1, replica_groups=mesh['sp_0'=8,'sp_1'=8,'tp'=8] {'tp'}, dimensions={0} | all-to-all | bytes 1048576 | tf_op jit(solution)/shard_map/all_to_all | solution.py:176
  143.6 0.8 copy.36
  (46 shorter events, 0.4 us)
Async XLA Ops:
  6.5 68.8 %copy-start = (bf16[256,2048]{1,0:T(8,128)(2,1)S(1)}, bf16[256,2048]{1,0:T(8,128)(2,1)}, u32[]{:S(2)}) copy-start(bf16[256,2048]{1,0:T(8,128)(2,1)} %param.24) | copy-start | bytes 3145732
  8.7 11.1 %copy-start.6 = (f32[128,128]{1,0:T(8,128)S(1)}, f32[128,128]{1,0:T(8,128)}, u32[]{:S(2)}) copy-start(f32[128,128]{1,0:T(8,128)} %param.21) | copy-start | bytes 196612
  8.7 11.4 %copy-start.9 = (bf16[128,128]{1,0:T(8,128)(2,1)S(1)}, bf16[128,128]{1,0:T(8,128)(2,1)}, u32[]{:S(2)}) copy-start(bf16[128,128]{1,0:T(8,128)(2,1)} %param.18) | copy-start | bytes 98308
  8.7 11.5 %copy-start.7 = (bf16[128,256]{1,0:T(8,128)(2,1)S(1)}, bf16[128,256]{1,0:T(8,128)(2,1)}, u32[]{:S(2)}) copy-start(bf16[128,256]{1,0:T(8,128)(2,1)} %param.20) | copy-start | bytes 196612
  8.7 11.5 %copy-start.10 = (bf16[128,128]{1,0:T(8,128)(2,1)S(1)}, bf16[128,128]{1,0:T(8,128)(2,1)}, u32[]{:S(2)}) copy-start(bf16[128,128]{1,0:T(8,128)(2,1)} %param.19) | copy-start | bytes 98308
  8.7 29.7 %all-to-all-start = ((bf16[8,32,2112]{2,1,0:T(8,128)(2,1)}), bf16[8,32,2112]{2,1,0:T(8,128)(2,1)S(1)}, u32[]{:S(2)}, u32[]{:S(2)}) async-start(bf16[8,32,2112]{2,1,0:T(8,128)(2,1)} %broadcast_in_dim.53), calls=%async_computation | async-start | bytes 2228224 | tf_op jit(solution)/shard_map/all_to_all | solution.py:96
  19.7 88.8 %all-gather.2.cloned.1.call-start = ((), (), s32[]{:S(2)}) async-start(), calls=%async_computation.7 | async-start | bytes 10027008 | tf_op jit(solution)/shard_map/all_gather | solution.py:108
  38.4 1.0 copy-start.5
  38.4 36.9 %copy-start.8 = (bf16[128,256]{1,0:T(8,128)(2,1)S(1)}, bf16[128,256]{1,0:T(8,128)(2,1)}, u32[]{:S(2)}) copy-start(bf16[128,256]{1,0:T(8,128)(2,1)} %param.22) | copy-start | bytes 196612
  38.4 36.9 %copy-start.11 = (f32[256]{0:T(256)S(1)}, f32[256]{0:T(256)}, u32[]{:S(2)}) copy-start(f32[256]{0:T(256)} %param.23) | copy-start | bytes 3076
  75.4 19.3 %copy-start.1 = (f32[2048]{0:T(1024)S(1)}, f32[2048]{0:T(1024)}, u32[]{:S(2)}) copy-start(f32[2048]{0:T(1024)} %param.25) | copy-start | bytes 24580
  75.4 19.3 %copy-start.2 = (f32[2048]{0:T(1024)S(1)}, f32[2048]{0:T(1024)}, u32[]{:S(2)}) copy-start(f32[2048]{0:T(1024)} %param.26) | copy-start | bytes 24580
  76.5 18.2 %all-to-all-start.3 = ((bf16[8,16,2048]{2,1,0:T(8,128)(2,1)}), bf16[8,16,2048]{2,1,0:T(8,128)(2,1)S(1)}, u32[]{:S(2)}, u32[]{:S(2)}) async-start(bf16[8,16,2048]{2,1,0:T(8,128)(2,1)} %bitcast.20), calls=%async_computation.3 | async-start | bytes 1048576 | tf_op jit(solution)/shard_map/all_to_all | solution.py:176
  108.5 21.9 %copy-start.3 = (f32[2048]{0:T(1024)S(1)}, f32[2048]{0:T(1024)}, u32[]{:S(2)}) copy-start(f32[2048]{0:T(1024)} %param.30) | copy-start | bytes 24580
  108.5 21.9 %copy-start.4 = (f32[2048]{0:T(1024)S(1)}, f32[2048]{0:T(1024)}, u32[]{:S(2)}) copy-start(f32[2048]{0:T(1024)} %param.31) | copy-start | bytes 24580
Sparse Core Ops, SparseCore 0:
  39.5 58.7 all-gather.1

commit v3 on v2

--- a/solution.py
+++ b/solution.py
@@ -130,44 +130,115 @@
     return jnp.concatenate(tiles, axis=1)
 
 
+def collected_projection(out_proj):
+    parts = lax.axis_size("tp")
+    chips, wide = parts // 2, out_proj.shape[1] // 2
+    first = lax.axis_index("tp") % 2 == 0
+    left, right = out_proj[:, :wide], out_proj[:, wide:]
+    swap = [(part, part ^ 1) for part in range(parts)]
+    other = lax.ppermute(jnp.where(first, right, left), "tp", swap)
+    own = jnp.where(first, left, right)
+    block = jnp.concatenate([jnp.where(first, own, other), jnp.where(first, other, own)], axis=0)
+    blocks = [block]
+    for step in (2, 1, 3)[: chips - 1]:
+        path = [(part, (part + 2 * step) % parts) for part in range(parts)]
+        blocks.append(lax.ppermute(block, "tp", path))
+    return blocks
+
+
+def project_kernel(steps, place_ref, gated_ref, *refs):
+    out_ref = refs[-1]
+    chip, depth = place_ref[0] // 2, gated_ref.shape[2]
+    count = gated_ref.shape[0] // 2
+    total = None
+    for step, block_ref in zip(steps, refs[:-1]):
+        source = lax.rem(chip + (count - step), count)
+        for core in range(2):
+            product = jnp.dot(
+                gated_ref[2 * source + core],
+                block_ref[core * depth : (core + 1) * depth],
+                preferred_element_type=jnp.float32,
+            )
+            total = product if total is None else total + product
+    out_ref[...] = total.astype(jnp.bfloat16)
+
+
+def middle_kernel(
+    outer, width, place_ref, own_ref, other_ref, before_ref, gain_ref, shift_ref, mid_ref, turned_ref
+):
+    own, other = own_ref[...].astype(jnp.float32), other_ref[...].astype(jnp.float32)
+    odd = lax.rem(place_ref[0], 2) == 1
+    mixed = jnp.concatenate([jnp.where(odd, other, own), jnp.where(odd, own, other)], axis=1)
+    inputs = ALPHA * before_ref[...].astype(jnp.float32) + mixed
+    center = inputs - jnp.mean(inputs, axis=-1, keepdims=True)
+    spread = jnp.mean(center * center, axis=-1, keepdims=True)
+    rows = center * lax.rsqrt(spread + LN_EPS) * gain_ref[...] + shift_ref[...]
+    rows = rows.astype(jnp.bfloat16)
+    mid_ref[...] = rows
+
+    @pl.when(jnp.logical_not(odd))
+    def _():
+        turned_ref[...] = rows
+
+    @pl.when(odd)
+    def _():
+        turned_ref[...] = swapped(rows.astype(jnp.float32), outer, width).astype(jnp.bfloat16)
+
+
+def middle_rows(gated, blocks, resid, gain, shift):
+    parts = lax.axis_size("tp")
+    place = lax.axis_index("tp")[None].astype(jnp.int32)
+    smem, vmem = (pl.BlockSpec(memory_space=space) for space in (pltpu.SMEM, pltpu.VMEM))
+    copies = jnp.broadcast_to(gated, (parts, *gated.shape))
+    everyone = lax.all_to_all(copies, "tp", split_axis=0, concat_axis=0, tiled=True)
+    own = pl.pallas_call(
+        functools.partial(project_kernel, (0, 2, 1, 3)),
+        out_shape=jax.ShapeDtypeStruct((gated.shape[0], blocks[0].shape[1]), jnp.bfloat16),
+        in_specs=[smem] + [vmem] * (1 + len(blocks)),
+        out_specs=vmem,
+        compiler_params=pltpu.CompilerParams(vmem_limit_bytes=16 << 20),
+        name="project",
+    )(place, everyone, *blocks)
+    other = lax.ppermute(own, "tp", [(part, part ^ 1) for part in range(parts)])
+    outer = lax.axis_size(SP[0])
+    rows = jax.ShapeDtypeStruct(resid.shape, jnp.bfloat16)
+    return pl.pallas_call(
+        functools.partial(middle_kernel, outer, resid.shape[1] // (outer * lax.axis_size(SP[1]))),
+        out_shape=(rows, rows),
+        in_specs=[smem] + [vmem] * 5,
+        out_specs=(vmem, vmem),
+        compiler_params=pltpu.CompilerParams(vmem_limit_bytes=16 << 20),
+        name="middle",
+    )(place, own, other, resid, gain[None], shift[None])
+
+
 def settle_kernel(
-    scale, outer, width, back, forth, arrived_ref, before_ref, gain_ref, shift_ref, *out_refs
+    scale, outer, width, arrived_ref, before_ref, gain_ref, shift_ref, out_ref
 ):
     parts = arrived_ref.shape[0]
     even, odd = (
         sum(arrived_ref[k].astype(jnp.float32) for k in range(start, parts, 2))
         for start in range(2)
     )
-    if back:
-        odd = swapped(odd, outer, width)
+    odd = swapped(odd, outer, width)
     inputs = ALPHA * before_ref[...].astype(jnp.float32) + scale * (even + odd)
     center = inputs - jnp.mean(inputs, axis=-1, keepdims=True)
     spread = jnp.mean(center * center, axis=-1, keepdims=True)
     rows = center * lax.rsqrt(spread + LN_EPS) * gain_ref[...] + shift_ref[...]
     rows = rows.astype(jnp.bfloat16)
-    turned = rows
-    if forth:
-        turned = swapped(rows.astype(jnp.float32), outer, width).astype(jnp.bfloat16)
-        out_refs[1][...] = rows
     for k in range(parts):
-        out_refs[0][k] = turned if k % 2 else rows
-
-
-def settle(arrived, before, gain, shift, scale, back, forth):
+        out_ref[k] = rows
+
+
+def settle(arrived, before, gain, shift, scale):
     outer = lax.axis_size(SP[0])
     width = before.shape[1] // (outer * lax.axis_size(SP[1]))
-    copies = jax.ShapeDtypeStruct(arrived.shape, jnp.bfloat16)
-    kept = jax.ShapeDtypeStruct(before.shape, jnp.bfloat16)
-    vmem = pl.BlockSpec(memory_space=pltpu.VMEM)
-    out = pl.pallas_call(
-        functools.partial(settle_kernel, scale, outer, width, back, forth),
-        out_shape=(copies, kept) if forth else (copies,),
-        in_specs=[vmem] * 4,
-        out_specs=(vmem, vmem) if forth else (vmem,),
+    return pl.pallas_call(
+        functools.partial(settle_kernel, scale, outer, width),
+        out_shape=jax.ShapeDtypeStruct(arrived.shape, jnp.bfloat16),
         compiler_params=pltpu.CompilerParams(vmem_limit_bytes=8 << 20),
         name="settle",
     )(arrived, before, gain[None], shift[None])
-    return out
 
 
 def sent(array, axis):
@@ -244,14 +315,15 @@
             fetch(step, part).start()
     for step in range(steps):
         fetch(step, 0).wait()
-        rows = pl.ds(step * depth, depth)
-        product = jnp.dot(
-            mid_ref[:, rows], held[rows, pl.ds(0, wide)], preferred_element_type=jnp.float32
-        )
-        if step == 0:
-            total[...] = product
-        else:
-            total[...] += product
+        for at in range(step * depth, (step + 1) * depth, 256):
+            rows = pl.ds(at, 256)
+            product = jnp.dot(
+                mid_ref[:, rows], held[rows, pl.ds(0, wide)], preferred_element_type=jnp.float32
+            )
+            if at == 0:
+                total[...] = product
+            else:
+                total[...] += product
     hidden = (jax.nn.silu(total[:, :units]) * total[:, units:]).astype(jnp.bfloat16)
     for step in range(steps):
         fetch(step, 1).wait()
@@ -265,7 +337,7 @@
 
 
 def mix_channels(mid_rows, weights):
-    units, depth = weights.shape[1] // 3, 256
+    units, depth = weights.shape[1] // 3, 512
     steps = weights.shape[0] // depth
     return pl.pallas_call(
         functools.partial(mixer_kernel, units, depth),
@@ -288,7 +360,7 @@
     )(mid_rows, weights)
 
 
-def body(
+def whole(
     resid,
     queries,
     keys,
@@ -307,15 +379,12 @@
 ):
     own_count = queries.shape[0] // lax.axis_size("tp")
     nearby = nearby_weights(gate_in, up_in, down_out)
+    blocks = collected_projection(out_proj)
     gated, weights = mix_tokens(queries, keys, values, decay_pre, out_gate, head_gain, nearby)
-    mixed = jnp.dot(gated, out_proj, preferred_element_type=jnp.float32).astype(jnp.bfloat16)
-    own_resid = lax.dynamic_slice_in_dim(resid, lax.axis_index("tp") * own_count, own_count, 0)
-    copies, mid = settle(
-        sent(mixed, "tp"), own_resid, mix_gain, mix_shift, 1.0, back=False, forth=True
-    )
-    mid_rows = sent(copies, "tp").reshape(resid.shape)
-    ffn = sent(mix_channels(mid_rows, weights), "tp")
-    (finished,) = settle(ffn, mid, out_gain, out_shift, 0.5, back=True, forth=False)
+    mid, mid_turned = middle_rows(gated, blocks, resid, mix_gain, mix_shift)
+    ffn = sent(mix_channels(mid_turned, weights), "tp")
+    own_mid = lax.dynamic_slice_in_dim(mid, lax.axis_index("tp") * own_count, own_count, 0)
+    finished = settle(ffn, own_mid, out_gain, out_shift, 0.5)
     return sent(finished, "tp").reshape(resid.shape)
 
 
@@ -338,4 +407,4 @@
         P(),
         P(),
     )
-    return jax.shard_map(body, mesh=finer, in_specs=placed, out_specs=P(SP, None), check_vma=False)
+    return jax.shard_map(whole, mesh=finer, in_specs=placed, out_specs=P(SP, None), check_vma=False)

time: 152 us -> 175 us (1.15)
  blocking collectives: 74.1 us -> 12.7 us
  waiting for transfers between devices: 25.3 us -> 73.4 us
  starting transfers between devices: 19.9 us -> 53.6 us
    all_to_all x2 -> x0, blocking collectives: 34.2 us -> none  [the longest x1 19 us: mix_tokens(): lax.all_to_all(packed, SP, split_axis=0, concat_axis=0, tiled=True)]
    ppermute x0 -> x5, waiting for transfers between devices: none -> 32.6 us  [the longest x3 31.5 us: collected_projection(): blocks.append(lax.ppermute(block, 'tp', path))]
    all_to_all x3 -> x1, blocking collectives: 39.9 us -> 12.7 us  [sent(): return lax.all_to_all(blocks, axis, split_axis=0, concat_axis=0, tiled=True)]
    all_to_all x0 -> x3, starting transfers between devices: none -> 21.5 us  [the longest x1 9.33 us: mix_tokens(): lax.all_to_all(packed, SP, split_axis=0, concat_axis=0, tiled=True)]
    ppermute x0 -> x5, starting transfers between devices: none -> 16.8 us  [the longest x3 11.2 us: collected_projection(): blocks.append(lax.ppermute(block, 'tp', path))]
    all_to_all x0 -> x3, waiting for transfers between devices: none -> 15.3 us  [the longest x1 11.2 us: mix_tokens(): lax.all_to_all(packed, SP, split_axis=0, concat_axis=0, tiled=True)]
    all_to_all x1, starting transfers between devices: 8.86 us -> 4.45 us  [sent(): return lax.all_to_all(blocks, axis, split_axis=0, concat_axis=0, tiled=True)]
    pallas_call x2 -> x3, Pallas kernels: 0.79 us -> 3.72 us  [the longest x1 2.31 us: middle_rows(): pl.pallas_call(functools.partial(project_kernel, (0, 2, 1, 3)), out_shape...]
  transfers between devices with their start and end apart: 3 -> 11, of which waited for: 2 -> 8; matrix products, arithmetic and copies ran while one was open for 3% -> 3% of each run, Pallas kernels for 1% -> 3%
where the time goes in v3:
time: 175 us; the launch traced here: 174 us
  waiting for transfers between devices  73.4 us (42%)
  starting transfers between devices  53.6 us (31%)
  between operations  13.8 us (8%)
  blocking collectives  12.7 us (7%)
  Pallas kernels  11.6 us (7%)
  local copies, waits for them, and re-layouts  6.55 us (4%)
    ppermute x3, waiting for transfers between devices, collected_projection(): blocks.append(lax.ppermute(block, 'tp', path))  31.5 us
    all_to_all x1, waiting for transfers between devices, nearby_weights(): lax.all_to_all(copies, (*SP, 'tp'), split_axis=0, concat_axis=0, tiled=Tr...  16.1 us
    all_to_all x1, blocking collectives, sent(): return lax.all_to_all(blocks, axis, split_axis=0, concat_axis=0, tiled=True)  12.7 us
    all_to_all x1, waiting for transfers between devices, mix_tokens(): lax.all_to_all(packed, SP, split_axis=0, concat_axis=0, tiled=True)  11.2 us
    ppermute x3, starting transfers between devices, collected_projection(): blocks.append(lax.ppermute(block, 'tp', path))  11.2 us
    all_to_all x1, starting transfers between devices, nearby_weights(): lax.all_to_all(copies, (*SP, 'tp'), split_axis=0, concat_axis=0, tiled=Tr...  10.9 us
    all_to_all x1, waiting for transfers between devices, sent(): return lax.all_to_all(blocks, axis, split_axis=0, concat_axis=0, tiled=True)  9.34 us
    all_to_all x1, starting transfers between devices, mix_tokens(): lax.all_to_all(packed, SP, split_axis=0, concat_axis=0, tiled=True)  9.33 us
  transfers between devices with their start and end apart: 11, of which 8 were waited for; matrix products, arithmetic and copies ran while one was open for 3% of the time, Pallas kernels for 3%

profile of v3, /device:TPU:1, one launch (start us, length us, event | category | flops | bytes accessed | tf_op | source)
XLA Modules:
  0.0 174.4 jit_solution(105704702737899292)
XLA Ops:
  6.5 1.0 concatenate.15
  7.5 1.1 broadcast_in_dim.60
  8.6 10.9 %all-to-all-start = ((bf16[8,32,2112]{2,1,0:T(8,128)(2,1)}), bf16[8,32,2112]{2,1,0:T(8,128)(2,1)S(1)}, u32[]{:S(2)}, u32[]{:S(2)}) async-start(bf16[8,32,2112]{2,1,0:T(8,128)(2,1)} %broadcast_in_dim.60), calls=%async_computation | async-start | bytes 2228224 | tf_op jit(solution)/shard_map/all_to_all | solution.py:96
  20.1 0.8 while.13
  21.4 0.7 pad_maximum_fusion.1
  22.1 16.1 %all-to-all-done = bf16[8,32,2112]{2,1,0:T(8,128)(2,1)S(1)} async-done(((bf16[8,32,2112]{2,1,0:T(8,128)(2,1)}), bf16[8,32,2112]{2,1,0:T(8,128)(2,1)S(1)}, u32[]{:S(2)}, u32[]{:S(2)}) %all-to-all-start) | async-done | bytes 1081376 | tf_op jit(solution)/shard_map/all_to_all | solution.py:96
  38.2 1.0 copy-done.7
  39.3 2.3 %collective-permute-start = (bf16[256,1024]{1,0:T(8,128)(2,1)S(1)}, bf16[256,1024]{1,0:T(8,128)(2,1)S(1)}, u32[]{:S(2)}, u32[]{:S(2)}) collective-permute-start(bf16[256,1024]{1,0:T(8,128)(2,1)S(1)} %broadcast_select_fusion.2), channel_id=1, source_target_pairs={{0,1},{1,0},{2,3},{3,2},{4,5},{5,4},{6,7},{7,6},{8,9},{9,8},{10,11... | collective-permute-start | bytes 1572872 | tf_op jit(solution)/shard_map/ppermute | solution.py:139
  41.6 9.3 %all-to-all-start.1 = ((bf16[64,2,384]{2,1,0:T(2,128)(2,1)}), bf16[64,2,384]{2,1,0:T(2,128)(2,1)S(1)}, u32[]{:S(2)}, u32[]{:S(2)}) async-start(bf16[64,2,384]{2,1,0:T(2,128)(2,1)} %pad_maximum_fusion.1), calls=%async_computation.1 | async-start | bytes 196608 | tf_op jit(solution)/shard_map/all_to_all | solution.py:282
  51.1 11.2 %all-to-all-done.1 = bf16[64,2,384]{2,1,0:T(2,128)(2,1)S(1)} async-done(((bf16[64,2,384]{2,1,0:T(2,128)(2,1)}), bf16[64,2,384]{2,1,0:T(2,128)(2,1)S(1)}, u32[]{:S(2)}, u32[]{:S(2)}) %all-to-all-start.1) | async-done | bytes 98336 | tf_op jit(solution)/shard_map/all_to_all | solution.py:282
  62.4 1.2 prefix.1
  63.5 0.7 reshape.190
  64.2 4.6 %all-to-all-start.2 = ((bf16[64,2,256]{2,1,0:T(2,128)(2,1)}), bf16[64,2,256]{2,1,0:T(2,128)(2,1)S(1)}, u32[]{:S(2)}, u32[]{:S(2)}) async-start(bf16[64,2,256]{2,1,0:T(2,128)(2,1)} %reshape.190), calls=%async_computation.2 | async-start | bytes 131072 | tf_op jit(solution)/shard_map/all_to_all | solution.py:73
  68.9 4.7 %collective-permute-start.1 = (bf16[512,1024]{1,0:T(8,128)(2,1)S(1)}, bf16[512,1024]{1,0:T(8,128)(2,1)S(1)}, u32[]{:S(2)}, u32[]{:S(2)}) collective-permute-start(bf16[512,1024]{1,0:T(8,128)(2,1)S(1)} %pad_maximum_fusion.refs_0_), channel_id=1, source_target_pairs={{0,4},{1,5},{2,6},{3,7},{4,0},{5,1},{6,2},{7,3},{8,12},{9,13},{10,... | collective-permute-start | bytes 3145736 | tf_op jit(solution)/shard_map/ppermute | solution.py:145
  73.6 2.4 %collective-permute-start.2 = (bf16[512,1024]{1,0:T(8,128)(2,1)S(1)}, bf16[512,1024]{1,0:T(8,128)(2,1)}, u32[]{:S(2)}, u32[]{:S(2)}) collective-permute-start(bf16[512,1024]{1,0:T(8,128)(2,1)S(1)} %pad_maximum_fusion.refs_0_), channel_id=1, source_target_pairs={{0,2},{1,3},{2,4},{3,5},{4,6},{5,7},{6,0},{7,1},{8,10},{9,11},{10,... | collective-permute-start | bytes 3145736 | tf_op jit(solution)/shard_map/ppermute | solution.py:145
  76.0 4.1 %collective-permute-start.3 = (bf16[512,1024]{1,0:T(8,128)(2,1)S(1)}, bf16[512,1024]{1,0:T(8,128)(2,1)}, u32[]{:S(2)}, u32[]{:S(2)}) collective-permute-start(bf16[512,1024]{1,0:T(8,128)(2,1)S(1)} %pad_maximum_fusion.refs_0_), channel_id=1, source_target_pairs={{0,6},{1,7},{2,0},{3,1},{4,2},{5,3},{6,4},{7,5},{8,14},{9,15},{10,... | collective-permute-start | bytes 3145736 | tf_op jit(solution)/shard_map/ppermute | solution.py:145
  80.8 0.8 broadcast_in_dim.61
  81.6 7.5 %all-to-all-start.3 = ((bf16[8,128,256]{2,1,0:T(8,128)(2,1)}), bf16[8,128,256]{2,1,0:T(8,128)(2,1)S(1)}, u32[]{:S(2)}, u32[]{:S(2)}) async-start(bf16[8,128,256]{2,1,0:T(8,128)(2,1)} %broadcast_in_dim.61), calls=%async_computation.3 | async-start | bytes 1048576 | tf_op jit(solution)/shard_map/all_to_all | solution.py:193
  89.1 5.8 %collective-permute-done.1.refs_1_ = bf16[512,1024]{1,0:T(8,128)(2,1)S(1)} collective-permute-done((bf16[512,1024]{1,0:T(8,128)(2,1)S(1)}, bf16[512,1024]{1,0:T(8,128)(2,1)S(1)}, u32[]{:S(2)}, u32[]{:S(2)}) %collective-permute-start.1) | collective-permute-done | bytes 1048608 | tf_op jit(solution)/shard_map/ppermute | solution.py:145
  94.9 25.7 %collective-permute-done.2.refs_2_ = bf16[512,1024]{1,0:T(8,128)(2,1)} collective-permute-done((bf16[512,1024]{1,0:T(8,128)(2,1)S(1)}, bf16[512,1024]{1,0:T(8,128)(2,1)}, u32[]{:S(2)}, u32[]{:S(2)}) %collective-permute-start.2) | collective-permute-done | bytes 1048608 | tf_op jit(solution)/shard_map/ppermute | solution.py:145
  120.6 4.0 %all-to-all-done.3.gated_ref = bf16[8,128,256]{2,1,0:T(8,128)(2,1)S(1)} async-done(((bf16[8,128,256]{2,1,0:T(8,128)(2,1)}), bf16[8,128,256]{2,1,0:T(8,128)(2,1)S(1)}, u32[]{:S(2)}, u32[]{:S(2)}) %all-to-all-start.3) | async-done | bytes 524320 | tf_op jit(solution)/shard_map/all_to_all | solution.py:193
  124.6 2.3 %project.1.own_ref = bf16[128,1024]{1,0:T(8,128)(2,1)S(1)} custom-call(s32[1]{0:T(128)} %bitcast.place_ref, bf16[8,128,256]{2,1,0:T(8,128)(2,1)S(1)} %all-to-all-done.3.gated_ref, bf16[512,1024]{1,0:T(8,128)(2,1)S(1)} %pad_maximum_fusion.refs_0_, bf16[512,1024]{1,0:T(8,128)(2,1)S(1)} %collective-permute-done.1.refs_1_, ...), custom_call_target="tpu_custom_call" | custom-call | tf_op jit(solution)/shard_map/project/pallas_call | solution.py:194
  126.9 3.3 %collective-permute-start.4 = (bf16[128,1024]{1,0:T(8,128)(2,1)S(1)}, bf16[128,1024]{1,0:T(8,128)(2,1)S(1)}, u32[]{:S(2)}, u32[]{:S(2)}) collective-permute-start(bf16[128,1024]{1,0:T(8,128)(2,1)S(1)} %project.1.own_ref), channel_id=1, source_target_pairs={{0,1},{1,0},{2,3},{3,2},{4,5},{5,4},{6,7},{7,6},{8,9},{9,8},{10,11... | collective-permute-start | bytes 786440 | tf_op jit(solution)/shard_map/ppermute | solution.py:202
  130.2 1.1 collective-permute-done.4.other_ref
  131.4 1.0 middle.1
  132.4 0.8 copy-done.1
  133.2 6.7 %mix_channels.1 = bf16[128,2048]{1,0:T(8,128)(2,1)} custom-call(bf16[128,2048]{1,0:T(8,128)(2,1)} %copy-done.1, bf16[2048,2112]{1,0:T(8,128)(2,1)} %all-gather.2.cloned.1.call-done.weights_ref), custom_call_target="tpu_custom_call" | custom-call | flops 1107296256 | bytes 8650752 | tf_op jit(solution)/shard_map/mix_channels/pallas_call | solution.py:342
  139.9 4.5 %all-to-all-start.4 = ((bf16[8,16,2048]{2,1,0:T(8,128)(2,1)}), bf16[8,16,2048]{2,1,0:T(8,128)(2,1)S(1)}, u32[]{:S(2)}, u32[]{:S(2)}) async-start(bf16[8,16,2048]{2,1,0:T(8,128)(2,1)} %bitcast.90), calls=%async_computation.4 | async-start | bytes 1048576 | tf_op jit(solution)/shard_map/all_to_all | solution.py:247
  144.3 9.3 %all-to-all-done.4.arrived_ref = bf16[8,16,2048]{2,1,0:T(8,128)(2,1)S(1)} async-done(((bf16[8,16,2048]{2,1,0:T(8,128)(2,1)}), bf16[8,16,2048]{2,1,0:T(8,128)(2,1)S(1)}, u32[]{:S(2)}, u32[]{:S(2)}) %all-to-all-start.4) | async-done | bytes 524320 | tf_op jit(solution)/shard_map/all_to_all | solution.py:247
  153.7 0.4 settle.1
  154.1 12.7 %all_to_all.30 = bf16[8,16,2048]{2,1,0:T(8,128)(2,1)S(1)} all-to-all(bf16[8,16,2048]{2,1,0:T(8,128)(2,1)S(1)} %settle.1), channel_id=1, replica_groups=mesh['sp_0'=8,'sp_1'=8,'tp'=8] {'tp'}, dimensions={0} | all-to-all | bytes 1048576 | tf_op jit(solution)/shard_map/all_to_all | solution.py:247
  166.8 0.8 copy.36
  (70 shorter events, 2.6 us)
Async XLA Ops:
  6.5 13.2 %copy-start = (bf16[128,256]{1,0:T(8,128)(2,1)S(1)}, bf16[128,256]{1,0:T(8,128)(2,1)}, u32[]{:S(2)}) copy-start(bf16[128,256]{1,0:T(8,128)(2,1)} %param.20) | copy-start | bytes 196612
  6.5 13.0 %copy-start.11 = (f32[128,128]{1,0:T(8,128)S(1)}, f32[128,128]{1,0:T(8,128)}, u32[]{:S(2)}) copy-start(f32[128,128]{1,0:T(8,128)} %param.21) | copy-start | bytes 196612
  6.5 13.2 %copy-start.13 = (bf16[128,128]{1,0:T(8,128)(2,1)S(1)}, bf16[128,128]{1,0:T(8,128)(2,1)}, u32[]{:S(2)}) copy-start(bf16[128,128]{1,0:T(8,128)(2,1)} %param.18) | copy-start | bytes 98308
  6.5 13.2 %copy-start.14 = (bf16[128,128]{1,0:T(8,128)(2,1)S(1)}, bf16[128,128]{1,0:T(8,128)(2,1)}, u32[]{:S(2)}) copy-start(bf16[128,128]{1,0:T(8,128)(2,1)} %param.19) | copy-start | bytes 98308
  8.6 29.6 %all-to-all-start = ((bf16[8,32,2112]{2,1,0:T(8,128)(2,1)}), bf16[8,32,2112]{2,1,0:T(8,128)(2,1)S(1)}, u32[]{:S(2)}, u32[]{:S(2)}) async-start(bf16[8,32,2112]{2,1,0:T(8,128)(2,1)} %broadcast_in_dim.60), calls=%async_computation | async-start | bytes 2228224 | tf_op jit(solution)/shard_map/all_to_all | solution.py:96
  19.5 113.7 %all-gather.2.cloned.1.call-start = ((), (), s32[]{:S(2)}) async-start(), calls=%async_computation.6 | async-start | bytes 10027008 | tf_op jit(solution)/shard_map/all_gather | solution.py:108
  20.1 19.1 %copy-start.8 = (bf16[256,2048]{1,0:T(8,128)(2,1)S(1)}, bf16[256,2048]{1,0:T(8,128)(2,1)}, u32[]{:S(2)}) copy-start(bf16[256,2048]{1,0:T(8,128)(2,1)} %param.24) | copy-start | bytes 3145732
  20.9 30.1 %copy-start.9 = (f32[2,64,1,256]{3,1,2,0:T(8,128)}, f32[2,64,1,256]{3,1,2,0:T(8,128)S(1)}, u32[]{:S(2)}) copy-start(f32[2,64,1,256]{3,1,2,0:T(8,128)S(1)} %get-tuple-element.42) | copy-start | bytes 393220
  38.2 1.0 copy-start.7
  39.3 11.7 %collective-permute-start = (bf16[256,1024]{1,0:T(8,128)(2,1)S(1)}, bf16[256,1024]{1,0:T(8,128)(2,1)S(1)}, u32[]{:S(2)}, u32[]{:S(2)}) collective-permute-start(bf16[256,1024]{1,0:T(8,128)(2,1)S(1)} %broadcast_select_fusion.2), channel_id=1, source_target_pairs={{0,1},{1,0},{2,3},{3,2},{4,5},{5,4},{6,7},{7,6},{8,9},{9,8},{10,11... | collective-permute-start | bytes 1572872 | tf_op jit(solution)/shard_map/ppermute | solution.py:139
  41.6 20.7 %all-to-all-start.1 = ((bf16[64,2,384]{2,1,0:T(2,128)(2,1)}), bf16[64,2,384]{2,1,0:T(2,128)(2,1)S(1)}, u32[]{:S(2)}, u32[]{:S(2)}) async-start(bf16[64,2,384]{2,1,0:T(2,128)(2,1)} %pad_maximum_fusion.1), calls=%async_computation.1 | async-start | bytes 196608 | tf_op jit(solution)/shard_map/all_to_all | solution.py:282
  51.1 29.6 %copy-start.12 = (bf16[128,256]{1,0:T(8,128)(2,1)S(1)}, bf16[128,256]{1,0:T(8,128)(2,1)}, u32[]{:S(2)}) copy-start(bf16[128,256]{1,0:T(8,128)(2,1)} %param.22) | copy-start | bytes 196612
  51.1 29.6 %copy-start.15 = (f32[256]{0:T(256)S(1)}, f32[256]{0:T(256)}, u32[]{:S(2)}) copy-start(f32[256]{0:T(256)} %param.23) | copy-start | bytes 3076
  62.4 17.9 %copy-start.10 = (f32[2,64,1,256]{3,1,2,0:T(8,128)S(1)}, f32[2,64,1,256]{3,1,2,0:T(8,128)}, u32[]{:S(2)}) copy-start(f32[2,64,1,256]{3,1,2,0:T(8,128)} %copy-done.9) | copy-start | bytes 393220
  64.2 16.0 %all-to-all-start.2 = ((bf16[64,2,256]{2,1,0:T(2,128)(2,1)}), bf16[64,2,256]{2,1,0:T(2,128)(2,1)S(1)}, u32[]{:S(2)}, u32[]{:S(2)}) async-start(bf16[64,2,256]{2,1,0:T(2,128)(2,1)} %reshape.190), calls=%async_computation.2 | async-start | bytes 131072 | tf_op jit(solution)/shard_map/all_to_all | solution.py:73
  68.9 26.1 %collective-permute-start.1 = (bf16[512,1024]{1,0:T(8,128)(2,1)S(1)}, bf16[512,1024]{1,0:T(8,128)(2,1)S(1)}, u32[]{:S(2)}, u32[]{:S(2)}) collective-permute-start(bf16[512,1024]{1,0:T(8,128)(2,1)S(1)} %pad_maximum_fusion.refs_0_), channel_id=1, source_target_pairs={{0,4},{1,5},{2,6},{3,7},{4,0},{5,1},{6,2},{7,3},{8,12},{9,13},{10,... | collective-permute-start | bytes 3145736 | tf_op jit(solution)/shard_map/ppermute | solution.py:145
  73.6 47.1 %collective-permute-start.2 = (bf16[512,1024]{1,0:T(8,128)(2,1)S(1)}, bf16[512,1024]{1,0:T(8,128)(2,1)}, u32[]{:S(2)}, u32[]{:S(2)}) collective-permute-start(bf16[512,1024]{1,0:T(8,128)(2,1)S(1)} %pad_maximum_fusion.refs_0_), channel_id=1, source_target_pairs={{0,2},{1,3},{2,4},{3,5},{4,6},{5,7},{6,0},{7,1},{8,10},{9,11},{10,... | collective-permute-start | bytes 3145736 | tf_op jit(solution)/shard_map/ppermute | solution.py:145
  76.0 44.6 %collective-permute-start.3 = (bf16[512,1024]{1,0:T(8,128)(2,1)S(1)}, bf16[512,1024]{1,0:T(8,128)(2,1)}, u32[]{:S(2)}, u32[]{:S(2)}) collective-permute-start(bf16[512,1024]{1,0:T(8,128)(2,1)S(1)} %pad_maximum_fusion.refs_0_), channel_id=1, source_target_pairs={{0,6},{1,7},{2,0},{3,1},{4,2},{5,3},{6,4},{7,5},{8,14},{9,15},{10,... | collective-permute-start | bytes 3145736 | tf_op jit(solution)/shard_map/ppermute | solution.py:145
  81.6 43.0 %all-to-all-start.3 = ((bf16[8,128,256]{2,1,0:T(8,128)(2,1)}), bf16[8,128,256]{2,1,0:T(8,128)(2,1)S(1)}, u32[]{:S(2)}, u32[]{:S(2)}) async-start(bf16[8,128,256]{2,1,0:T(8,128)(2,1)} %broadcast_in_dim.61), calls=%async_computation.3 | async-start | bytes 1048576 | tf_op jit(solution)/shard_map/all_to_all | solution.py:193
  124.6 6.8 %copy-start.2 = (bf16[128,2048]{1,0:T(8,128)(2,1)S(1)}, bf16[128,2048]{1,0:T(8,128)(2,1)}, u32[]{:S(2)}) copy-start(bf16[128,2048]{1,0:T(8,128)(2,1)} %before_ref.1) | copy-start | bytes 1572868
  124.6 6.8 %copy-start.3 = (f32[2048]{0:T(1024)S(1)}, f32[2048]{0:T(1024)}, u32[]{:S(2)}) copy-start(f32[2048]{0:T(1024)} %param.25) | copy-start | bytes 24580
  124.6 6.8 %copy-start.4 = (f32[2048]{0:T(1024)S(1)}, f32[2048]{0:T(1024)}, u32[]{:S(2)}) copy-start(f32[2048]{0:T(1024)} %param.26) | copy-start | bytes 24580
  126.9 4.4 %collective-permute-start.4 = (bf16[128,1024]{1,0:T(8,128)(2,1)S(1)}, bf16[128,1024]{1,0:T(8,128)(2,1)S(1)}, u32[]{:S(2)}, u32[]{:S(2)}) collective-permute-start(bf16[128,1024]{1,0:T(8,128)(2,1)S(1)} %project.1.own_ref), channel_id=1, source_target_pairs={{0,1},{1,0},{2,3},{3,2},{4,5},{5,4},{6,7},{7,6},{8,9},{9,8},{10,11... | collective-permute-start | bytes 786440 | tf_op jit(solution)/shard_map/ppermute | solution.py:202
  132.4 0.8 copy-start.1
  133.2 20.5 %copy-start.5 = (f32[2048]{0:T(1024)S(1)}, f32[2048]{0:T(1024)}, u32[]{:S(2)}) copy-start(f32[2048]{0:T(1024)} %param.30) | copy-start | bytes 24580
  133.2 20.5 %copy-start.6 = (f32[2048]{0:T(1024)S(1)}, f32[2048]{0:T(1024)}, u32[]{:S(2)}) copy-start(f32[2048]{0:T(1024)} %param.31) | copy-start | bytes 24580
  139.9 13.8 %all-to-all-start.4 = ((bf16[8,16,2048]{2,1,0:T(8,128)(2,1)}), bf16[8,16,2048]{2,1,0:T(8,128)(2,1)S(1)}, u32[]{:S(2)}, u32[]{:S(2)}) async-start(bf16[8,16,2048]{2,1,0:T(8,128)(2,1)} %bitcast.90), calls=%async_computation.4 | async-start | bytes 1048576 | tf_op jit(solution)/shard_map/all_to_all | solution.py:247
Sparse Core Ops, SparseCore 0:
  39.3 60.5 all-gather.1

commit v4 on v3

--- a/solution.py
+++ b/solution.py
@@ -71,7 +71,7 @@
     )(arrived.reshape(count, -1))
     entering = entering.reshape(count, channels, HV)
     back = lax.all_to_all(entering, SP, split_axis=0, concat_axis=0, tiled=True)
-    return back.reshape(shape).astype(jnp.float32)
+    return back.reshape(shape)
 
 
 def ring_groups(first):
@@ -90,9 +90,19 @@
     ]
 
 
+def copies_kernel(gate_ref, up_ref, down_ref, out_ref):
+    own = jnp.concatenate([gate_ref[...], up_ref[...], down_ref[...]], axis=1)
+    for k in range(out_ref.shape[0]):
+        out_ref[k] = own
+
+
 def nearby_weights(gate_in, up_in, down_out):
-    own = jnp.concatenate([gate_in, up_in, down_out.T], axis=1)
-    copies = jnp.broadcast_to(own, (lax.axis_size(SP[0]), *own.shape))
+    rows, units = gate_in.shape
+    copies = pl.pallas_call(
+        copies_kernel,
+        out_shape=jax.ShapeDtypeStruct((lax.axis_size(SP[0]), rows, 3 * units), jnp.bfloat16),
+        name="copies",
+    )(gate_in, up_in, down_out.T)
     arrived = lax.all_to_all(
         copies,
         (*SP, "tp"),
@@ -101,7 +111,7 @@
         tiled=True,
         axis_index_groups=ring_groups(True),
     )
-    return arrived.reshape(-1, own.shape[1])
+    return arrived.reshape(-1, 3 * units)
 
 
 def gathered_weights(nearby):
@@ -150,17 +160,18 @@
     out_ref = refs[-1]
     chip, depth = place_ref[0] // 2, gated_ref.shape[2]
     count = gated_ref.shape[0] // 2
-    total = None
-    for step, block_ref in zip(steps, refs[:-1]):
-        source = lax.rem(chip + (count - step), count)
-        for core in range(2):
-            product = jnp.dot(
-                gated_ref[2 * source + core],
-                block_ref[core * depth : (core + 1) * depth],
-                preferred_element_type=jnp.float32,
-            )
-            total = product if total is None else total + product
-    out_ref[...] = total.astype(jnp.bfloat16)
+    for at in range(0, out_ref.shape[1], 256):
+        total = None
+        for step, block_ref in zip(steps, refs[:-1]):
+            source = lax.rem(chip + (count - step), count)
+            for core in range(2):
+                product = jnp.dot(
+                    gated_ref[2 * source + core],
+                    block_ref[core * depth : (core + 1) * depth, at : at + 256],
+                    preferred_element_type=jnp.float32,
+                )
+                total = product if total is None else total + product
+        out_ref[:, at : at + 256] = total.astype(jnp.bfloat16)
 
 
 def middle_kernel(
@@ -185,15 +196,14 @@
         turned_ref[...] = swapped(rows.astype(jnp.float32), outer, width).astype(jnp.bfloat16)
 
 
-def middle_rows(gated, blocks, resid, gain, shift):
+def middle_rows(copies, blocks, resid, gain, shift):
     parts = lax.axis_size("tp")
     place = lax.axis_index("tp")[None].astype(jnp.int32)
     smem, vmem = (pl.BlockSpec(memory_space=space) for space in (pltpu.SMEM, pltpu.VMEM))
-    copies = jnp.broadcast_to(gated, (parts, *gated.shape))
     everyone = lax.all_to_all(copies, "tp", split_axis=0, concat_axis=0, tiled=True)
     own = pl.pallas_call(
         functools.partial(project_kernel, (0, 2, 1, 3)),
-        out_shape=jax.ShapeDtypeStruct((gated.shape[0], blocks[0].shape[1]), jnp.bfloat16),
+        out_shape=jax.ShapeDtypeStruct((resid.shape[0], blocks[0].shape[1]), jnp.bfloat16),
         in_specs=[smem] + [vmem] * (1 + len(blocks)),
         out_specs=vmem,
         compiler_params=pltpu.CompilerParams(vmem_limit_bytes=16 << 20),
@@ -247,6 +257,20 @@
     return lax.all_to_all(blocks, axis, split_axis=0, concat_axis=0, tiled=True)
 
 
+def gate_kernel(readers_ref, state_ref, local_ref, gate_ref, gain_ref, out_ref):
+    readout = local_ref[...] + jnp.dot(
+        readers_ref[...],
+        state_ref[...].astype(jnp.float32),
+        precision=lax.Precision.HIGHEST,
+        preferred_element_type=jnp.float32,
+    )
+    square = jnp.mean(readout * readout, axis=-1, keepdims=True)
+    normed = readout * lax.rsqrt(square + RMS_EPS) * gain_ref[...]
+    gated = (normed * jax.nn.silu(gate_ref[...].astype(jnp.float32))).astype(jnp.bfloat16)
+    for k in range(out_ref.shape[0]):
+        out_ref[k] = gated
+
+
 def mix_tokens(queries, keys, values, decay_pre, out_gate, head_gain, nearby):
     tok_rows = queries.shape[0]
     local_heads = queries.shape[1] // HK
@@ -280,26 +304,18 @@
     packed, nearby = lax.optimization_barrier((packed, nearby))
     weights = gathered_weights(nearby)
     arrived = lax.all_to_all(packed, SP, split_axis=0, concat_axis=0, tiled=True)
-    incoming = incoming_state(arrived, own_state.shape)
-    carried = jnp.einsum(
-        "xepj,pjw->xepw",
-        scaled_q * jnp.exp(block_ends)[:, None],
-        incoming,
-        precision=lax.Precision.HIGHEST,
-    )
-    state_readout = (local_read + carried).reshape(tok_rows, local_heads, HV)
-    normed = (
-        state_readout
-        * lax.rsqrt(jnp.mean(state_readout * state_readout, axis=-1, keepdims=True) + RMS_EPS)
-        * head_gain
-    )
-    gated = (
-        normed.reshape(tok_rows, local_heads * HV) * jax.nn.silu(out_gate.astype(jnp.float32))
-    ).astype(jnp.bfloat16)
-    return gated, weights
-
-
-def mixer_kernel(units, depth, mid_ref, weights_ref, out_ref, held, total, sems):
+    incoming = incoming_state(arrived, own_state.shape[1:])
+    readers = (scaled_q * jnp.exp(block_ends)[:, None]).reshape(tok_rows, HK)
+    copies = pl.pallas_call(
+        gate_kernel,
+        out_shape=jax.ShapeDtypeStruct((lax.axis_size("tp"), *values.shape), jnp.bfloat16),
+        compiler_params=pltpu.CompilerParams(vmem_limit_bytes=8 << 20),
+        name="gate",
+    )(readers, incoming, local_read.reshape(tok_rows, HV), out_gate, head_gain[None])
+    return copies, weights
+
+
+def mixer_kernel(units, depth, mid_ref, weights_ref, out_ref, held, total, made, sems, out_sems):
     steps = mid_ref.shape[1] // depth
     wide = 2 * units
 
@@ -308,6 +324,12 @@
         columns = pl.ds(0, wide) if part == 0 else pl.ds(wide, units)
         return pltpu.make_async_copy(
             weights_ref.at[rows, columns], held.at[rows, columns], sems.at[part, step]
+        )
+
+    def give(step):
+        columns = pl.ds(step * depth, depth)
+        return pltpu.make_async_copy(
+            made.at[:, columns], out_ref.at[:, columns], out_sems.at[step]
         )
 
     for part in range(2):
@@ -328,12 +350,15 @@
     for step in range(steps):
         fetch(step, 1).wait()
         rows = pl.ds(step * depth, depth)
-        out_ref[:, rows] = lax.dot_general(
+        made[:, rows] = lax.dot_general(
             hidden,
             held[rows, pl.ds(wide, units)],
             (((1,), (1,)), ((), ())),
             preferred_element_type=jnp.float32,
         ).astype(jnp.bfloat16)
+        give(step).start()
+    for step in range(steps):
+        give(step).wait()
 
 
 def mix_channels(mid_rows, weights):
@@ -346,13 +371,15 @@
             pl.BlockSpec(memory_space=pltpu.VMEM),
             pl.BlockSpec(memory_space=pltpu.HBM),
         ],
-        out_specs=pl.BlockSpec(memory_space=pltpu.VMEM),
+        out_specs=pl.BlockSpec(memory_space=pltpu.HBM),
         scratch_shapes=[
             pltpu.VMEM(weights.shape, jnp.bfloat16),
             pltpu.VMEM((mid_rows.shape[0], 2 * units), jnp.float32),
+            pltpu.VMEM(mid_rows.shape, jnp.bfloat16),
             pltpu.SemaphoreType.DMA((2, steps)),
+            pltpu.SemaphoreType.DMA((steps,)),
         ],
-        compiler_params=pltpu.CompilerParams(vmem_limit_bytes=56 << 20),
+        compiler_params=pltpu.CompilerParams(vmem_limit_bytes=52 << 20),
         cost_estimate=pl.CostEstimate(
             flops=6 * mid_rows.size * units, bytes_accessed=2 * weights.size, transcendentals=0
         ),
@@ -380,8 +407,8 @@
     own_count = queries.shape[0] // lax.axis_size("tp")
     nearby = nearby_weights(gate_in, up_in, down_out)
     blocks = collected_projection(out_proj)
-    gated, weights = mix_tokens(queries, keys, values, decay_pre, out_gate, head_gain, nearby)
-    mid, mid_turned = middle_rows(gated, blocks, resid, mix_gain, mix_shift)
+    gated_copies, weights = mix_tokens(queries, keys, values, decay_pre, out_gate, head_gain, nearby)
+    mid, mid_turned = middle_rows(gated_copies, blocks, resid, mix_gain, mix_shift)
     ffn = sent(mix_channels(mid_turned, weights), "tp")
     own_mid = lax.dynamic_slice_in_dim(mid, lax.axis_index("tp") * own_count, own_count, 0)
     finished = settle(ffn, own_mid, out_gain, out_shift, 0.5)

time: 175 us -> 157 us (0.90)
  blocking collectives: 12.7 us -> 49.1 us
  waiting for transfers between devices: 73.4 us -> 38 us
  starting transfers between devices: 53.6 us -> 37.7 us
  local copies, waits for them, and re-layouts: 6.55 us -> 2.15 us
  Pallas kernels: 11.6 us -> 13.5 us
    all_to_all x0 -> x2, blocking collectives: none -> 36.4 us  [the longest x1 21.1 us: mix_tokens(): lax.all_to_all(packed, SP, split_axis=0, concat_axis=0, tiled=True)]
    ppermute x3, waiting for transfers between devices: 31.5 us -> 0.01 us  [collected_projection(): blocks.append(lax.ppermute(block, 'tp', path))]
    all_to_all x2 -> x0, starting transfers between devices: 13.9 us -> none  [the longest x1 9.33 us: mix_tokens(): lax.all_to_all(packed, SP, split_axis=0, concat_axis=0, tiled=True)]
    all_to_all x2 -> x0, waiting for transfers between devices: 11.4 us -> none  [the longest x1 11.2 us: mix_tokens(): lax.all_to_all(packed, SP, split_axis=0, concat_axis=0, tiled=True)]
    all_to_all x1, waiting for transfers between devices: 3.95 us -> 9.36 us  [middle_rows(): lax.all_to_all(copies, 'tp', split_axis=0, concat_axis=0, tiled=True)]
    pallas_call x0 -> x2, Pallas kernels: none -> 3.16 us  [the longest x1 2.01 us: nearby_weights(): pl.pallas_call(copies_kernel, out_shape=jax.ShapeDtypeStruct((lax.axis_si...]
    broadcast_in_dim x2 -> x0, local copies, waits for them, and re-layouts: 1.93 us -> none  [the longest x1 1.1 us: nearby_weights(): copies = jnp.broadcast_to(own, (lax.axis_size(SP[0]), *own.shape))]
  transfers between devices with their start and end apart: 11 -> 9, of which waited for: 8 -> 5; matrix products, arithmetic and copies ran while one was open for 3% -> 1% of each run, Pallas kernels for 3% -> 4%
where the time goes in v4:
time: 157 us; the launch traced here: 156 us
  blocking collectives  49.1 us (31%)
  waiting for transfers between devices  38 us (24%)
  starting transfers between devices  37.7 us (24%)
  between operations  13.8 us (9%)
  Pallas kernels  13.5 us (9%)
  local copies, waits for them, and re-layouts  2.15 us (1%)
    all_to_all x1, blocking collectives, mix_tokens(): lax.all_to_all(packed, SP, split_axis=0, concat_axis=0, tiled=True)  21.1 us
    all_to_all x1, waiting for transfers between devices, nearby_weights(): lax.all_to_all(copies, (*SP, 'tp'), split_axis=0, concat_axis=0, tiled=Tr...  16.8 us
    all_to_all x1, blocking collectives, incoming_state(): back = lax.all_to_all(entering, SP, split_axis=0, concat_axis=0, tiled=True)  15.2 us
    all_to_all x1, blocking collectives, sent(): return lax.all_to_all(blocks, axis, split_axis=0, concat_axis=0, tiled=True)  12.7 us
    ppermute x3, starting transfers between devices, collected_projection(): blocks.append(lax.ppermute(block, 'tp', path))  10.9 us
    all_to_all x1, starting transfers between devices, nearby_weights(): lax.all_to_all(copies, (*SP, 'tp'), split_axis=0, concat_axis=0, tiled=Tr...  10.9 us
    all_to_all x1, waiting for transfers between devices, middle_rows(): lax.all_to_all(copies, 'tp', split_axis=0, concat_axis=0, tiled=True)  9.36 us
    all_to_all x1, waiting for transfers between devices, sent(): return lax.all_to_all(blocks, axis, split_axis=0, concat_axis=0, tiled=True)  9.23 us
  transfers between devices with their start and end apart: 9, of which 5 were waited for; matrix products, arithmetic and copies ran while one was open for 1% of the time, Pallas kernels for 4%

profile of v4, /device:TPU:1, one launch (start us, length us, event | category | flops | bytes accessed | tf_op | source)
XLA Modules:
  0.0 156.0 jit_solution(9167503031176537032)
XLA Ops:
  6.5 2.0 %copies.1 = bf16[8,32,2112]{2,1,0:T(8,128)(2,1)} custom-call(bf16[32,704]{1,0:T(8,128)(2,1)} %gate_ref.2, bf16[32,704]{1,0:T(8,128)(2,1)} %up_ref.1, bf16[32,704]{1,0:T(8,128)(2,1)} %bitcast.82), custom_call_target="tpu_custom_call" | custom-call | tf_op jit(solution)/shard_map/copies/pallas_call | solution.py:101
  8.6 10.9 %all-to-all-start = ((bf16[8,32,2112]{2,1,0:T(8,128)(2,1)}), bf16[8,32,2112]{2,1,0:T(8,128)(2,1)S(1)}, u32[]{:S(2)}, u32[]{:S(2)}) async-start(bf16[8,32,2112]{2,1,0:T(8,128)(2,1)} %copies.1), calls=%async_computation | async-start | bytes 2228224 | tf_op jit(solution)/shard_map/all_to_all | solution.py:106
  19.7 0.3 convolution_bitcast_fusion.1
  20.1 0.8 while.13
  20.2 0.2 fusion.21
  20.6 0.2 fusion.21
  20.9 0.1 squeeze.16
  21.1 0.2 select_convert_fusion
  21.3 0.1 pad_maximum_fusion.1
  21.4 16.8 %all-to-all-done = bf16[8,32,2112]{2,1,0:T(8,128)(2,1)S(1)} async-done(((bf16[8,32,2112]{2,1,0:T(8,128)(2,1)}), bf16[8,32,2112]{2,1,0:T(8,128)(2,1)S(1)}, u32[]{:S(2)}, u32[]{:S(2)}) %all-to-all-start) | async-done | bytes 1081376 | tf_op jit(solution)/shard_map/all_to_all | solution.py:106
  38.1 1.0 copy-done.8
  39.2 2.3 %collective-permute-start = (bf16[256,1024]{1,0:T(8,128)(2,1)S(1)}, bf16[256,1024]{1,0:T(8,128)(2,1)S(1)}, u32[]{:S(2)}, u32[]{:S(2)}) collective-permute-start(bf16[256,1024]{1,0:T(8,128)(2,1)S(1)} %broadcast_select_fusion.2), channel_id=1, source_target_pairs={{0,1},{1,0},{2,3},{3,2},{4,5},{5,4},{6,7},{7,6},{8,9},{9,8},{10,11... | collective-permute-start | bytes 1572872 | tf_op jit(solution)/shard_map/ppermute | solution.py:149
  41.5 1.5 collective-permute-done
  43.3 4.4 %collective-permute-start.1 = (bf16[512,1024]{1,0:T(8,128)(2,1)S(1)}, bf16[512,1024]{1,0:T(8,128)(2,1)S(1)}, u32[]{:S(2)}, u32[]{:S(2)}) collective-permute-start(bf16[512,1024]{1,0:T(8,128)(2,1)S(1)} %pad_maximum_fusion.refs_0_), channel_id=1, source_target_pairs={{0,4},{1,5},{2,6},{3,7},{4,0},{5,1},{6,2},{7,3},{8,12},{9,13},{10,... | collective-permute-start | bytes 3145736 | tf_op jit(solution)/shard_map/ppermute | solution.py:155
  47.7 2.2 %collective-permute-start.2 = (bf16[512,1024]{1,0:T(8,128)(2,1)S(1)}, bf16[512,1024]{1,0:T(8,128)(2,1)}, u32[]{:S(2)}, u32[]{:S(2)}) collective-permute-start(bf16[512,1024]{1,0:T(8,128)(2,1)S(1)} %pad_maximum_fusion.refs_0_), channel_id=1, source_target_pairs={{0,2},{1,3},{2,4},{3,5},{4,6},{5,7},{6,0},{7,1},{8,10},{9,11},{10,... | collective-permute-start | bytes 3145736 | tf_op jit(solution)/shard_map/ppermute | solution.py:155
  49.9 4.3 %collective-permute-start.3 = (bf16[512,1024]{1,0:T(8,128)(2,1)S(1)}, bf16[512,1024]{1,0:T(8,128)(2,1)}, u32[]{:S(2)}, u32[]{:S(2)}) collective-permute-start(bf16[512,1024]{1,0:T(8,128)(2,1)S(1)} %pad_maximum_fusion.refs_0_), channel_id=1, source_target_pairs={{0,6},{1,7},{2,0},{3,1},{4,2},{5,3},{6,4},{7,5},{8,14},{9,15},{10,... | collective-permute-start | bytes 3145736 | tf_op jit(solution)/shard_map/ppermute | solution.py:155
  54.2 21.1 %all_to_all.30 = bf16[64,2,384]{2,1,0:T(2,128)(2,1)S(1)} all-to-all(bf16[64,2,384]{2,1,0:T(2,128)(2,1)S(1)} %pad_maximum_fusion.1), channel_id=1, replica_groups=mesh['sp_0'=8,'sp_1'=8,'tp'=8] {'sp_0','sp_1'}, dimensions={0} | all-to-all | bytes 196608 | tf_op jit(solution)/shard_map/all_to_all | solution.py:306
  75.3 1.2 prefix.1
  76.6 15.2 %all_to_all.31 = bf16[64,2,256]{2,1,0:T(2,128)(2,1)S(1)} all-to-all(bf16[64,2,256]{2,1,0:T(2,128)(2,1)S(1)} %reshape.139), channel_id=1, replica_groups=mesh['sp_0'=8,'sp_1'=8,'tp'=8] {'sp_0','sp_1'}, dimensions={0} | all-to-all | bytes 131072 | tf_op jit(solution)/shard_map/all_to_all | solution.py:73
  91.8 1.2 gate.1
  93.0 7.2 %all-to-all-start.3 = ((bf16[8,128,256]{2,1,0:T(8,128)(2,1)}), bf16[8,128,256]{2,1,0:T(8,128)(2,1)S(1)}, u32[]{:S(2)}, u32[]{:S(2)}) async-start(bf16[8,128,256]{2,1,0:T(8,128)(2,1)} %gate.1), calls=%async_computation.3 | async-start | bytes 1048576 | tf_op jit(solution)/shard_map/all_to_all | solution.py:203
  100.3 9.4 %all-to-all-done.3.gated_ref = bf16[8,128,256]{2,1,0:T(8,128)(2,1)S(1)} async-done(((bf16[8,128,256]{2,1,0:T(8,128)(2,1)}), bf16[8,128,256]{2,1,0:T(8,128)(2,1)S(1)}, u32[]{:S(2)}, u32[]{:S(2)}) %all-to-all-start.3) | async-done | bytes 524320 | tf_op jit(solution)/shard_map/all_to_all | solution.py:203
  109.6 2.3 %project.1.own_ref = bf16[128,1024]{1,0:T(8,128)(2,1)S(1)} custom-call(s32[1]{0:T(128)} %bitcast.place_ref, bf16[8,128,256]{2,1,0:T(8,128)(2,1)S(1)} %all-to-all-done.3.gated_ref, bf16[512,1024]{1,0:T(8,128)(2,1)S(1)} %pad_maximum_fusion.refs_0_, bf16[512,1024]{1,0:T(8,128)(2,1)S(1)} %collective-permute-done.1.refs_1_, ...), custom_call_target="tpu_custom_call" | custom-call | tf_op jit(solution)/shard_map/project/pallas_call | solution.py:204
  112.0 2.9 %collective-permute-start.4 = (bf16[128,1024]{1,0:T(8,128)(2,1)S(1)}, bf16[128,1024]{1,0:T(8,128)(2,1)S(1)}, u32[]{:S(2)}, u32[]{:S(2)}) collective-permute-start(bf16[128,1024]{1,0:T(8,128)(2,1)S(1)} %project.1.own_ref), channel_id=1, source_target_pairs={{0,1},{1,0},{2,3},{3,2},{4,5},{5,4},{6,7},{7,6},{8,9},{9,8},{10,11... | collective-permute-start | bytes 786440 | tf_op jit(solution)/shard_map/ppermute | solution.py:212
  114.8 1.1 collective-permute-done.4.other_ref
  116.0 1.0 middle.1
  117.0 5.5 %mix_channels.1 = bf16[128,2048]{1,0:T(8,128)(2,1)} custom-call(bf16[128,2048]{1,0:T(8,128)(2,1)S(1)} %get-tuple-element.45.mid_ref, bf16[2048,2112]{1,0:T(8,128)(2,1)} %all-gather.2.cloned.1.call-done.weights_ref), custom_call_target="tpu_custom_call" | custom-call | flops 1107296256 | bytes 8650752 | tf_op jit(solution)/shard_map/mix_channels/pallas_call | solution.py:367
  122.5 3.5 %all-to-all-start.4 = ((bf16[8,16,2048]{2,1,0:T(8,128)(2,1)}), bf16[8,16,2048]{2,1,0:T(8,128)(2,1)S(1)}, u32[]{:S(2)}, u32[]{:S(2)}) async-start(bf16[8,16,2048]{2,1,0:T(8,128)(2,1)} %bitcast.21), calls=%async_computation.4 | async-start | bytes 1048576 | tf_op jit(solution)/shard_map/all_to_all | solution.py:257
  126.0 9.2 %all-to-all-done.4.arrived_ref = bf16[8,16,2048]{2,1,0:T(8,128)(2,1)S(1)} async-done(((bf16[8,16,2048]{2,1,0:T(8,128)(2,1)}), bf16[8,16,2048]{2,1,0:T(8,128)(2,1)S(1)}, u32[]{:S(2)}, u32[]{:S(2)}) %all-to-all-start.4) | async-done | bytes 524320 | tf_op jit(solution)/shard_map/all_to_all | solution.py:257
  135.3 0.4 settle.1
  135.7 12.7 %all_to_all.32 = bf16[8,16,2048]{2,1,0:T(8,128)(2,1)S(1)} all-to-all(bf16[8,16,2048]{2,1,0:T(8,128)(2,1)S(1)} %settle.1), channel_id=1, replica_groups=mesh['sp_0'=8,'sp_1'=8,'tp'=8] {'tp'}, dimensions={0} | all-to-all | bytes 1048576 | tf_op jit(solution)/shard_map/all_to_all | solution.py:257
  148.4 0.8 copy.36
  (57 shorter events, 0.9 us)
Async XLA Ops:
  6.5 13.2 %copy-start = (bf16[128,256]{1,0:T(8,128)(2,1)S(1)}, bf16[128,256]{1,0:T(8,128)(2,1)}, u32[]{:S(2)}) copy-start(bf16[128,256]{1,0:T(8,128)(2,1)} %param.20) | copy-start | bytes 196612
  6.5 12.9 %copy-start.10 = (f32[128,128]{1,0:T(8,128)S(1)}, f32[128,128]{1,0:T(8,128)}, u32[]{:S(2)}) copy-start(f32[128,128]{1,0:T(8,128)} %param.21) | copy-start | bytes 196612
  6.5 13.1 %copy-start.11 = (bf16[128,128]{1,0:T(8,128)(2,1)S(1)}, bf16[128,128]{1,0:T(8,128)(2,1)}, u32[]{:S(2)}) copy-start(bf16[128,128]{1,0:T(8,128)(2,1)} %param.18) | copy-start | bytes 98308
  6.5 13.2 %copy-start.12 = (bf16[128,128]{1,0:T(8,128)(2,1)S(1)}, bf16[128,128]{1,0:T(8,128)(2,1)}, u32[]{:S(2)}) copy-start(bf16[128,128]{1,0:T(8,128)(2,1)} %param.19) | copy-start | bytes 98308
  8.6 29.6 %all-to-all-start = ((bf16[8,32,2112]{2,1,0:T(8,128)(2,1)}), bf16[8,32,2112]{2,1,0:T(8,128)(2,1)S(1)}, u32[]{:S(2)}, u32[]{:S(2)}) async-start(bf16[8,32,2112]{2,1,0:T(8,128)(2,1)} %copies.1), calls=%async_computation | async-start | bytes 2228224 | tf_op jit(solution)/shard_map/all_to_all | solution.py:106
  19.4 97.6 %all-gather.2.cloned.1.call-start = ((), (), s32[]{:S(2)}) async-start(), calls=%async_computation.6 | async-start | bytes 10027008 | tf_op jit(solution)/shard_map/all_gather | solution.py:118
  20.1 19.1 %copy-start.9 = (bf16[256,2048]{1,0:T(8,128)(2,1)S(1)}, bf16[256,2048]{1,0:T(8,128)(2,1)}, u32[]{:S(2)}) copy-start(bf16[256,2048]{1,0:T(8,128)(2,1)} %param.24) | copy-start | bytes 3145732
  38.1 1.0 copy-start.8
  39.2 3.8 %collective-permute-start = (bf16[256,1024]{1,0:T(8,128)(2,1)S(1)}, bf16[256,1024]{1,0:T(8,128)(2,1)S(1)}, u32[]{:S(2)}, u32[]{:S(2)}) collective-permute-start(bf16[256,1024]{1,0:T(8,128)(2,1)S(1)} %broadcast_select_fusion.2), channel_id=1, source_target_pairs={{0,1},{1,0},{2,3},{3,2},{4,5},{5,4},{6,7},{7,6},{8,9},{9,8},{10,11... | collective-permute-start | bytes 1572872 | tf_op jit(solution)/shard_map/ppermute | solution.py:149
  43.2 48.7 %copy-start.2 = (bf16[128,256]{1,0:T(8,128)(2,1)S(1)}, bf16[128,256]{1,0:T(8,128)(2,1)}, u32[]{:S(2)}) copy-start(bf16[128,256]{1,0:T(8,128)(2,1)} %gate_ref.3) | copy-start | bytes 196612
  43.2 48.7 %copy-start.7 = (f32[256]{0:T(256)S(1)}, f32[256]{0:T(256)}, u32[]{:S(2)}) copy-start(f32[256]{0:T(256)} %param.23) | copy-start | bytes 3076
  43.3 57.0 %collective-permute-start.1 = (bf16[512,1024]{1,0:T(8,128)(2,1)S(1)}, bf16[512,1024]{1,0:T(8,128)(2,1)S(1)}, u32[]{:S(2)}, u32[]{:S(2)}) collective-permute-start(bf16[512,1024]{1,0:T(8,128)(2,1)S(1)} %pad_maximum_fusion.refs_0_), channel_id=1, source_target_pairs={{0,4},{1,5},{2,6},{3,7},{4,0},{5,1},{6,2},{7,3},{8,12},{9,13},{10,... | collective-permute-start | bytes 3145736 | tf_op jit(solution)/shard_map/ppermute | solution.py:155
  47.7 52.6 %collective-permute-start.2 = (bf16[512,1024]{1,0:T(8,128)(2,1)S(1)}, bf16[512,1024]{1,0:T(8,128)(2,1)}, u32[]{:S(2)}, u32[]{:S(2)}) collective-permute-start(bf16[512,1024]{1,0:T(8,128)(2,1)S(1)} %pad_maximum_fusion.refs_0_), channel_id=1, source_target_pairs={{0,2},{1,3},{2,4},{3,5},{4,6},{5,7},{6,0},{7,1},{8,10},{9,11},{10,... | collective-permute-start | bytes 3145736 | tf_op jit(solution)/shard_map/ppermute | solution.py:155
  49.9 50.3 %collective-permute-start.3 = (bf16[512,1024]{1,0:T(8,128)(2,1)S(1)}, bf16[512,1024]{1,0:T(8,128)(2,1)}, u32[]{:S(2)}, u32[]{:S(2)}) collective-permute-start(bf16[512,1024]{1,0:T(8,128)(2,1)S(1)} %pad_maximum_fusion.refs_0_), channel_id=1, source_target_pairs={{0,6},{1,7},{2,0},{3,1},{4,2},{5,3},{6,4},{7,5},{8,14},{9,15},{10,... | collective-permute-start | bytes 3145736 | tf_op jit(solution)/shard_map/ppermute | solution.py:155
  93.0 16.6 %all-to-all-start.3 = ((bf16[8,128,256]{2,1,0:T(8,128)(2,1)}), bf16[8,128,256]{2,1,0:T(8,128)(2,1)S(1)}, u32[]{:S(2)}, u32[]{:S(2)}) async-start(bf16[8,128,256]{2,1,0:T(8,128)(2,1)} %gate.1), calls=%async_computation.3 | async-start | bytes 1048576 | tf_op jit(solution)/shard_map/all_to_all | solution.py:203
  109.6 6.4 %copy-start.1 = (bf16[128,2048]{1,0:T(8,128)(2,1)S(1)}, bf16[128,2048]{1,0:T(8,128)(2,1)}, u32[]{:S(2)}) copy-start(bf16[128,2048]{1,0:T(8,128)(2,1)} %before_ref.1) | copy-start | bytes 1572868
  109.6 6.4 %copy-start.3 = (f32[2048]{0:T(1024)S(1)}, f32[2048]{0:T(1024)}, u32[]{:S(2)}) copy-start(f32[2048]{0:T(1024)} %param.25) | copy-start | bytes 24580
  109.6 6.4 %copy-start.4 = (f32[2048]{0:T(1024)S(1)}, f32[2048]{0:T(1024)}, u32[]{:S(2)}) copy-start(f32[2048]{0:T(1024)} %param.26) | copy-start | bytes 24580
  112.0 4.0 %collective-permute-start.4 = (bf16[128,1024]{1,0:T(8,128)(2,1)S(1)}, bf16[128,1024]{1,0:T(8,128)(2,1)S(1)}, u32[]{:S(2)}, u32[]{:S(2)}) collective-permute-start(bf16[128,1024]{1,0:T(8,128)(2,1)S(1)} %project.1.own_ref), channel_id=1, source_target_pairs={{0,1},{1,0},{2,3},{3,2},{4,5},{5,4},{6,7},{7,6},{8,9},{9,8},{10,11... | collective-permute-start | bytes 786440 | tf_op jit(solution)/shard_map/ppermute | solution.py:212
  117.0 18.2 %copy-start.5 = (f32[2048]{0:T(1024)S(1)}, f32[2048]{0:T(1024)}, u32[]{:S(2)}) copy-start(f32[2048]{0:T(1024)} %param.30) | copy-start | bytes 24580
  117.0 18.2 %copy-start.6 = (f32[2048]{0:T(1024)S(1)}, f32[2048]{0:T(1024)}, u32[]{:S(2)}) copy-start(f32[2048]{0:T(1024)} %param.31) | copy-start | bytes 24580
  122.5 12.7 %all-to-all-start.4 = ((bf16[8,16,2048]{2,1,0:T(8,128)(2,1)}), bf16[8,16,2048]{2,1,0:T(8,128)(2,1)S(1)}, u32[]{:S(2)}, u32[]{:S(2)}) async-start(bf16[8,16,2048]{2,1,0:T(8,128)(2,1)} %bitcast.21), calls=%async_computation.4 | async-start | bytes 1048576 | tf_op jit(solution)/shard_map/all_to_all | solution.py:257
Sparse Core Ops, SparseCore 0:
  39.3 60.5 all-gather.1

commit v5 on v4

--- a/solution.py
+++ b/solution.py
@@ -12,6 +12,7 @@
 HV = 256
 SPAN = 64
 SP = ("sp_0", "sp_1")
+FAR = (2, 1, 3)
 
 
 ALPHA = 2.0**0.25
@@ -20,13 +21,54 @@
 TAU = 16.0
 
 
-def with_decay(state, logs):
-    coarse = lax.reduce_precision(logs, 8, 7)
-    lane = lax.broadcasted_iota(jnp.int32, (*logs.shape, 128), logs.ndim)
-    extra = jnp.where(
-        lane == 0, coarse[..., None], jnp.where(lane == 1, (logs - coarse)[..., None], 0.0)
-    )
-    return jnp.concatenate([state, extra], axis=-1).astype(jnp.bfloat16)
+def local_kernel(
+    queries_ref, keys_ref, values_ref, decay_ref, packed_ref, readers_ref, local_ref
+):
+    exact = dict(precision=lax.Precision.HIGHEST, preferred_element_type=jnp.float32)
+    over_tokens = (((0,), (0,)), ((), ()))
+    row = lax.broadcasted_iota(jnp.int32, (SPAN, SPAN), 0)
+    col = lax.broadcasted_iota(jnp.int32, (SPAN, SPAN), 1)
+    until = (col <= row).astype(jnp.float32)
+    state, before, logs = None, 0.0, 0.0
+    for at in range(0, queries_ref.shape[0], SPAN):
+        rows = pl.ds(at, SPAN)
+        pre = decay_ref[rows]
+        logdecay = (jnp.minimum(pre, 0.0) - jnp.log1p(jnp.exp(-jnp.abs(pre)))) / TAU
+        cumul = jnp.dot(until, logdecay, **exact)
+        last = cumul[SPAN - 1 :]
+        decayed = keys_ref[rows].astype(jnp.float32) * jnp.exp(last - cumul)
+        update = lax.dot_general(
+            decayed, values_ref[rows].astype(jnp.float32), over_tokens, **exact
+        )
+        if state is None:
+            state = update
+        else:
+            ends = lax.dot_general(logdecay, jnp.ones((SPAN, HV), jnp.float32), over_tokens, **exact)
+            state = jnp.exp(ends) * state + update
+        scaled_q = queries_ref[rows].astype(jnp.float32) * HK ** (-0.5)
+        local_ref[rows] = jnp.dot(scaled_q, state, **exact)
+        before, logs = before + last, logs + logdecay
+        readers_ref[rows] = scaled_q * jnp.exp(before)
+    total = lax.dot_general(logs, jnp.ones((SPAN, 128), jnp.float32), over_tokens, **exact)
+    coarse = total.astype(jnp.bfloat16).astype(jnp.float32)
+    lane = lax.broadcasted_iota(jnp.int32, total.shape, 1)
+    extra = jnp.where(lane == 0, coarse, jnp.where(lane == 1, total - coarse, 0.0))
+    packed_ref[:, :HV] = state.astype(jnp.bfloat16)
+    packed_ref[:, HV:] = extra.astype(jnp.bfloat16)
+
+
+def local_states(queries, keys, values, decay_pre):
+    tokens = queries.shape[0]
+    return pl.pallas_call(
+        local_kernel,
+        out_shape=(
+            jax.ShapeDtypeStruct((HK, HV + 128), jnp.bfloat16),
+            jax.ShapeDtypeStruct((tokens, HK), jnp.float32),
+            jax.ShapeDtypeStruct((tokens, HV), jnp.float32),
+        ),
+        compiler_params=pltpu.CompilerParams(vmem_limit_bytes=8 << 20),
+        name="local",
+    )(queries, keys, values, decay_pre)
 
 
 def prefix_kernel(packed_ref, out_ref):
@@ -90,10 +132,19 @@
     ]
 
 
-def copies_kernel(gate_ref, up_ref, down_ref, out_ref):
-    own = jnp.concatenate([gate_ref[...], up_ref[...], down_ref[...]], axis=1)
-    for k in range(out_ref.shape[0]):
-        out_ref[k] = own
+def give_copies(made_ref, out_ref, sems):
+    copies = [
+        pltpu.make_async_copy(made_ref, out_ref.at[k], sems.at[k]) for k in range(out_ref.shape[0])
+    ]
+    for copy in copies:
+        copy.start()
+    for copy in copies:
+        copy.wait()
+
+
+def copies_kernel(gate_ref, up_ref, down_ref, out_ref, made_ref, sems):
+    made_ref[...] = jnp.concatenate([gate_ref[...], up_ref[...], down_ref[...]], axis=1)
+    give_copies(made_ref, out_ref, sems)
 
 
 def nearby_weights(gate_in, up_in, down_out):
@@ -101,6 +152,11 @@
     copies = pl.pallas_call(
         copies_kernel,
         out_shape=jax.ShapeDtypeStruct((lax.axis_size(SP[0]), rows, 3 * units), jnp.bfloat16),
+        out_specs=pl.BlockSpec(memory_space=pltpu.HBM),
+        scratch_shapes=[
+            pltpu.VMEM((rows, 3 * units), jnp.bfloat16),
+            pltpu.SemaphoreType.DMA((lax.axis_size(SP[0]),)),
+        ],
         name="copies",
     )(gate_in, up_in, down_out.T)
     arrived = lax.all_to_all(
@@ -142,49 +198,38 @@
 
 def collected_projection(out_proj):
     parts = lax.axis_size("tp")
-    chips, wide = parts // 2, out_proj.shape[1] // 2
-    first = lax.axis_index("tp") % 2 == 0
-    left, right = out_proj[:, :wide], out_proj[:, wide:]
-    swap = [(part, part ^ 1) for part in range(parts)]
-    other = lax.ppermute(jnp.where(first, right, left), "tp", swap)
-    own = jnp.where(first, left, right)
-    block = jnp.concatenate([jnp.where(first, own, other), jnp.where(first, other, own)], axis=0)
-    blocks = [block]
-    for step in (2, 1, 3)[: chips - 1]:
+    blocks = [out_proj]
+    for step in FAR[: parts // 2 - 1]:
         path = [(part, (part + 2 * step) % parts) for part in range(parts)]
-        blocks.append(lax.ppermute(block, "tp", path))
+        blocks.append(lax.ppermute(out_proj, "tp", path))
     return blocks
 
 
 def project_kernel(steps, place_ref, gated_ref, *refs):
     out_ref = refs[-1]
-    chip, depth = place_ref[0] // 2, gated_ref.shape[2]
-    count = gated_ref.shape[0] // 2
+    chip, count = place_ref[0] // 2, gated_ref.shape[0]
     for at in range(0, out_ref.shape[1], 256):
         total = None
         for step, block_ref in zip(steps, refs[:-1]):
-            source = lax.rem(chip + (count - step), count)
-            for core in range(2):
-                product = jnp.dot(
-                    gated_ref[2 * source + core],
-                    block_ref[core * depth : (core + 1) * depth, at : at + 256],
-                    preferred_element_type=jnp.float32,
-                )
-                total = product if total is None else total + product
+            product = jnp.dot(
+                gated_ref[lax.rem(chip + (count - step), count)],
+                block_ref[:, at : at + 256],
+                preferred_element_type=jnp.float32,
+            )
+            total = product if total is None else total + product
         out_ref[:, at : at + 256] = total.astype(jnp.bfloat16)
 
 
 def middle_kernel(
     outer, width, place_ref, own_ref, other_ref, before_ref, gain_ref, shift_ref, mid_ref, turned_ref
 ):
-    own, other = own_ref[...].astype(jnp.float32), other_ref[...].astype(jnp.float32)
-    odd = lax.rem(place_ref[0], 2) == 1
-    mixed = jnp.concatenate([jnp.where(odd, other, own), jnp.where(odd, own, other)], axis=1)
+    mixed = own_ref[...].astype(jnp.float32) + other_ref[...].astype(jnp.float32)
     inputs = ALPHA * before_ref[...].astype(jnp.float32) + mixed
     center = inputs - jnp.mean(inputs, axis=-1, keepdims=True)
     spread = jnp.mean(center * center, axis=-1, keepdims=True)
     rows = center * lax.rsqrt(spread + LN_EPS) * gain_ref[...] + shift_ref[...]
     rows = rows.astype(jnp.bfloat16)
+    odd = lax.rem(place_ref[0], 2) == 1
     mid_ref[...] = rows
 
     @pl.when(jnp.logical_not(odd))
@@ -200,10 +245,18 @@
     parts = lax.axis_size("tp")
     place = lax.axis_index("tp")[None].astype(jnp.int32)
     smem, vmem = (pl.BlockSpec(memory_space=space) for space in (pltpu.SMEM, pltpu.VMEM))
-    everyone = lax.all_to_all(copies, "tp", split_axis=0, concat_axis=0, tiled=True)
+    everyone = lax.all_to_all(
+        copies,
+        "tp",
+        split_axis=0,
+        concat_axis=0,
+        tiled=True,
+        axis_index_groups=[list(range(core, parts, 2)) for core in range(2)],
+    )
+    rows = jax.ShapeDtypeStruct(resid.shape, jnp.bfloat16)
     own = pl.pallas_call(
-        functools.partial(project_kernel, (0, 2, 1, 3)),
-        out_shape=jax.ShapeDtypeStruct((resid.shape[0], blocks[0].shape[1]), jnp.bfloat16),
+        functools.partial(project_kernel, (0, *FAR)),
+        out_shape=rows,
         in_specs=[smem] + [vmem] * (1 + len(blocks)),
         out_specs=vmem,
         compiler_params=pltpu.CompilerParams(vmem_limit_bytes=16 << 20),
@@ -211,7 +264,6 @@
     )(place, everyone, *blocks)
     other = lax.ppermute(own, "tp", [(part, part ^ 1) for part in range(parts)])
     outer = lax.axis_size(SP[0])
-    rows = jax.ShapeDtypeStruct(resid.shape, jnp.bfloat16)
     return pl.pallas_call(
         functools.partial(middle_kernel, outer, resid.shape[1] // (outer * lax.axis_size(SP[1]))),
         out_shape=(rows, rows),
@@ -257,7 +309,7 @@
     return lax.all_to_all(blocks, axis, split_axis=0, concat_axis=0, tiled=True)
 
 
-def gate_kernel(readers_ref, state_ref, local_ref, gate_ref, gain_ref, out_ref):
+def gate_kernel(readers_ref, state_ref, local_ref, gate_ref, gain_ref, out_ref, made_ref, sems):
     readout = local_ref[...] + jnp.dot(
         readers_ref[...],
         state_ref[...].astype(jnp.float32),
@@ -266,53 +318,30 @@
     )
     square = jnp.mean(readout * readout, axis=-1, keepdims=True)
     normed = readout * lax.rsqrt(square + RMS_EPS) * gain_ref[...]
-    gated = (normed * jax.nn.silu(gate_ref[...].astype(jnp.float32))).astype(jnp.bfloat16)
-    for k in range(out_ref.shape[0]):
-        out_ref[k] = gated
-
-
-def mix_tokens(queries, keys, values, decay_pre, out_gate, head_gain, nearby):
-    tok_rows = queries.shape[0]
-    local_heads = queries.shape[1] // HK
-    blocks = tok_rows // SPAN
-    logdecay = jax.nn.log_sigmoid(decay_pre) / TAU
-    scaled_q = queries.astype(jnp.float32).reshape(blocks, SPAN, local_heads, HK) * HK ** (-0.5)
-    key_block = keys.astype(jnp.float32).reshape(blocks, SPAN, local_heads, HK)
-    value_block = values.astype(jnp.float32).reshape(blocks, SPAN, local_heads, HV)
-    cumul = jnp.cumsum(logdecay.reshape(blocks, SPAN, local_heads, HK), axis=1)
-    last = cumul[:, -1]
-    key_decayed = key_block * jnp.exp(last[:, None] - cumul)
-    updates = jnp.einsum(
-        "nchk,nchv->nhkv", key_decayed, value_block, precision=lax.Precision.HIGHEST
-    )
-
-    def advance(running_state, inputs):
-        decay_end, state_increment, current_query = inputs
-        running_state = jnp.exp(decay_end)[..., None] * running_state + state_increment
-        return (
-            running_state,
-            jnp.einsum(
-                "qpy,pyr->qpr", current_query, running_state, precision=lax.Precision.HIGHEST
-            ),
-        )
-
-    own_state, local_read = lax.scan(
-        advance, jnp.zeros((local_heads, HK, HV), jnp.float32), (last, updates, scaled_q)
-    )
-    block_ends = jnp.cumsum(last, axis=0)
-    packed = with_decay(own_state[0], block_ends[-1, 0]).reshape(lax.axis_size(SP), -1, HV + 128)
+    made_ref[...] = (normed * jax.nn.silu(gate_ref[...].astype(jnp.float32))).astype(jnp.bfloat16)
+    give_copies(made_ref, out_ref, sems)
+
+
+def mix_tokens(queries, keys, values, decay_pre, out_gate, head_gain, nearby, blocks):
+    packed, readers, local_read = local_states(queries, keys, values, decay_pre)
+    packed = packed.reshape(lax.axis_size(SP), -1, HV + 128)
     packed, nearby = lax.optimization_barrier((packed, nearby))
     weights = gathered_weights(nearby)
     arrived = lax.all_to_all(packed, SP, split_axis=0, concat_axis=0, tiled=True)
-    incoming = incoming_state(arrived, own_state.shape[1:])
-    readers = (scaled_q * jnp.exp(block_ends)[:, None]).reshape(tok_rows, HK)
+    incoming = incoming_state(arrived, (HK, HV))
+    incoming, *blocks = lax.optimization_barrier((incoming, *blocks))
     copies = pl.pallas_call(
         gate_kernel,
-        out_shape=jax.ShapeDtypeStruct((lax.axis_size("tp"), *values.shape), jnp.bfloat16),
-        compiler_params=pltpu.CompilerParams(vmem_limit_bytes=8 << 20),
+        out_shape=jax.ShapeDtypeStruct((lax.axis_size("tp") // 2, *values.shape), jnp.bfloat16),
+        out_specs=pl.BlockSpec(memory_space=pltpu.HBM),
+        scratch_shapes=[
+            pltpu.VMEM(values.shape, jnp.bfloat16),
+            pltpu.SemaphoreType.DMA((lax.axis_size("tp") // 2,)),
+        ],
+        compiler_params=pltpu.CompilerParams(vmem_limit_bytes=60 << 20),
         name="gate",
-    )(readers, incoming, local_read.reshape(tok_rows, HV), out_gate, head_gain[None])
-    return copies, weights
+    )(readers, incoming, local_read, out_gate, head_gain[None])
+    return copies, blocks, weights
 
 
 def mixer_kernel(units, depth, mid_ref, weights_ref, out_ref, held, total, made, sems, out_sems):
@@ -407,7 +436,9 @@
     own_count = queries.shape[0] // lax.axis_size("tp")
     nearby = nearby_weights(gate_in, up_in, down_out)
     blocks = collected_projection(out_proj)
-    gated_copies, weights = mix_tokens(queries, keys, values, decay_pre, out_gate, head_gain, nearby)
+    gated_copies, blocks, weights = mix_tokens(
+        queries, keys, values, decay_pre, out_gate, head_gain, nearby, blocks
+    )
     mid, mid_turned = middle_rows(gated_copies, blocks, resid, mix_gain, mix_shift)
     ffn = sent(mix_channels(mid_turned, weights), "tp")
     own_mid = lax.dynamic_slice_in_dim(mid, lax.axis_index("tp") * own_count, own_count, 0)

time: 157 us -> 151 us (0.962)
  starting transfers between devices: 37.7 us -> 33.8 us
  waiting for transfers between devices: 38 us -> 35.6 us
  Pallas kernels: 13.5 us -> 15.7 us
  local copies, waits for them, and re-layouts: 2.15 us -> 3.83 us
    all_to_all x1, waiting for transfers between devices: 9.36 us -> 5.49 us  [middle_rows(): lax.all_to_all(copies, 'tp', split_axis=0, concat_axis=0, tiled=True, axi...]
    all_to_all x1, starting transfers between devices: 7.25 us -> 3.42 us  [middle_rows(): lax.all_to_all(copies, 'tp', split_axis=0, concat_axis=0, tiled=True, axi...]
    ppermute x4 -> x3, starting transfers between devices: 13.2 us -> 10.9 us  [collected_projection(): blocks.append(lax.ppermute(out_proj, 'tp', path))]
    ppermute x1, starting transfers between devices: 2.87 us -> 4.95 us  [middle_rows(): other = lax.ppermute(own, 'tp', [(part, part ^ 1) for part in range(parts)])]
    ppermute x4 -> x3, waiting for transfers between devices: 1.52 us -> 3.44 us  [collected_projection(): blocks.append(lax.ppermute(out_proj, 'tp', path))]
    pallas_call x1 -> x2, Pallas kernels: 2.32 us -> 3.48 us  [the longest x1 2 us: middle_rows(): pl.pallas_call(functools.partial(project_kernel, (0, *FAR)), out_shape=ro...]
  transfers between devices with their start and end apart: 9 -> 8, of which waited for: 5 -> 5; matrix products, arithmetic and copies ran while one was open for 1% -> 0% of each run, Pallas kernels for 4% -> 5%
where the time goes in v5:
time: 151 us; the launch traced here: 150 us
  blocking collectives  47.6 us (32%)
  waiting for transfers between devices  35.6 us (24%)
  starting transfers between devices  33.8 us (22%)
  Pallas kernels  15.7 us (10%)
  between operations  13.6 us (9%)
  local copies, waits for them, and re-layouts  3.83 us (3%)
    all_to_all x1, blocking collectives, mix_tokens(): lax.all_to_all(packed, SP, split_axis=0, concat_axis=0, tiled=True)  19.7 us
    all_to_all x1, waiting for transfers between devices, nearby_weights(): lax.all_to_all(copies, (*SP, 'tp'), split_axis=0, concat_axis=0, tiled=Tr...  15.8 us
    all_to_all x1, blocking collectives, incoming_state(): back = lax.all_to_all(entering, SP, split_axis=0, concat_axis=0, tiled=True)  15.2 us
    all_to_all x1, blocking collectives, sent(): return lax.all_to_all(blocks, axis, split_axis=0, concat_axis=0, tiled=True)  12.7 us
    all_to_all x1, starting transfers between devices, nearby_weights(): lax.all_to_all(copies, (*SP, 'tp'), split_axis=0, concat_axis=0, tiled=Tr...  11 us
    ppermute x3, starting transfers between devices, collected_projection(): blocks.append(lax.ppermute(out_proj, 'tp', path))  10.9 us
    all_to_all x1, waiting for transfers between devices, sent(): return lax.all_to_all(blocks, axis, split_axis=0, concat_axis=0, tiled=True)  9.23 us
    all_to_all x1, waiting for transfers between devices, middle_rows(): lax.all_to_all(copies, 'tp', split_axis=0, concat_axis=0, tiled=True, axi...  5.49 us
  transfers between devices with their start and end apart: 8, of which 5 were waited for; matrix products, arithmetic and copies ran while one was open for 0% of the time, Pallas kernels for 5%

profile of v5, /device:TPU:1, one launch (start us, length us, event | category | flops | bytes accessed | tf_op | source)
XLA Modules:
  0.0 150.1 jit_solution(4120008717613387271)
XLA Ops:
  6.5 2.0 %copies.1 = bf16[8,32,2112]{2,1,0:T(8,128)(2,1)} custom-call(bf16[32,704]{1,0:T(8,128)(2,1)} %gate_ref.2, bf16[32,704]{1,0:T(8,128)(2,1)} %up_ref.1, bf16[32,704]{1,0:T(8,128)(2,1)} %bitcast.20), custom_call_target="tpu_custom_call" | custom-call | tf_op jit(solution)/shard_map/copies/pallas_call | solution.py:152
  8.6 0.0 copy-start.6
  8.6 11.0 %all-to-all-start = ((bf16[8,32,2112]{2,1,0:T(8,128)(2,1)}), bf16[8,32,2112]{2,1,0:T(8,128)(2,1)S(1)}, u32[]{:S(2)}, u32[]{:S(2)}) async-start(bf16[8,32,2112]{2,1,0:T(8,128)(2,1)} %copies.1), calls=%async_computation | async-start | bytes 2228224 | tf_op jit(solution)/shard_map/all_to_all | solution.py:162
  19.6 0.0 all-gather.2.cloned.1.call-start
  19.7 1.5 local.1
  21.2 0.6 copy-done.2
  21.8 0.6 copy-done.5
  22.5 15.8 %all-to-all-done = bf16[8,32,2112]{2,1,0:T(8,128)(2,1)S(1)} async-done(((bf16[8,32,2112]{2,1,0:T(8,128)(2,1)}), bf16[8,32,2112]{2,1,0:T(8,128)(2,1)S(1)}, u32[]{:S(2)}, u32[]{:S(2)}) %all-to-all-start) | async-done | bytes 1081376 | tf_op jit(solution)/shard_map/all_to_all | solution.py:162
  38.3 1.0 copy-done.12
  39.3 0.0 all-gather.2.cloned.1.call-update
  39.4 4.4 %collective-permute-start = (bf16[256,2048]{1,0:T(8,128)(2,1)S(1)}, bf16[256,2048]{1,0:T(8,128)(2,1)S(1)}, u32[]{:S(2)}, u32[]{:S(2)}) collective-permute-start(bf16[256,2048]{1,0:T(8,128)(2,1)S(1)} %copy-done), channel_id=1, source_target_pairs={{0,4},{1,5},{2,6},{3,7},{4,0},{5,1},{6,2},{7,3},{8,12},{9,13},{10,... | collective-permute-start | bytes 3145736 | tf_op jit(solution)/shard_map/ppermute | solution.py:204
  43.8 2.2 %collective-permute-start.1 = (bf16[256,2048]{1,0:T(8,128)(2,1)S(1)}, bf16[256,2048]{1,0:T(8,128)(2,1)S(1)}, u32[]{:S(2)}, u32[]{:S(2)}) collective-permute-start(bf16[256,2048]{1,0:T(8,128)(2,1)S(1)} %copy-done), channel_id=1, source_target_pairs={{0,2},{1,3},{2,4},{3,5},{4,6},{5,7},{6,0},{7,1},{8,10},{9,11},{10,... | collective-permute-start | bytes 3145736 | tf_op jit(solution)/shard_map/ppermute | solution.py:204
  46.0 4.3 %collective-permute-start.2 = (bf16[256,2048]{1,0:T(8,128)(2,1)S(1)}, bf16[256,2048]{1,0:T(8,128)(2,1)}, u32[]{:S(2)}, u32[]{:S(2)}) collective-permute-start(bf16[256,2048]{1,0:T(8,128)(2,1)S(1)} %copy-done), channel_id=1, source_target_pairs={{0,6},{1,7},{2,0},{3,1},{4,2},{5,3},{6,4},{7,5},{8,14},{9,15},{10,... | collective-permute-start | bytes 3145736 | tf_op jit(solution)/shard_map/ppermute | solution.py:204
  50.3 19.7 %all_to_all.30 = bf16[64,2,384]{2,1,0:T(2,128)(2,1)S(1)} all-to-all(bf16[64,2,384]{2,1,0:T(2,128)(2,1)S(1)} %reshape.21), channel_id=1, replica_groups=mesh['sp_0'=8,'sp_1'=8,'tp'=8] {'sp_0','sp_1'}, dimensions={0} | all-to-all | bytes 196608 | tf_op jit(solution)/shard_map/all_to_all | solution.py:330
  70.0 1.2 prefix.1
  71.2 15.2 %all_to_all.31 = bf16[64,2,256]{2,1,0:T(2,128)(2,1)S(1)} all-to-all(bf16[64,2,256]{2,1,0:T(2,128)(2,1)S(1)} %reshape.24), channel_id=1, replica_groups=mesh['sp_0'=8,'sp_1'=8,'tp'=8] {'sp_0','sp_1'}, dimensions={0} | all-to-all | bytes 131072 | tf_op jit(solution)/shard_map/all_to_all | solution.py:115
  86.4 0.6 reshape.25.state_ref
  87.1 3.4 %collective-permute-done.1.refs_2_ = bf16[256,2048]{1,0:T(8,128)(2,1)S(1)} collective-permute-done((bf16[256,2048]{1,0:T(8,128)(2,1)S(1)}, bf16[256,2048]{1,0:T(8,128)(2,1)S(1)}, u32[]{:S(2)}, u32[]{:S(2)}) %collective-permute-start.1) | collective-permute-done | bytes 1048608 | tf_op jit(solution)/shard_map/ppermute | solution.py:204
  90.5 2.1 %gate.1 = bf16[4,128,256]{2,1,0:T(8,128)(2,1)} custom-call(f32[128,128]{1,0:T(8,128)} %copy-done.5, bf16[128,256]{1,0:T(8,128)(2,1)} %reshape.25.state_ref, f32[128,256]{1,0:T(8,128)} %copy-done.2, bf16[128,256]{1,0:T(8,128)(2,1)} %gate_ref.3, f32[1,256]{1,0:T(1,128)} %bitcast.21), custom_call_target="tpu_custom_call" | custom-call | tf_op jit(solution)/shard_map/gate/pallas_call | solution.py:333
  92.6 3.4 %all-to-all-start.3 = ((bf16[4,128,256]{2,1,0:T(8,128)(2,1)}), bf16[4,128,256]{2,1,0:T(8,128)(2,1)S(1)}, u32[]{:S(2)}, u32[]{:S(2)}) async-start(bf16[4,128,256]{2,1,0:T(8,128)(2,1)} %gate.1), calls=%async_computation.3 | async-start | bytes 524288 | tf_op jit(solution)/shard_map/all_to_all | solution.py:248
  96.0 5.5 %all-to-all-done.3.gated_ref = bf16[4,128,256]{2,1,0:T(8,128)(2,1)S(1)} async-done(((bf16[4,128,256]{2,1,0:T(8,128)(2,1)}), bf16[4,128,256]{2,1,0:T(8,128)(2,1)S(1)}, u32[]{:S(2)}, u32[]{:S(2)}) %all-to-all-start.3) | async-done | bytes 262176 | tf_op jit(solution)/shard_map/all_to_all | solution.py:248
  101.5 2.0 %project.1.own_ref = bf16[128,2048]{1,0:T(8,128)(2,1)S(1)} custom-call(s32[1]{0:T(128)} %bitcast.place_ref, bf16[4,128,256]{2,1,0:T(8,128)(2,1)S(1)} %all-to-all-done.3.gated_ref, bf16[256,2048]{1,0:T(8,128)(2,1)S(1)} %copy-done, bf16[256,2048]{1,0:T(8,128)(2,1)S(1)} %collective-permute-done.refs_1_, bf16[256,2048]{1,0:T(8,128)(2,1)S(1)} %collective-permute-done.1.refs_2_, ...), custom_call_target="tpu_custom_call" | custom-call | tf_op jit(solution)/shard_map/project/pallas_call | solution.py:257
  103.5 4.9 %collective-permute-start.3 = (bf16[128,2048]{1,0:T(8,128)(2,1)S(1)}, bf16[128,2048]{1,0:T(8,128)(2,1)S(1)}, u32[]{:S(2)}, u32[]{:S(2)}) collective-permute-start(bf16[128,2048]{1,0:T(8,128)(2,1)S(1)} %project.1.own_ref), channel_id=1, source_target_pairs={{0,1},{1,0},{2,3},{3,2},{4,5},{5,4},{6,7},{7,6},{8,9},{9,8},{10,11... | collective-permute-start | bytes 1572872 | tf_op jit(solution)/shard_map/ppermute | solution.py:265
  108.5 1.5 %collective-permute-done.3.other_ref = bf16[128,2048]{1,0:T(8,128)(2,1)S(1)} collective-permute-done((bf16[128,2048]{1,0:T(8,128)(2,1)S(1)}, bf16[128,2048]{1,0:T(8,128)(2,1)S(1)}, u32[]{:S(2)}, u32[]{:S(2)}) %collective-permute-start.3) | collective-permute-done | bytes 524320 | tf_op jit(solution)/shard_map/ppermute | solution.py:265
  110.0 1.1 middle.1
  111.1 0.0 all-gather.2.cloned.1.call-done.weights_ref
  111.1 5.5 %mix_channels.1 = bf16[128,2048]{1,0:T(8,128)(2,1)} custom-call(bf16[128,2048]{1,0:T(8,128)(2,1)S(1)} %get-tuple-element.26.mid_ref, bf16[2048,2112]{1,0:T(8,128)(2,1)} %all-gather.2.cloned.1.call-done.weights_ref), custom_call_target="tpu_custom_call" | custom-call | flops 1107296256 | bytes 8650752 | tf_op jit(solution)/shard_map/mix_channels/pallas_call | solution.py:396
  116.7 3.5 %all-to-all-start.4 = ((bf16[8,16,2048]{2,1,0:T(8,128)(2,1)}), bf16[8,16,2048]{2,1,0:T(8,128)(2,1)S(1)}, u32[]{:S(2)}, u32[]{:S(2)}) async-start(bf16[8,16,2048]{2,1,0:T(8,128)(2,1)} %bitcast.6), calls=%async_computation.4 | async-start | bytes 1048576 | tf_op jit(solution)/shard_map/all_to_all | solution.py:309
  120.1 9.2 %all-to-all-done.4.arrived_ref = bf16[8,16,2048]{2,1,0:T(8,128)(2,1)S(1)} async-done(((bf16[8,16,2048]{2,1,0:T(8,128)(2,1)}), bf16[8,16,2048]{2,1,0:T(8,128)(2,1)S(1)}, u32[]{:S(2)}, u32[]{:S(2)}) %all-to-all-start.4) | async-done | bytes 524320 | tf_op jit(solution)/shard_map/all_to_all | solution.py:309
  129.4 0.4 settle.1
  129.8 12.7 %all_to_all.32 = bf16[8,16,2048]{2,1,0:T(8,128)(2,1)S(1)} all-to-all(bf16[8,16,2048]{2,1,0:T(8,128)(2,1)S(1)} %settle.1), channel_id=1, replica_groups=mesh['sp_0'=8,'sp_1'=8,'tp'=8] {'tp'}, dimensions={0} | all-to-all | bytes 1048576 | tf_op jit(solution)/shard_map/all_to_all | solution.py:309
  142.5 0.8 copy.18
  (28 shorter events, 0.1 us)
Async XLA Ops:
  8.6 11.1 %copy-start.3 = (bf16[128,256]{1,0:T(8,128)(2,1)S(1)}, bf16[128,256]{1,0:T(8,128)(2,1)}, u32[]{:S(2)}) copy-start(bf16[128,256]{1,0:T(8,128)(2,1)} %values_ref.1) | copy-start | bytes 196612
  8.6 11.1 %copy-start.4 = (f32[128,128]{1,0:T(8,128)S(1)}, f32[128,128]{1,0:T(8,128)}, u32[]{:S(2)}) copy-start(f32[128,128]{1,0:T(8,128)} %decay_ref.1) | copy-start | bytes 196612
  8.6 11.1 %copy-start.6 = (bf16[128,128]{1,0:T(8,128)(2,1)S(1)}, bf16[128,128]{1,0:T(8,128)(2,1)}, u32[]{:S(2)}) copy-start(bf16[128,128]{1,0:T(8,128)(2,1)} %queries_ref.1) | copy-start | bytes 98308
  8.6 11.1 %copy-start.7 = (bf16[128,128]{1,0:T(8,128)(2,1)S(1)}, bf16[128,128]{1,0:T(8,128)(2,1)}, u32[]{:S(2)}) copy-start(bf16[128,128]{1,0:T(8,128)(2,1)} %keys_ref.1) | copy-start | bytes 98308
  8.6 29.7 %all-to-all-start = ((bf16[8,32,2112]{2,1,0:T(8,128)(2,1)}), bf16[8,32,2112]{2,1,0:T(8,128)(2,1)S(1)}, u32[]{:S(2)}, u32[]{:S(2)}) async-start(bf16[8,32,2112]{2,1,0:T(8,128)(2,1)} %copies.1), calls=%async_computation | async-start | bytes 2228224 | tf_op jit(solution)/shard_map/all_to_all | solution.py:162
  19.6 19.7 %copy-start = (bf16[256,2048]{1,0:T(8,128)(2,1)S(1)}, bf16[256,2048]{1,0:T(8,128)(2,1)}, u32[]{:S(2)}) copy-start(bf16[256,2048]{1,0:T(8,128)(2,1)} %refs_0_) | copy-start | bytes 3145732
  19.6 91.5 %all-gather.2.cloned.1.call-start = ((), (), s32[]{:S(2)}) async-start(), calls=%async_computation.6 | async-start | bytes 10027008 | tf_op jit(solution)/shard_map/all_gather | solution.py:174
  21.2 0.6 copy-start.2
  21.8 0.6 copy-start.5
  38.3 1.0 copy-start.12
  39.4 47.7 %collective-permute-start = (bf16[256,2048]{1,0:T(8,128)(2,1)S(1)}, bf16[256,2048]{1,0:T(8,128)(2,1)S(1)}, u32[]{:S(2)}, u32[]{:S(2)}) collective-permute-start(bf16[256,2048]{1,0:T(8,128)(2,1)S(1)} %copy-done), channel_id=1, source_target_pairs={{0,4},{1,5},{2,6},{3,7},{4,0},{5,1},{6,2},{7,3},{8,12},{9,13},{10,... | collective-permute-start | bytes 3145736 | tf_op jit(solution)/shard_map/ppermute | solution.py:204
  43.8 46.7 %collective-permute-start.1 = (bf16[256,2048]{1,0:T(8,128)(2,1)S(1)}, bf16[256,2048]{1,0:T(8,128)(2,1)S(1)}, u32[]{:S(2)}, u32[]{:S(2)}) collective-permute-start(bf16[256,2048]{1,0:T(8,128)(2,1)S(1)} %copy-done), channel_id=1, source_target_pairs={{0,2},{1,3},{2,4},{3,5},{4,6},{5,7},{6,0},{7,1},{8,10},{9,11},{10,... | collective-permute-start | bytes 3145736 | tf_op jit(solution)/shard_map/ppermute | solution.py:204
  46.0 44.5 %collective-permute-start.2 = (bf16[256,2048]{1,0:T(8,128)(2,1)S(1)}, bf16[256,2048]{1,0:T(8,128)(2,1)}, u32[]{:S(2)}, u32[]{:S(2)}) collective-permute-start(bf16[256,2048]{1,0:T(8,128)(2,1)S(1)} %copy-done), channel_id=1, source_target_pairs={{0,6},{1,7},{2,0},{3,1},{4,2},{5,3},{6,4},{7,5},{8,14},{9,15},{10,... | collective-permute-start | bytes 3145736 | tf_op jit(solution)/shard_map/ppermute | solution.py:204
  92.6 8.9 %all-to-all-start.3 = ((bf16[4,128,256]{2,1,0:T(8,128)(2,1)}), bf16[4,128,256]{2,1,0:T(8,128)(2,1)S(1)}, u32[]{:S(2)}, u32[]{:S(2)}) async-start(bf16[4,128,256]{2,1,0:T(8,128)(2,1)} %gate.1), calls=%async_computation.3 | async-start | bytes 524288 | tf_op jit(solution)/shard_map/all_to_all | solution.py:248
  101.5 8.5 %copy-start.1 = (bf16[128,2048]{1,0:T(8,128)(2,1)S(1)}, bf16[128,2048]{1,0:T(8,128)(2,1)}, u32[]{:S(2)}) copy-start(bf16[128,2048]{1,0:T(8,128)(2,1)} %before_ref.1) | copy-start | bytes 1572868
  101.5 8.5 %copy-start.8 = (f32[2048]{0:T(1024)S(1)}, f32[2048]{0:T(1024)}, u32[]{:S(2)}) copy-start(f32[2048]{0:T(1024)} %param.23) | copy-start | bytes 24580
  101.5 8.5 %copy-start.9 = (f32[2048]{0:T(1024)S(1)}, f32[2048]{0:T(1024)}, u32[]{:S(2)}) copy-start(f32[2048]{0:T(1024)} %param.24) | copy-start | bytes 24580
  103.5 6.5 %collective-permute-start.3 = (bf16[128,2048]{1,0:T(8,128)(2,1)S(1)}, bf16[128,2048]{1,0:T(8,128)(2,1)S(1)}, u32[]{:S(2)}, u32[]{:S(2)}) collective-permute-start(bf16[128,2048]{1,0:T(8,128)(2,1)S(1)} %project.1.own_ref), channel_id=1, source_target_pairs={{0,1},{1,0},{2,3},{3,2},{4,5},{5,4},{6,7},{7,6},{8,9},{9,8},{10,11... | collective-permute-start | bytes 1572872 | tf_op jit(solution)/shard_map/ppermute | solution.py:265
  116.6 12.7 %copy-start.10 = (f32[2048]{0:T(1024)S(1)}, f32[2048]{0:T(1024)}, u32[]{:S(2)}) copy-start(f32[2048]{0:T(1024)} %param.28) | copy-start | bytes 24580
  116.6 12.7 %copy-start.11 = (f32[2048]{0:T(1024)S(1)}, f32[2048]{0:T(1024)}, u32[]{:S(2)}) copy-start(f32[2048]{0:T(1024)} %param.29) | copy-start | bytes 24580
  116.7 12.7 %all-to-all-start.4 = ((bf16[8,16,2048]{2,1,0:T(8,128)(2,1)}), bf16[8,16,2048]{2,1,0:T(8,128)(2,1)S(1)}, u32[]{:S(2)}, u32[]{:S(2)}) async-start(bf16[8,16,2048]{2,1,0:T(8,128)(2,1)} %bitcast.6), calls=%async_computation.4 | async-start | bytes 1048576 | tf_op jit(solution)/shard_map/all_to_all | solution.py:309
Sparse Core Ops, SparseCore 0:
  39.5 60.5 all-gather.1

commit v6 on v5

--- a/solution.py
+++ b/solution.py
@@ -116,20 +116,38 @@
     return back.reshape(shape)
 
 
+def orders():
+    rows, cols = (lax.axis_size(axis) for axis in SP)
+    return sorted(range(cols), key=lambda col: abs(col - cols // 2)), list(range(rows))[::-1]
+
+
 def ring_groups(first):
     rows, cols, parts = (lax.axis_size(axis) for axis in (*SP, "tp"))
+    col_order, row_order = orders() if first else (range(cols), range(rows))
     place = lambda row, col, part: (row * cols + col) * parts + part
     along_cols = lambda part: [
-        [place(row, col, part) for col in range(cols)] for row in range(rows)
+        [place(row, col, part) for col in col_order] for row in range(rows)
     ]
     along_rows = lambda part: [
-        [place(row, col, part) for row in range(rows)] for col in range(cols)
+        [place(row, col, part) for row in row_order] for col in range(cols)
     ]
     return [
         group
         for part in range(parts)
         for group in (along_cols if (part % 2 == 0) == first else along_rows)(part)
     ]
+
+
+def chunk_sources():
+    rows, cols = (lax.axis_size(axis) for axis in SP)
+    col_order, row_order = orders()
+    even = [row * cols + col for row in range(rows) for col in col_order]
+    odd = [row * cols + col for col in range(cols) for row in row_order]
+    return even, odd
+
+
+def turned_back(sources):
+    return [sources.index(chunk) for chunk in range(len(sources))]
 
 
 def give_copies(made_ref, out_ref, sems):
@@ -176,17 +194,14 @@
     )
 
 
-def swapped(rows, outer, width):
-    lanes = 128
-    inner = rows.shape[1] // (outer * width)
+def shuffled(rows, sources):
+    lanes, width = 128, rows.shape[1] // len(sources)
     lane = lax.broadcasted_iota(jnp.int32, (rows.shape[0], lanes), 1) // width
-    tiles = []
+    each, tiles = lanes // width, []
     for tile in range(rows.shape[1] // lanes):
         made = None
-        for k in range(lanes // width):
-            new = tile * (lanes // width) + k
-            old = (new % outer) * inner + new // outer
-            source, offset = divmod(old * width, lanes)
+        for k in range(each):
+            source, offset = divmod(sources[tile * each + k] * width, lanes)
             piece = rows[:, source * lanes : (source + 1) * lanes]
             shift = (k * width - offset) % lanes
             if shift:
@@ -221,7 +236,16 @@
 
 
 def middle_kernel(
-    outer, width, place_ref, own_ref, other_ref, before_ref, gain_ref, shift_ref, mid_ref, turned_ref
+    sources,
+    place_ref,
+    own_ref,
+    other_ref,
+    before_ref,
+    gain_ref,
+    shift_ref,
+    turned_ref,
+    kept_ref,
+    mid_ref,
 ):
     mixed = own_ref[...].astype(jnp.float32) + other_ref[...].astype(jnp.float32)
     inputs = ALPHA * before_ref[...].astype(jnp.float32) + mixed
@@ -229,21 +253,18 @@
     spread = jnp.mean(center * center, axis=-1, keepdims=True)
     rows = center * lax.rsqrt(spread + LN_EPS) * gain_ref[...] + shift_ref[...]
     rows = rows.astype(jnp.bfloat16)
-    odd = lax.rem(place_ref[0], 2) == 1
     mid_ref[...] = rows
-
-    @pl.when(jnp.logical_not(odd))
-    def _():
-        turned_ref[...] = rows
-
-    @pl.when(odd)
-    def _():
-        turned_ref[...] = swapped(rows.astype(jnp.float32), outer, width).astype(jnp.bfloat16)
-
-
-def middle_rows(copies, blocks, resid, gain, shift):
+    count = kept_ref.shape[0]
+    kept_ref[...] = mid_ref[pl.ds(pl.multiple_of(place_ref[0] * count, count), count)]
+    for core in range(2):
+
+        @pl.when(lax.rem(place_ref[0], 2) == core)
+        def _():
+            turned_ref[...] = shuffled(rows.astype(jnp.float32), sources[core]).astype(jnp.bfloat16)
+
+
+def middle_rows(place, copies, blocks, resid, gain, shift):
     parts = lax.axis_size("tp")
-    place = lax.axis_index("tp")[None].astype(jnp.int32)
     smem, vmem = (pl.BlockSpec(memory_space=space) for space in (pltpu.SMEM, pltpu.VMEM))
     everyone = lax.all_to_all(
         copies,
@@ -263,26 +284,29 @@
         name="project",
     )(place, everyone, *blocks)
     other = lax.ppermute(own, "tp", [(part, part ^ 1) for part in range(parts)])
-    outer = lax.axis_size(SP[0])
     return pl.pallas_call(
-        functools.partial(middle_kernel, outer, resid.shape[1] // (outer * lax.axis_size(SP[1]))),
-        out_shape=(rows, rows),
+        functools.partial(middle_kernel, chunk_sources()),
+        out_shape=(
+            rows,
+            jax.ShapeDtypeStruct((resid.shape[0] // parts, resid.shape[1]), jnp.bfloat16),
+        ),
         in_specs=[smem] + [vmem] * 5,
         out_specs=(vmem, vmem),
+        scratch_shapes=[pltpu.VMEM(resid.shape, jnp.bfloat16)],
         compiler_params=pltpu.CompilerParams(vmem_limit_bytes=16 << 20),
         name="middle",
     )(place, own, other, resid, gain[None], shift[None])
 
 
 def settle_kernel(
-    scale, outer, width, arrived_ref, before_ref, gain_ref, shift_ref, out_ref
+    scale, sources, arrived_ref, before_ref, gain_ref, shift_ref, out_ref
 ):
     parts = arrived_ref.shape[0]
     even, odd = (
         sum(arrived_ref[k].astype(jnp.float32) for k in range(start, parts, 2))
         for start in range(2)
     )
-    odd = swapped(odd, outer, width)
+    even, odd = (shuffled(part, turned_back(own)) for part, own in zip((even, odd), sources))
     inputs = ALPHA * before_ref[...].astype(jnp.float32) + scale * (even + odd)
     center = inputs - jnp.mean(inputs, axis=-1, keepdims=True)
     spread = jnp.mean(center * center, axis=-1, keepdims=True)
@@ -293,10 +317,8 @@
 
 
 def settle(arrived, before, gain, shift, scale):
-    outer = lax.axis_size(SP[0])
-    width = before.shape[1] // (outer * lax.axis_size(SP[1]))
     return pl.pallas_call(
-        functools.partial(settle_kernel, scale, outer, width),
+        functools.partial(settle_kernel, scale, chunk_sources()),
         out_shape=jax.ShapeDtypeStruct(arrived.shape, jnp.bfloat16),
         compiler_params=pltpu.CompilerParams(vmem_limit_bytes=8 << 20),
         name="settle",
@@ -309,7 +331,7 @@
     return lax.all_to_all(blocks, axis, split_axis=0, concat_axis=0, tiled=True)
 
 
-def gate_kernel(readers_ref, state_ref, local_ref, gate_ref, gain_ref, out_ref, made_ref, sems):
+def gate_kernel(readers_ref, state_ref, local_ref, gate_ref, gain_ref, out_ref):
     readout = local_ref[...] + jnp.dot(
         readers_ref[...],
         state_ref[...].astype(jnp.float32),
@@ -318,14 +340,15 @@
     )
     square = jnp.mean(readout * readout, axis=-1, keepdims=True)
     normed = readout * lax.rsqrt(square + RMS_EPS) * gain_ref[...]
-    made_ref[...] = (normed * jax.nn.silu(gate_ref[...].astype(jnp.float32))).astype(jnp.bfloat16)
-    give_copies(made_ref, out_ref, sems)
-
-
-def mix_tokens(queries, keys, values, decay_pre, out_gate, head_gain, nearby, blocks):
+    gated = (normed * jax.nn.silu(gate_ref[...].astype(jnp.float32))).astype(jnp.bfloat16)
+    for k in range(out_ref.shape[0]):
+        out_ref[k] = gated
+
+
+def mix_tokens(queries, keys, values, decay_pre, out_gate, head_gain, nearby, place, blocks):
     packed, readers, local_read = local_states(queries, keys, values, decay_pre)
     packed = packed.reshape(lax.axis_size(SP), -1, HV + 128)
-    packed, nearby = lax.optimization_barrier((packed, nearby))
+    packed, nearby, place = lax.optimization_barrier((packed, nearby, place))
     weights = gathered_weights(nearby)
     arrived = lax.all_to_all(packed, SP, split_axis=0, concat_axis=0, tiled=True)
     incoming = incoming_state(arrived, (HK, HV))
@@ -333,18 +356,13 @@
     copies = pl.pallas_call(
         gate_kernel,
         out_shape=jax.ShapeDtypeStruct((lax.axis_size("tp") // 2, *values.shape), jnp.bfloat16),
-        out_specs=pl.BlockSpec(memory_space=pltpu.HBM),
-        scratch_shapes=[
-            pltpu.VMEM(values.shape, jnp.bfloat16),
-            pltpu.SemaphoreType.DMA((lax.axis_size("tp") // 2,)),
-        ],
-        compiler_params=pltpu.CompilerParams(vmem_limit_bytes=60 << 20),
+        compiler_params=pltpu.CompilerParams(vmem_limit_bytes=8 << 20),
         name="gate",
     )(readers, incoming, local_read, out_gate, head_gain[None])
-    return copies, blocks, weights
-
-
-def mixer_kernel(units, depth, mid_ref, weights_ref, out_ref, held, total, made, sems, out_sems):
+    return copies, place, blocks, weights
+
+
+def mixer_kernel(units, depth, mid_ref, weights_ref, out_ref, held, total, sems):
     steps = mid_ref.shape[1] // depth
     wide = 2 * units
 
@@ -353,12 +371,6 @@
         columns = pl.ds(0, wide) if part == 0 else pl.ds(wide, units)
         return pltpu.make_async_copy(
             weights_ref.at[rows, columns], held.at[rows, columns], sems.at[part, step]
-        )
-
-    def give(step):
-        columns = pl.ds(step * depth, depth)
-        return pltpu.make_async_copy(
-            made.at[:, columns], out_ref.at[:, columns], out_sems.at[step]
         )
 
     for part in range(2):
@@ -379,15 +391,12 @@
     for step in range(steps):
         fetch(step, 1).wait()
         rows = pl.ds(step * depth, depth)
-        made[:, rows] = lax.dot_general(
+        out_ref[:, rows] = lax.dot_general(
             hidden,
             held[rows, pl.ds(wide, units)],
             (((1,), (1,)), ((), ())),
             preferred_element_type=jnp.float32,
         ).astype(jnp.bfloat16)
-        give(step).start()
-    for step in range(steps):
-        give(step).wait()
 
 
 def mix_channels(mid_rows, weights):
@@ -400,13 +409,11 @@
             pl.BlockSpec(memory_space=pltpu.VMEM),
             pl.BlockSpec(memory_space=pltpu.HBM),
         ],
-        out_specs=pl.BlockSpec(memory_space=pltpu.HBM),
+        out_specs=pl.BlockSpec(memory_space=pltpu.VMEM),
         scratch_shapes=[
             pltpu.VMEM(weights.shape, jnp.bfloat16),
             pltpu.VMEM((mid_rows.shape[0], 2 * units), jnp.float32),
-            pltpu.VMEM(mid_rows.shape, jnp.bfloat16),
             pltpu.SemaphoreType.DMA((2, steps)),
-            pltpu.SemaphoreType.DMA((steps,)),
         ],
         compiler_params=pltpu.CompilerParams(vmem_limit_bytes=52 << 20),
         cost_estimate=pl.CostEstimate(
@@ -433,15 +440,14 @@
     out_gain,
     out_shift,
 ):
-    own_count = queries.shape[0] // lax.axis_size("tp")
+    place = lax.axis_index("tp")[None].astype(jnp.int32)
     nearby = nearby_weights(gate_in, up_in, down_out)
     blocks = collected_projection(out_proj)
-    gated_copies, blocks, weights = mix_tokens(
-        queries, keys, values, decay_pre, out_gate, head_gain, nearby, blocks
-    )
-    mid, mid_turned = middle_rows(gated_copies, blocks, resid, mix_gain, mix_shift)
+    gated_copies, place, blocks, weights = mix_tokens(
+        queries, keys, values, decay_pre, out_gate, head_gain, nearby, place, blocks
+    )
+    mid_turned, own_mid = middle_rows(place, gated_copies, blocks, resid, mix_gain, mix_shift)
     ffn = sent(mix_channels(mid_turned, weights), "tp")
-    own_mid = lax.dynamic_slice_in_dim(mid, lax.axis_index("tp") * own_count, own_count, 0)
     finished = settle(ffn, own_mid, out_gain, out_shift, 0.5)
     return sent(finished, "tp").reshape(resid.shape)
 

time: 151 us -> 148 us (0.980)
  blocking collectives: 47.6 us -> 74 us
  waiting for transfers between devices: 35.6 us -> 12.2 us
  starting transfers between devices: 33.8 us -> 31 us
  Pallas kernels: 15.7 us -> 13.4 us
    all_to_all x2 -> x0, waiting for transfers between devices: 14.7 us -> none  [the longest x1 9.23 us: sent(): return lax.all_to_all(blocks, axis, split_axis=0, concat_axis=0, tiled=True)]
    all_to_all x1 -> x2, blocking collectives: 12.7 us -> 24.9 us  [sent(): return lax.all_to_all(blocks, axis, split_axis=0, concat_axis=0, tiled=True)]
    all_to_all x0 -> x1, blocking collectives: none -> 7.97 us  [middle_rows(): lax.all_to_all(copies, 'tp', split_axis=0, concat_axis=0, tiled=True, axi...]
    all_to_all x2 -> x0, starting transfers between devices: 6.88 us -> none  [the longest x1 3.46 us: sent(): return lax.all_to_all(blocks, axis, split_axis=0, concat_axis=0, tiled=True)]
    all_to_all x1, blocking collectives: 19.7 us -> 25.4 us  [mix_tokens(): lax.all_to_all(packed, SP, split_axis=0, concat_axis=0, tiled=True)]
    all_to_all x1, waiting for transfers between devices: 15.8 us -> 10.7 us  [nearby_weights(): lax.all_to_all(copies, (*SP, 'tp'), split_axis=0, concat_axis=0, tiled=Tr...]
    ppermute x3, waiting for transfers between devices: 3.44 us -> 0.01 us  [collected_projection(): blocks.append(lax.ppermute(out_proj, 'tp', path))]
    all_to_all x1, starting transfers between devices: 11 us -> 13.2 us  [nearby_weights(): lax.all_to_all(copies, (*SP, 'tp'), split_axis=0, concat_axis=0, tiled=Tr...]
  transfers between devices with their start and end apart: 8 -> 6, of which waited for: 5 -> 2; matrix products, arithmetic and copies ran while one was open for 0% -> 1% of each run, Pallas kernels for 5% -> 4%
where the time goes in v6:
time: 148 us; the launch traced here: 147 us
  blocking collectives  74 us (50%)
  starting transfers between devices  31 us (21%)
  between operations  13.7 us (9%)
  Pallas kernels  13.4 us (9%)
  waiting for transfers between devices  12.2 us (8%)
  local copies, waits for them, and re-layouts  2.79 us (2%)
    all_to_all x1, blocking collectives, mix_tokens(): lax.all_to_all(packed, SP, split_axis=0, concat_axis=0, tiled=True)  25.4 us
    all_to_all x2, blocking collectives, sent(): return lax.all_to_all(blocks, axis, split_axis=0, concat_axis=0, tiled=True)  24.9 us
    all_to_all x1, blocking collectives, incoming_state(): back = lax.all_to_all(entering, SP, split_axis=0, concat_axis=0, tiled=True)  15.8 us
    all_to_all x1, starting transfers between devices, nearby_weights(): lax.all_to_all(copies, (*SP, 'tp'), split_axis=0, concat_axis=0, tiled=Tr...  13.2 us
    ppermute x3, starting transfers between devices, collected_projection(): blocks.append(lax.ppermute(out_proj, 'tp', path))  11.1 us
    all_to_all x1, waiting for transfers between devices, nearby_weights(): lax.all_to_all(copies, (*SP, 'tp'), split_axis=0, concat_axis=0, tiled=Tr...  10.7 us
    all_to_all x1, blocking collectives, middle_rows(): lax.all_to_all(copies, 'tp', split_axis=0, concat_axis=0, tiled=True, axi...  7.97 us
    ppermute x1, starting transfers between devices, middle_rows(): other = lax.ppermute(own, 'tp', [(part, part ^ 1) for part in range(parts)])  6.6 us
  transfers between devices with their start and end apart: 6, of which 2 were waited for; matrix products, arithmetic and copies ran while one was open for 1% of the time, Pallas kernels for 4%

profile of v6, /device:TPU:1, one launch (start us, length us, event | category | flops | bytes accessed | tf_op | source)
XLA Modules:
  0.0 147.0 jit_solution(15315409421325083570)
XLA Ops:
  6.5 2.0 %copies.1 = bf16[8,32,2112]{2,1,0:T(8,128)(2,1)} custom-call(bf16[32,704]{1,0:T(8,128)(2,1)} %gate_ref.2, bf16[32,704]{1,0:T(8,128)(2,1)} %up_ref.1, bf16[32,704]{1,0:T(8,128)(2,1)} %bitcast.22), custom_call_target="tpu_custom_call" | custom-call | tf_op jit(solution)/shard_map/copies/pallas_call | solution.py:170
  8.6 0.0 copy-start.2
  8.6 0.0 copy-start.3
  8.6 0.0 copy-start.5
  8.6 0.0 copy-start.6
  8.6 13.2 %all-to-all-start = ((bf16[8,32,2112]{2,1,0:T(8,128)(2,1)}), bf16[8,32,2112]{2,1,0:T(8,128)(2,1)S(1)}, u32[]{:S(2)}, u32[]{:S(2)}) async-start(bf16[8,32,2112]{2,1,0:T(8,128)(2,1)} %copies.1), calls=%async_computation | async-start | bytes 2228224 | tf_op jit(solution)/shard_map/all_to_all | solution.py:180
  21.9 1.5 %local.1 = (bf16[128,384]{1,0:T(8,128)(2,1)S(1)}, f32[128,128]{1,0:T(8,128)S(1)}, f32[128,256]{1,0:T(8,128)S(1)}) custom-call(bf16[128,128]{1,0:T(8,128)(2,1)S(1)} %copy-done.5, bf16[128,128]{1,0:T(8,128)(2,1)S(1)} %copy-done.6, bf16[128,256]{1,0:T(8,128)(2,1)S(1)} %copy-done.2, f32[128,128]{1,0:T(8,128)S(1)} %copy-done.3), custom_call_target="tpu_custom_call" | custom-call | tf_op jit(solution)/shard_map/local/pallas_call | solution.py:62
  23.4 0.0 copy-start.4
  23.4 0.0 copy-start.11
  23.4 10.7 %all-to-all-done = bf16[8,32,2112]{2,1,0:T(8,128)(2,1)S(1)} async-done(((bf16[8,32,2112]{2,1,0:T(8,128)(2,1)}), bf16[8,32,2112]{2,1,0:T(8,128)(2,1)S(1)}, u32[]{:S(2)}, u32[]{:S(2)}) %all-to-all-start) | async-done | bytes 1081376 | tf_op jit(solution)/shard_map/all_to_all | solution.py:180
  34.1 1.0 copy-done.12
  35.1 0.0 all-gather.2.cloned.1.call-update
  35.1 4.7 %collective-permute-start = (bf16[256,2048]{1,0:T(8,128)(2,1)S(1)}, bf16[256,2048]{1,0:T(8,128)(2,1)S(1)}, u32[]{:S(2)}, u32[]{:S(2)}) collective-permute-start(bf16[256,2048]{1,0:T(8,128)(2,1)S(1)} %copy-done), channel_id=1, source_target_pairs={{0,4},{1,5},{2,6},{3,7},{4,0},{5,1},{6,2},{7,3},{8,12},{9,13},{10,... | collective-permute-start | bytes 3145736 | tf_op jit(solution)/shard_map/ppermute | solution.py:219
  39.8 2.2 %collective-permute-start.1 = (bf16[256,2048]{1,0:T(8,128)(2,1)S(1)}, bf16[256,2048]{1,0:T(8,128)(2,1)S(1)}, u32[]{:S(2)}, u32[]{:S(2)}) collective-permute-start(bf16[256,2048]{1,0:T(8,128)(2,1)S(1)} %copy-done), channel_id=1, source_target_pairs={{0,2},{1,3},{2,4},{3,5},{4,6},{5,7},{6,0},{7,1},{8,10},{9,11},{10,... | collective-permute-start | bytes 3145736 | tf_op jit(solution)/shard_map/ppermute | solution.py:219
  42.0 4.3 %collective-permute-start.2 = (bf16[256,2048]{1,0:T(8,128)(2,1)S(1)}, bf16[256,2048]{1,0:T(8,128)(2,1)}, u32[]{:S(2)}, u32[]{:S(2)}) collective-permute-start(bf16[256,2048]{1,0:T(8,128)(2,1)S(1)} %copy-done), channel_id=1, source_target_pairs={{0,6},{1,7},{2,0},{3,1},{4,2},{5,3},{6,4},{7,5},{8,14},{9,15},{10,... | collective-permute-start | bytes 3145736 | tf_op jit(solution)/shard_map/ppermute | solution.py:219
  46.3 25.4 %all_to_all.30 = bf16[64,2,384]{2,1,0:T(2,128)(2,1)S(1)} all-to-all(bf16[64,2,384]{2,1,0:T(2,128)(2,1)S(1)} %reshape.21), channel_id=1, replica_groups=mesh['sp_0'=8,'sp_1'=8,'tp'=8] {'sp_0','sp_1'}, dimensions={0} | all-to-all | bytes 196608 | tf_op jit(solution)/shard_map/all_to_all | solution.py:353
  71.7 1.2 prefix.1
  72.9 15.8 %all_to_all.31 = bf16[64,2,256]{2,1,0:T(2,128)(2,1)} all-to-all(bf16[64,2,256]{2,1,0:T(2,128)(2,1)S(1)} %reshape.24), channel_id=1, replica_groups=mesh['sp_0'=8,'sp_1'=8,'tp'=8] {'sp_0','sp_1'}, dimensions={0} | all-to-all | bytes 131072 | tf_op jit(solution)/shard_map/all_to_all | solution.py:115
  88.6 0.9 reshape.25.state_ref
  89.6 0.3 gate.1
  89.9 8.0 %all_to_all.32.gated_ref = bf16[4,128,256]{2,1,0:T(8,128)(2,1)S(1)} all-to-all(bf16[4,128,256]{2,1,0:T(8,128)(2,1)S(1)} %gate.1), channel_id=1, replica_groups={{0,2,4,6},{1,3,5,7},{8,10,12,14},{9,11,13,15},{16,18,20,22},{17,19,21,2..., dimensions={0} | all-to-all | bytes 524288 | tf_op jit(solution)/shard_map/all_to_all | solution.py:269
  97.9 2.0 %project.1.own_ref = bf16[128,2048]{1,0:T(8,128)(2,1)S(1)} custom-call(s32[1]{0:T(128)} %bitcast.2.place_ref, bf16[4,128,256]{2,1,0:T(8,128)(2,1)S(1)} %all_to_all.32.gated_ref, bf16[256,2048]{1,0:T(8,128)(2,1)S(1)} %copy-done, bf16[256,2048]{1,0:T(8,128)(2,1)S(1)} %collective-permute-done.refs_1_, bf16[256,2048]{1,0:T(8,128)(2,1)S(1)} %collective-permute-done.1.refs_2_, ...), custom_call_target="tpu_custom_call" | custom-call | tf_op jit(solution)/shard_map/project/pallas_call | solution.py:278
  99.9 6.6 %collective-permute-start.3 = (bf16[128,2048]{1,0:T(8,128)(2,1)S(1)}, bf16[128,2048]{1,0:T(8,128)(2,1)S(1)}, u32[]{:S(2)}, u32[]{:S(2)}) collective-permute-start(bf16[128,2048]{1,0:T(8,128)(2,1)S(1)} %project.1.own_ref), channel_id=1, source_target_pairs={{0,1},{1,0},{2,3},{3,2},{4,5},{5,4},{6,7},{7,6},{8,9},{9,8},{10,11... | collective-permute-start | bytes 1572872 | tf_op jit(solution)/shard_map/ppermute | solution.py:286
  106.5 1.5 %collective-permute-done.3.other_ref = bf16[128,2048]{1,0:T(8,128)(2,1)S(1)} collective-permute-done((bf16[128,2048]{1,0:T(8,128)(2,1)S(1)}, bf16[128,2048]{1,0:T(8,128)(2,1)S(1)}, u32[]{:S(2)}, u32[]{:S(2)}) %collective-permute-start.3) | collective-permute-done | bytes 524320 | tf_op jit(solution)/shard_map/ppermute | solution.py:286
  108.0 1.1 middle.1
  109.1 0.0 all-gather.2.cloned.1.call-done.weights_ref
  109.2 0.0 copy-start.9
  109.2 4.8 %mix_channels.1 = bf16[128,2048]{1,0:T(8,128)(2,1)S(1)} custom-call(bf16[128,2048]{1,0:T(8,128)(2,1)S(1)} %get-tuple-element.28.mid_ref, bf16[2048,2112]{1,0:T(8,128)(2,1)} %all-gather.2.cloned.1.call-done.weights_ref), custom_call_target="tpu_custom_call" | custom-call | flops 1107296256 | bytes 8650752 | tf_op jit(solution)/shard_map/mix_channels/pallas_call | solution.py:405
  114.0 12.1 %all_to_all.33.arrived_ref = bf16[8,16,2048]{2,1,0:T(8,128)(2,1)S(1)} all-to-all(bf16[8,16,2048]{2,1,0:T(8,128)(2,1)S(1)} %bitcast.12), channel_id=1, replica_groups=mesh['sp_0'=8,'sp_1'=8,'tp'=8] {'tp'}, dimensions={0} | all-to-all | bytes 1048576 | tf_op jit(solution)/shard_map/all_to_all | solution.py:331
  126.1 0.5 settle.1
  126.6 12.8 %all_to_all.34 = bf16[8,16,2048]{2,1,0:T(8,128)(2,1)S(1)} all-to-all(bf16[8,16,2048]{2,1,0:T(8,128)(2,1)S(1)} %settle.1), channel_id=1, replica_groups=mesh['sp_0'=8,'sp_1'=8,'tp'=8] {'tp'}, dimensions={0} | all-to-all | bytes 1048576 | tf_op jit(solution)/shard_map/all_to_all | solution.py:331
  139.3 0.8 copy.18
  (25 shorter events, 0.1 us)
Async XLA Ops:
  8.6 13.3 %copy-start.2 = (bf16[128,256]{1,0:T(8,128)(2,1)S(1)}, bf16[128,256]{1,0:T(8,128)(2,1)}, u32[]{:S(2)}) copy-start(bf16[128,256]{1,0:T(8,128)(2,1)} %values_ref.1) | copy-start | bytes 196612
  8.6 13.3 %copy-start.3 = (f32[128,128]{1,0:T(8,128)S(1)}, f32[128,128]{1,0:T(8,128)}, u32[]{:S(2)}) copy-start(f32[128,128]{1,0:T(8,128)} %decay_ref.1) | copy-start | bytes 196612
  8.6 13.3 %copy-start.5 = (bf16[128,128]{1,0:T(8,128)(2,1)S(1)}, bf16[128,128]{1,0:T(8,128)(2,1)}, u32[]{:S(2)}) copy-start(bf16[128,128]{1,0:T(8,128)(2,1)} %queries_ref.1) | copy-start | bytes 98308
  8.6 13.3 %copy-start.6 = (bf16[128,128]{1,0:T(8,128)(2,1)S(1)}, bf16[128,128]{1,0:T(8,128)(2,1)}, u32[]{:S(2)}) copy-start(bf16[128,128]{1,0:T(8,128)(2,1)} %keys_ref.1) | copy-start | bytes 98308
  8.6 25.5 %all-to-all-start = ((bf16[8,32,2112]{2,1,0:T(8,128)(2,1)}), bf16[8,32,2112]{2,1,0:T(8,128)(2,1)S(1)}, u32[]{:S(2)}, u32[]{:S(2)}) async-start(bf16[8,32,2112]{2,1,0:T(8,128)(2,1)} %copies.1), calls=%async_computation | async-start | bytes 2228224 | tf_op jit(solution)/shard_map/all_to_all | solution.py:180
  21.8 13.3 %copy-start = (bf16[256,2048]{1,0:T(8,128)(2,1)S(1)}, bf16[256,2048]{1,0:T(8,128)(2,1)}, u32[]{:S(2)}) copy-start(bf16[256,2048]{1,0:T(8,128)(2,1)} %refs_0_) | copy-start | bytes 3145732
  21.8 87.3 %all-gather.2.cloned.1.call-start = ((), (), s32[]{:S(2)}) async-start(), calls=%async_computation.6 | async-start | bytes 10027008 | tf_op jit(solution)/shard_map/all_gather | solution.py:192
  23.4 66.2 %copy-start.4 = (bf16[128,256]{1,0:T(8,128)(2,1)S(1)}, bf16[128,256]{1,0:T(8,128)(2,1)}, u32[]{:S(2)}) copy-start(bf16[128,256]{1,0:T(8,128)(2,1)} %gate_ref.3) | copy-start | bytes 196612
  23.4 66.2 %copy-start.11 = (f32[256]{0:T(256)S(1)}, f32[256]{0:T(256)}, u32[]{:S(2)}) copy-start(f32[256]{0:T(256)} %param.21) | copy-start | bytes 3076
  34.1 1.0 copy-start.12
  35.1 54.4 %collective-permute-start = (bf16[256,2048]{1,0:T(8,128)(2,1)S(1)}, bf16[256,2048]{1,0:T(8,128)(2,1)S(1)}, u32[]{:S(2)}, u32[]{:S(2)}) collective-permute-start(bf16[256,2048]{1,0:T(8,128)(2,1)S(1)} %copy-done), channel_id=1, source_target_pairs={{0,4},{1,5},{2,6},{3,7},{4,0},{5,1},{6,2},{7,3},{8,12},{9,13},{10,... | collective-permute-start | bytes 3145736 | tf_op jit(solution)/shard_map/ppermute | solution.py:219
  39.8 49.7 %collective-permute-start.1 = (bf16[256,2048]{1,0:T(8,128)(2,1)S(1)}, bf16[256,2048]{1,0:T(8,128)(2,1)S(1)}, u32[]{:S(2)}, u32[]{:S(2)}) collective-permute-start(bf16[256,2048]{1,0:T(8,128)(2,1)S(1)} %copy-done), channel_id=1, source_target_pairs={{0,2},{1,3},{2,4},{3,5},{4,6},{5,7},{6,0},{7,1},{8,10},{9,11},{10,... | collective-permute-start | bytes 3145736 | tf_op jit(solution)/shard_map/ppermute | solution.py:219
  42.0 47.5 %collective-permute-start.2 = (bf16[256,2048]{1,0:T(8,128)(2,1)S(1)}, bf16[256,2048]{1,0:T(8,128)(2,1)}, u32[]{:S(2)}, u32[]{:S(2)}) collective-permute-start(bf16[256,2048]{1,0:T(8,128)(2,1)S(1)} %copy-done), channel_id=1, source_target_pairs={{0,6},{1,7},{2,0},{3,1},{4,2},{5,3},{6,4},{7,5},{8,14},{9,15},{10,... | collective-permute-start | bytes 3145736 | tf_op jit(solution)/shard_map/ppermute | solution.py:219
  97.9 10.2 %copy-start.1 = (bf16[128,2048]{1,0:T(8,128)(2,1)S(1)}, bf16[128,2048]{1,0:T(8,128)(2,1)}, u32[]{:S(2)}) copy-start(bf16[128,2048]{1,0:T(8,128)(2,1)} %before_ref.1) | copy-start | bytes 1572868
  97.9 10.2 %copy-start.7 = (f32[2048]{0:T(1024)S(1)}, f32[2048]{0:T(1024)}, u32[]{:S(2)}) copy-start(f32[2048]{0:T(1024)} %param.23) | copy-start | bytes 24580
  97.9 10.2 %copy-start.8 = (f32[2048]{0:T(1024)S(1)}, f32[2048]{0:T(1024)}, u32[]{:S(2)}) copy-start(f32[2048]{0:T(1024)} %param.24) | copy-start | bytes 24580
  99.9 8.1 %collective-permute-start.3 = (bf16[128,2048]{1,0:T(8,128)(2,1)S(1)}, bf16[128,2048]{1,0:T(8,128)(2,1)S(1)}, u32[]{:S(2)}, u32[]{:S(2)}) collective-permute-start(bf16[128,2048]{1,0:T(8,128)(2,1)S(1)} %project.1.own_ref), channel_id=1, source_target_pairs={{0,1},{1,0},{2,3},{3,2},{4,5},{5,4},{6,7},{7,6},{8,9},{9,8},{10,11... | collective-permute-start | bytes 1572872 | tf_op jit(solution)/shard_map/ppermute | solution.py:286
  109.2 16.9 %copy-start.9 = (f32[2048]{0:T(1024)S(1)}, f32[2048]{0:T(1024)}, u32[]{:S(2)}) copy-start(f32[2048]{0:T(1024)} %param.28) | copy-start | bytes 24580
  109.2 16.9 %copy-start.10 = (f32[2048]{0:T(1024)S(1)}, f32[2048]{0:T(1024)}, u32[]{:S(2)}) copy-start(f32[2048]{0:T(1024)} %param.29) | copy-start | bytes 24580
Sparse Core Ops, SparseCore 0:
  35.2 64.8 all-gather.1

commit v7 on v6

--- a/solution.py
+++ b/solution.py
@@ -116,20 +116,14 @@
     return back.reshape(shape)
 
 
-def orders():
-    rows, cols = (lax.axis_size(axis) for axis in SP)
-    return sorted(range(cols), key=lambda col: abs(col - cols // 2)), list(range(rows))[::-1]
-
-
 def ring_groups(first):
     rows, cols, parts = (lax.axis_size(axis) for axis in (*SP, "tp"))
-    col_order, row_order = orders() if first else (range(cols), range(rows))
     place = lambda row, col, part: (row * cols + col) * parts + part
     along_cols = lambda part: [
-        [place(row, col, part) for col in col_order] for row in range(rows)
+        [place(row, col, part) for col in range(cols)] for row in range(rows)
     ]
     along_rows = lambda part: [
-        [place(row, col, part) for row in row_order] for col in range(cols)
+        [place(row, col, part) for row in range(rows)] for col in range(cols)
     ]
     return [
         group
@@ -140,10 +134,9 @@
 
 def chunk_sources():
     rows, cols = (lax.axis_size(axis) for axis in SP)
-    col_order, row_order = orders()
-    even = [row * cols + col for row in range(rows) for col in col_order]
-    odd = [row * cols + col for col in range(cols) for row in row_order]
-    return even, odd
+    even = list(range(rows * cols))
+    odd = [row * cols + col for col in range(cols) for row in range(rows)]
+    return [[2 * chunk + half for half in range(2) for chunk in own] for own in (even, odd)]
 
 
 def turned_back(sources):
@@ -161,7 +154,10 @@
 
 
 def copies_kernel(gate_ref, up_ref, down_ref, out_ref, made_ref, sems):
-    made_ref[...] = jnp.concatenate([gate_ref[...], up_ref[...], down_ref[...]], axis=1)
+    half = made_ref.shape[0]
+    pair = lambda ref: (ref[:half], ref[half:])
+    gate, up, down = pair(gate_ref), pair(up_ref), pair(down_ref)
+    made_ref[...] = jnp.concatenate([gate[0], up[0], gate[1], up[1], *down], axis=1)
     give_copies(made_ref, out_ref, sems)
 
 
@@ -169,10 +165,12 @@
     rows, units = gate_in.shape
     copies = pl.pallas_call(
         copies_kernel,
-        out_shape=jax.ShapeDtypeStruct((lax.axis_size(SP[0]), rows, 3 * units), jnp.bfloat16),
+        out_shape=jax.ShapeDtypeStruct(
+            (lax.axis_size(SP[0]), rows // 2, 6 * units), jnp.bfloat16
+        ),
         out_specs=pl.BlockSpec(memory_space=pltpu.HBM),
         scratch_shapes=[
-            pltpu.VMEM((rows, 3 * units), jnp.bfloat16),
+            pltpu.VMEM((rows // 2, 6 * units), jnp.bfloat16),
             pltpu.SemaphoreType.DMA((lax.axis_size(SP[0]),)),
         ],
         name="copies",
@@ -185,7 +183,7 @@
         tiled=True,
         axis_index_groups=ring_groups(True),
     )
-    return arrived.reshape(-1, 3 * units)
+    return arrived.reshape(-1, 6 * units)
 
 
 def gathered_weights(nearby):
@@ -362,13 +360,13 @@
     return copies, place, blocks, weights
 
 
-def mixer_kernel(units, depth, mid_ref, weights_ref, out_ref, held, total, sems):
-    steps = mid_ref.shape[1] // depth
-    wide = 2 * units
+def mixer_kernel(units, depth, mid_ref, weights_ref, out_ref, held, total, pair, sems):
+    tokens, half = mid_ref.shape[0], weights_ref.shape[0]
+    steps, wide = half // depth, 2 * units
 
     def fetch(step, part):
         rows = pl.ds(step * depth, depth)
-        columns = pl.ds(0, wide) if part == 0 else pl.ds(wide, units)
+        columns = pl.ds(0, 2 * wide) if part == 0 else pl.ds(2 * wide, wide)
         return pltpu.make_async_copy(
             weights_ref.at[rows, columns], held.at[rows, columns], sems.at[part, step]
         )
@@ -376,31 +374,37 @@
     for part in range(2):
         for step in range(steps):
             fetch(step, part).start()
+    pair[...] = jnp.zeros_like(pair)
     for step in range(steps):
         fetch(step, 0).wait()
-        for at in range(step * depth, (step + 1) * depth, 256):
-            rows = pl.ds(at, 256)
+        rows = pl.ds(step * depth, depth)
+        for side in range(2):
             product = jnp.dot(
-                mid_ref[:, rows], held[rows, pl.ds(0, wide)], preferred_element_type=jnp.float32
+                mid_ref[:, pl.ds(side * half + step * depth, depth)],
+                held[rows, pl.ds(side * wide, wide)],
+                preferred_element_type=jnp.float32,
             )
-            if at == 0:
+            if step == 0 and side == 0:
                 total[...] = product
             else:
                 total[...] += product
     hidden = (jax.nn.silu(total[:, :units]) * total[:, units:]).astype(jnp.bfloat16)
+    pair[:tokens, :units] = hidden
+    pair[tokens:, units:] = hidden
     for step in range(steps):
         fetch(step, 1).wait()
-        rows = pl.ds(step * depth, depth)
-        out_ref[:, rows] = lax.dot_general(
-            hidden,
-            held[rows, pl.ds(wide, units)],
+        both = lax.dot_general(
+            pair[...],
+            held[pl.ds(step * depth, depth), pl.ds(2 * wide, wide)],
             (((1,), (1,)), ((), ())),
             preferred_element_type=jnp.float32,
         ).astype(jnp.bfloat16)
+        out_ref[:, pl.ds(step * depth, depth)] = both[:tokens]
+        out_ref[:, pl.ds(half + step * depth, depth)] = both[tokens:]
 
 
 def mix_channels(mid_rows, weights):
-    units, depth = weights.shape[1] // 3, 512
+    units, depth = weights.shape[1] // 6, 256
     steps = weights.shape[0] // depth
     return pl.pallas_call(
         functools.partial(mixer_kernel, units, depth),
@@ -413,6 +417,7 @@
         scratch_shapes=[
             pltpu.VMEM(weights.shape, jnp.bfloat16),
             pltpu.VMEM((mid_rows.shape[0], 2 * units), jnp.float32),
+            pltpu.VMEM((2 * mid_rows.shape[0], 2 * units), jnp.bfloat16),
             pltpu.SemaphoreType.DMA((2, steps)),
         ],
         compiler_params=pltpu.CompilerParams(vmem_limit_bytes=52 << 20),

time: 148 us -> 149 us (level)
  waiting for transfers between devices: 12.2 us -> 21 us
  blocking collectives: 74 us -> 68.4 us
  starting transfers between devices: 31 us -> 27.3 us
  Pallas kernels: 13.4 us -> 15.1 us
    all_to_all x1, waiting for transfers between devices: 10.7 us -> 16.7 us  [nearby_weights(): lax.all_to_all(copies, (*SP, 'tp'), split_axis=0, concat_axis=0, tiled=Tr...]
    all_to_all x1, blocking collectives: 25.4 us -> 19.7 us  [mix_tokens(): lax.all_to_all(packed, SP, split_axis=0, concat_axis=0, tiled=True)]
    ppermute x3, waiting for transfers between devices: 0.01 us -> 2.73 us  [collected_projection(): blocks.append(lax.ppermute(out_proj, 'tp', path))]
    all_to_all x1, starting transfers between devices: 13.2 us -> 11 us  [nearby_weights(): lax.all_to_all(copies, (*SP, 'tp'), split_axis=0, concat_axis=0, tiled=Tr...]
  transfers between devices with their start and end apart: 6 -> 6, of which waited for: 2 -> 3; matrix products, arithmetic and copies ran while one was open for 1% -> 1% of each run, Pallas kernels for 4% -> 4%
where the time goes in v7:
time: 149 us; the launch traced here: 148 us
  blocking collectives  68.4 us (46%)
  starting transfers between devices  27.3 us (18%)
  waiting for transfers between devices  21 us (14%)
  Pallas kernels  15.1 us (10%)
  between operations  13.6 us (9%)
  local copies, waits for them, and re-layouts  2.8 us (2%)
    all_to_all x2, blocking collectives, sent(): return lax.all_to_all(blocks, axis, split_axis=0, concat_axis=0, tiled=True)  24.6 us
    all_to_all x1, blocking collectives, mix_tokens(): lax.all_to_all(packed, SP, split_axis=0, concat_axis=0, tiled=True)  19.7 us
    all_to_all x1, waiting for transfers between devices, nearby_weights(): lax.all_to_all(copies, (*SP, 'tp'), split_axis=0, concat_axis=0, tiled=Tr...  16.7 us
    all_to_all x1, blocking collectives, incoming_state(): back = lax.all_to_all(entering, SP, split_axis=0, concat_axis=0, tiled=True)  15.7 us
    all_to_all x1, starting transfers between devices, nearby_weights(): lax.all_to_all(copies, (*SP, 'tp'), split_axis=0, concat_axis=0, tiled=Tr...  11 us
    ppermute x3, starting transfers between devices, collected_projection(): blocks.append(lax.ppermute(out_proj, 'tp', path))  10.9 us
    all_to_all x1, blocking collectives, middle_rows(): lax.all_to_all(copies, 'tp', split_axis=0, concat_axis=0, tiled=True, axi...  8.44 us
    pallas_call x1, Pallas kernels, mix_channels(): pl.pallas_call(functools.partial(mixer_kernel, units, depth), out_shape=j...  5.65 us
  transfers between devices with their start and end apart: 6, of which 3 were waited for; matrix products, arithmetic and copies ran while one was open for 1% of the time, Pallas kernels for 4%

profile of v7, /device:TPU:1, one launch (start us, length us, event | category | flops | bytes accessed | tf_op | source)
XLA Modules:
  0.0 148.3 jit_solution(9316631344528671221)
XLA Ops:
  6.5 2.0 %copies.1 = bf16[8,16,4224]{2,1,0:T(8,128)(2,1)} custom-call(bf16[32,704]{1,0:T(8,128)(2,1)} %gate_ref.2, bf16[32,704]{1,0:T(8,128)(2,1)} %up_ref.1, bf16[32,704]{1,0:T(8,128)(2,1)} %bitcast.22), custom_call_target="tpu_custom_call" | custom-call | tf_op jit(solution)/shard_map/copies/pallas_call | solution.py:166
  8.6 0.0 copy-start.2
  8.6 0.0 copy-start.3
  8.6 0.0 copy-start.5
  8.6 11.0 %all-to-all-start = ((bf16[8,16,4224]{2,1,0:T(8,128)(2,1)}), bf16[8,16,4224]{2,1,0:T(8,128)(2,1)S(1)}, u32[]{:S(2)}, u32[]{:S(2)}) async-start(bf16[8,16,4224]{2,1,0:T(8,128)(2,1)} %copies.1), calls=%async_computation | async-start | bytes 2162688 | tf_op jit(solution)/shard_map/all_to_all | solution.py:178
  19.6 0.0 all-gather.2.cloned.1.call-start
  19.7 1.5 local.1
  21.2 0.0 copy-start.11
  21.3 16.7 %all-to-all-done = bf16[8,16,4224]{2,1,0:T(8,128)(2,1)S(1)} async-done(((bf16[8,16,4224]{2,1,0:T(8,128)(2,1)}), bf16[8,16,4224]{2,1,0:T(8,128)(2,1)S(1)}, u32[]{:S(2)}, u32[]{:S(2)}) %all-to-all-start) | async-done | bytes 1081376 | tf_op jit(solution)/shard_map/all_to_all | solution.py:178
  38.0 1.0 copy-done.12
  39.0 0.0 all-gather.2.cloned.1.call-update
  39.0 4.4 %collective-permute-start = (bf16[256,2048]{1,0:T(8,128)(2,1)S(1)}, bf16[256,2048]{1,0:T(8,128)(2,1)S(1)}, u32[]{:S(2)}, u32[]{:S(2)}) collective-permute-start(bf16[256,2048]{1,0:T(8,128)(2,1)S(1)} %copy-done), channel_id=1, source_target_pairs={{0,4},{1,5},{2,6},{3,7},{4,0},{5,1},{6,2},{7,3},{8,12},{9,13},{10,... | collective-permute-start | bytes 3145736 | tf_op jit(solution)/shard_map/ppermute | solution.py:217
  43.5 2.2 %collective-permute-start.1 = (bf16[256,2048]{1,0:T(8,128)(2,1)S(1)}, bf16[256,2048]{1,0:T(8,128)(2,1)S(1)}, u32[]{:S(2)}, u32[]{:S(2)}) collective-permute-start(bf16[256,2048]{1,0:T(8,128)(2,1)S(1)} %copy-done), channel_id=1, source_target_pairs={{0,2},{1,3},{2,4},{3,5},{4,6},{5,7},{6,0},{7,1},{8,10},{9,11},{10,... | collective-permute-start | bytes 3145736 | tf_op jit(solution)/shard_map/ppermute | solution.py:217
  45.7 4.3 %collective-permute-start.2 = (bf16[256,2048]{1,0:T(8,128)(2,1)S(1)}, bf16[256,2048]{1,0:T(8,128)(2,1)}, u32[]{:S(2)}, u32[]{:S(2)}) collective-permute-start(bf16[256,2048]{1,0:T(8,128)(2,1)S(1)} %copy-done), channel_id=1, source_target_pairs={{0,6},{1,7},{2,0},{3,1},{4,2},{5,3},{6,4},{7,5},{8,14},{9,15},{10,... | collective-permute-start | bytes 3145736 | tf_op jit(solution)/shard_map/ppermute | solution.py:217
  50.0 19.7 %all_to_all.30 = bf16[64,2,384]{2,1,0:T(2,128)(2,1)S(1)} all-to-all(bf16[64,2,384]{2,1,0:T(2,128)(2,1)S(1)} %reshape.21), channel_id=1, replica_groups=mesh['sp_0'=8,'sp_1'=8,'tp'=8] {'sp_0','sp_1'}, dimensions={0} | all-to-all | bytes 196608 | tf_op jit(solution)/shard_map/all_to_all | solution.py:351
  69.6 1.2 prefix.1
  70.8 15.7 %all_to_all.31 = bf16[64,2,256]{2,1,0:T(2,128)(2,1)} all-to-all(bf16[64,2,256]{2,1,0:T(2,128)(2,1)S(1)} %reshape.24), channel_id=1, replica_groups=mesh['sp_0'=8,'sp_1'=8,'tp'=8] {'sp_0','sp_1'}, dimensions={0} | all-to-all | bytes 131072 | tf_op jit(solution)/shard_map/all_to_all | solution.py:115
  86.6 0.9 reshape.25.state_ref
  87.4 2.7 %collective-permute-done.1.refs_2_ = bf16[256,2048]{1,0:T(8,128)(2,1)S(1)} collective-permute-done((bf16[256,2048]{1,0:T(8,128)(2,1)S(1)}, bf16[256,2048]{1,0:T(8,128)(2,1)S(1)}, u32[]{:S(2)}, u32[]{:S(2)}) %collective-permute-start.1) | collective-permute-done | bytes 1048608 | tf_op jit(solution)/shard_map/ppermute | solution.py:217
  90.2 0.4 gate.1
  90.5 8.4 %all_to_all.32.gated_ref = bf16[4,128,256]{2,1,0:T(8,128)(2,1)S(1)} all-to-all(bf16[4,128,256]{2,1,0:T(8,128)(2,1)S(1)} %gate.1), channel_id=1, replica_groups={{0,2,4,6},{1,3,5,7},{8,10,12,14},{9,11,13,15},{16,18,20,22},{17,19,21,2..., dimensions={0} | all-to-all | bytes 524288 | tf_op jit(solution)/shard_map/all_to_all | solution.py:267
  99.0 2.0 %project.1.own_ref = bf16[128,2048]{1,0:T(8,128)(2,1)S(1)} custom-call(s32[1]{0:T(128)} %bitcast.2.place_ref, bf16[4,128,256]{2,1,0:T(8,128)(2,1)S(1)} %all_to_all.32.gated_ref, bf16[256,2048]{1,0:T(8,128)(2,1)S(1)} %copy-done, bf16[256,2048]{1,0:T(8,128)(2,1)S(1)} %collective-permute-done.refs_1_, bf16[256,2048]{1,0:T(8,128)(2,1)S(1)} %collective-permute-done.1.refs_2_, ...), custom_call_target="tpu_custom_call" | custom-call | tf_op jit(solution)/shard_map/project/pallas_call | solution.py:276
  101.0 5.3 %collective-permute-start.3 = (bf16[128,2048]{1,0:T(8,128)(2,1)S(1)}, bf16[128,2048]{1,0:T(8,128)(2,1)S(1)}, u32[]{:S(2)}, u32[]{:S(2)}) collective-permute-start(bf16[128,2048]{1,0:T(8,128)(2,1)S(1)} %project.1.own_ref), channel_id=1, source_target_pairs={{0,1},{1,0},{2,3},{3,2},{4,5},{5,4},{6,7},{7,6},{8,9},{9,8},{10,11... | collective-permute-start | bytes 1572872 | tf_op jit(solution)/shard_map/ppermute | solution.py:284
  106.3 1.5 %collective-permute-done.3.other_ref = bf16[128,2048]{1,0:T(8,128)(2,1)S(1)} collective-permute-done((bf16[128,2048]{1,0:T(8,128)(2,1)S(1)}, bf16[128,2048]{1,0:T(8,128)(2,1)S(1)}, u32[]{:S(2)}, u32[]{:S(2)}) %collective-permute-start.3) | collective-permute-done | bytes 524320 | tf_op jit(solution)/shard_map/ppermute | solution.py:284
  107.8 1.7 %middle.1 = (bf16[128,2048]{1,0:T(8,128)(2,1)S(1)}, bf16[16,2048]{1,0:T(8,128)(2,1)S(1)}) custom-call(s32[1]{0:T(128)} %bitcast.2.place_ref, bf16[128,2048]{1,0:T(8,128)(2,1)S(1)} %project.1.own_ref, bf16[128,2048]{1,0:T(8,128)(2,1)S(1)} %collective-permute-done.3.other_ref, bf16[128,2048]{1,0:T(8,128)(2,1)S(1)} %copy-done.1, f32[1,2048]{1,0:T(1,128)S(1)} %bitcast.14, ...), custom_call_target="tpu_custom_call" | custom-call | tf_op jit(solution)/shard_map/middle/pallas_call | solution.py:285
  109.5 0.0 all-gather.2.cloned.1.call-done.weights_ref
  109.5 0.0 copy-start.10
  109.6 5.6 %mix_channels.1 = bf16[128,2048]{1,0:T(8,128)(2,1)S(1)} custom-call(bf16[128,2048]{1,0:T(8,128)(2,1)S(1)} %get-tuple-element.28.mid_ref, bf16[1024,4224]{1,0:T(8,128)(2,1)} %all-gather.2.cloned.1.call-done.weights_ref), custom_call_target="tpu_custom_call" | custom-call | flops 1107296256 | bytes 8650752 | tf_op jit(solution)/shard_map/mix_channels/pallas_call | solution.py:409
  115.2 11.9 %all_to_all.33.arrived_ref = bf16[8,16,2048]{2,1,0:T(8,128)(2,1)S(1)} all-to-all(bf16[8,16,2048]{2,1,0:T(8,128)(2,1)S(1)} %bitcast.12), channel_id=1, replica_groups=mesh['sp_0'=8,'sp_1'=8,'tp'=8] {'tp'}, dimensions={0} | all-to-all | bytes 1048576 | tf_op jit(solution)/shard_map/all_to_all | solution.py:329
  127.1 0.8 settle.1
  127.9 12.8 %all_to_all.34 = bf16[8,16,2048]{2,1,0:T(8,128)(2,1)S(1)} all-to-all(bf16[8,16,2048]{2,1,0:T(8,128)(2,1)S(1)} %settle.1), channel_id=1, replica_groups=mesh['sp_0'=8,'sp_1'=8,'tp'=8] {'tp'}, dimensions={0} | all-to-all | bytes 1048576 | tf_op jit(solution)/shard_map/all_to_all | solution.py:329
  140.6 0.8 copy.18
  (25 shorter events, 0.1 us)
Async XLA Ops:
  8.6 11.1 %copy-start.2 = (bf16[128,256]{1,0:T(8,128)(2,1)S(1)}, bf16[128,256]{1,0:T(8,128)(2,1)}, u32[]{:S(2)}) copy-start(bf16[128,256]{1,0:T(8,128)(2,1)} %values_ref.1) | copy-start | bytes 196612
  8.6 11.1 %copy-start.3 = (f32[128,128]{1,0:T(8,128)S(1)}, f32[128,128]{1,0:T(8,128)}, u32[]{:S(2)}) copy-start(f32[128,128]{1,0:T(8,128)} %decay_ref.1) | copy-start | bytes 196612
  8.6 11.1 %copy-start.5 = (bf16[128,128]{1,0:T(8,128)(2,1)S(1)}, bf16[128,128]{1,0:T(8,128)(2,1)}, u32[]{:S(2)}) copy-start(bf16[128,128]{1,0:T(8,128)(2,1)} %queries_ref.1) | copy-start | bytes 98308
  8.6 11.1 %copy-start.6 = (bf16[128,128]{1,0:T(8,128)(2,1)S(1)}, bf16[128,128]{1,0:T(8,128)(2,1)}, u32[]{:S(2)}) copy-start(bf16[128,128]{1,0:T(8,128)(2,1)} %keys_ref.1) | copy-start | bytes 98308
  8.6 29.4 %all-to-all-start = ((bf16[8,16,4224]{2,1,0:T(8,128)(2,1)}), bf16[8,16,4224]{2,1,0:T(8,128)(2,1)S(1)}, u32[]{:S(2)}, u32[]{:S(2)}) async-start(bf16[8,16,4224]{2,1,0:T(8,128)(2,1)} %copies.1), calls=%async_computation | async-start | bytes 2162688 | tf_op jit(solution)/shard_map/all_to_all | solution.py:178
  19.6 19.4 %copy-start = (bf16[256,2048]{1,0:T(8,128)(2,1)S(1)}, bf16[256,2048]{1,0:T(8,128)(2,1)}, u32[]{:S(2)}) copy-start(bf16[256,2048]{1,0:T(8,128)(2,1)} %refs_0_) | copy-start | bytes 3145732
  19.6 89.9 %all-gather.2.cloned.1.call-start = ((), (), s32[]{:S(2)}) async-start(), calls=%async_computation.6 | async-start | bytes 9732096 | tf_op jit(solution)/shard_map/all_gather | solution.py:190
  21.2 69.0 %copy-start.4 = (bf16[128,256]{1,0:T(8,128)(2,1)S(1)}, bf16[128,256]{1,0:T(8,128)(2,1)}, u32[]{:S(2)}) copy-start(bf16[128,256]{1,0:T(8,128)(2,1)} %gate_ref.3) | copy-start | bytes 196612
  21.2 69.0 %copy-start.11 = (f32[256]{0:T(256)S(1)}, f32[256]{0:T(256)}, u32[]{:S(2)}) copy-start(f32[256]{0:T(256)} %param.21) | copy-start | bytes 3076
  38.0 1.0 copy-start.12
  39.0 48.4 %collective-permute-start = (bf16[256,2048]{1,0:T(8,128)(2,1)S(1)}, bf16[256,2048]{1,0:T(8,128)(2,1)S(1)}, u32[]{:S(2)}, u32[]{:S(2)}) collective-permute-start(bf16[256,2048]{1,0:T(8,128)(2,1)S(1)} %copy-done), channel_id=1, source_target_pairs={{0,4},{1,5},{2,6},{3,7},{4,0},{5,1},{6,2},{7,3},{8,12},{9,13},{10,... | collective-permute-start | bytes 3145736 | tf_op jit(solution)/shard_map/ppermute | solution.py:217
  43.5 46.7 %collective-permute-start.1 = (bf16[256,2048]{1,0:T(8,128)(2,1)S(1)}, bf16[256,2048]{1,0:T(8,128)(2,1)S(1)}, u32[]{:S(2)}, u32[]{:S(2)}) collective-permute-start(bf16[256,2048]{1,0:T(8,128)(2,1)S(1)} %copy-done), channel_id=1, source_target_pairs={{0,2},{1,3},{2,4},{3,5},{4,6},{5,7},{6,0},{7,1},{8,10},{9,11},{10,... | collective-permute-start | bytes 3145736 | tf_op jit(solution)/shard_map/ppermute | solution.py:217
  45.7 44.5 %collective-permute-start.2 = (bf16[256,2048]{1,0:T(8,128)(2,1)S(1)}, bf16[256,2048]{1,0:T(8,128)(2,1)}, u32[]{:S(2)}, u32[]{:S(2)}) collective-permute-start(bf16[256,2048]{1,0:T(8,128)(2,1)S(1)} %copy-done), channel_id=1, source_target_pairs={{0,6},{1,7},{2,0},{3,1},{4,2},{5,3},{6,4},{7,5},{8,14},{9,15},{10,... | collective-permute-start | bytes 3145736 | tf_op jit(solution)/shard_map/ppermute | solution.py:217
  99.0 8.9 %copy-start.1 = (bf16[128,2048]{1,0:T(8,128)(2,1)S(1)}, bf16[128,2048]{1,0:T(8,128)(2,1)}, u32[]{:S(2)}) copy-start(bf16[128,2048]{1,0:T(8,128)(2,1)} %before_ref.1) | copy-start | bytes 1572868
  99.0 8.9 %copy-start.7 = (f32[2048]{0:T(1024)S(1)}, f32[2048]{0:T(1024)}, u32[]{:S(2)}) copy-start(f32[2048]{0:T(1024)} %param.23) | copy-start | bytes 24580
  99.0 8.9 %copy-start.8 = (f32[2048]{0:T(1024)S(1)}, f32[2048]{0:T(1024)}, u32[]{:S(2)}) copy-start(f32[2048]{0:T(1024)} %param.24) | copy-start | bytes 24580
  101.0 6.8 %collective-permute-start.3 = (bf16[128,2048]{1,0:T(8,128)(2,1)S(1)}, bf16[128,2048]{1,0:T(8,128)(2,1)S(1)}, u32[]{:S(2)}, u32[]{:S(2)}) collective-permute-start(bf16[128,2048]{1,0:T(8,128)(2,1)S(1)} %project.1.own_ref), channel_id=1, source_target_pairs={{0,1},{1,0},{2,3},{3,2},{4,5},{5,4},{6,7},{7,6},{8,9},{9,8},{10,11... | collective-permute-start | bytes 1572872 | tf_op jit(solution)/shard_map/ppermute | solution.py:284
  109.5 17.5 %copy-start.9 = (f32[2048]{0:T(1024)S(1)}, f32[2048]{0:T(1024)}, u32[]{:S(2)}) copy-start(f32[2048]{0:T(1024)} %param.28) | copy-start | bytes 24580
  109.5 17.5 %copy-start.10 = (f32[2048]{0:T(1024)S(1)}, f32[2048]{0:T(1024)}, u32[]{:S(2)}) copy-start(f32[2048]{0:T(1024)} %param.29) | copy-start | bytes 24580
Sparse Core Ops, SparseCore 0:
  39.1 59.3 all-gather.1

commit v8 on v7

--- a/solution.py
+++ b/solution.py
@@ -258,7 +258,7 @@
 
         @pl.when(lax.rem(place_ref[0], 2) == core)
         def _():
-            turned_ref[...] = shuffled(rows.astype(jnp.float32), sources[core]).astype(jnp.bfloat16)
+            turned_ref[...] = shuffled(rows, sources[core])
 
 
 def middle_rows(place, copies, blocks, resid, gain, shift):
@@ -361,7 +361,7 @@
 
 
 def mixer_kernel(units, depth, mid_ref, weights_ref, out_ref, held, total, pair, sems):
-    tokens, half = mid_ref.shape[0], weights_ref.shape[0]
+    half = weights_ref.shape[0]
     steps, wide = half // depth, 2 * units
 
     def fetch(step, part):
@@ -389,18 +389,18 @@
             else:
                 total[...] += product
     hidden = (jax.nn.silu(total[:, :units]) * total[:, units:]).astype(jnp.bfloat16)
-    pair[:tokens, :units] = hidden
-    pair[tokens:, units:] = hidden
+    room = pair.shape[2]
+    pair[0, :, :units] = hidden
+    pair[1, :, room - units :] = hidden
     for step in range(steps):
         fetch(step, 1).wait()
-        both = lax.dot_general(
-            pair[...],
-            held[pl.ds(step * depth, depth), pl.ds(2 * wide, wide)],
-            (((1,), (1,)), ((), ())),
-            preferred_element_type=jnp.float32,
-        ).astype(jnp.bfloat16)
-        out_ref[:, pl.ds(step * depth, depth)] = both[:tokens]
-        out_ref[:, pl.ds(half + step * depth, depth)] = both[tokens:]
+        for side in range(2):
+            out_ref[:, pl.ds(side * half + step * depth, depth)] = lax.dot_general(
+                pair[side],
+                held[pl.ds(step * depth, depth), pl.ds((2 + side) * wide - side * room, room)],
+                (((1,), (1,)), ((), ())),
+                preferred_element_type=jnp.float32,
+            ).astype(jnp.bfloat16)
 
 
 def mix_channels(mid_rows, weights):
@@ -417,7 +417,7 @@
         scratch_shapes=[
             pltpu.VMEM(weights.shape, jnp.bfloat16),
             pltpu.VMEM((mid_rows.shape[0], 2 * units), jnp.float32),
-            pltpu.VMEM((2 * mid_rows.shape[0], 2 * units), jnp.bfloat16),
+            pltpu.VMEM((2, mid_rows.shape[0], -(-units // 128) * 128), jnp.bfloat16),
             pltpu.SemaphoreType.DMA((2, steps)),
         ],
         compiler_params=pltpu.CompilerParams(vmem_limit_bytes=52 << 20),

time: 149 us -> 148 us (level)
  transfers between devices with their start and end apart: 6 -> 6, of which waited for: 3 -> 3; matrix products, arithmetic and copies ran while one was open for 1% -> 1% of each run, Pallas kernels for 4% -> 5%
where the time goes in v8:
time: 148 us; the launch traced here: 147 us
  blocking collectives  68.3 us (46%)
  starting transfers between devices  27.3 us (18%)
  waiting for transfers between devices  21 us (14%)
  Pallas kernels  14.3 us (10%)
  between operations  13.6 us (9%)
  local copies, waits for them, and re-layouts  2.8 us (2%)
    all_to_all x2, blocking collectives, sent(): return lax.all_to_all(blocks, axis, split_axis=0, concat_axis=0, tiled=True)  24.5 us
    all_to_all x1, blocking collectives, mix_tokens(): lax.all_to_all(packed, SP, split_axis=0, concat_axis=0, tiled=True)  19.7 us
    all_to_all x1, waiting for transfers between devices, nearby_weights(): lax.all_to_all(copies, (*SP, 'tp'), split_axis=0, concat_axis=0, tiled=Tr...  16.7 us
    all_to_all x1, blocking collectives, incoming_state(): back = lax.all_to_all(entering, SP, split_axis=0, concat_axis=0, tiled=True)  15.7 us
    all_to_all x1, starting transfers between devices, nearby_weights(): lax.all_to_all(copies, (*SP, 'tp'), split_axis=0, concat_axis=0, tiled=Tr...  11 us
    ppermute x3, starting transfers between devices, collected_projection(): blocks.append(lax.ppermute(out_proj, 'tp', path))  10.9 us
    all_to_all x1, blocking collectives, middle_rows(): lax.all_to_all(copies, 'tp', split_axis=0, concat_axis=0, tiled=True, axi...  8.44 us
    ppermute x1, starting transfers between devices, middle_rows(): other = lax.ppermute(own, 'tp', [(part, part ^ 1) for part in range(parts)])  5.31 us
  transfers between devices with their start and end apart: 6, of which 3 were waited for; matrix products, arithmetic and copies ran while one was open for 1% of the time, Pallas kernels for 5%

profile of v8, /device:TPU:1, one launch (start us, length us, event | category | flops | bytes accessed | tf_op | source)
XLA Modules:
  0.0 147.3 jit_solution(14670560260152190205)
XLA Ops:
  6.5 2.0 %copies.1 = bf16[8,16,4224]{2,1,0:T(8,128)(2,1)} custom-call(bf16[32,704]{1,0:T(8,128)(2,1)} %gate_ref.2, bf16[32,704]{1,0:T(8,128)(2,1)} %up_ref.1, bf16[32,704]{1,0:T(8,128)(2,1)} %bitcast.22), custom_call_target="tpu_custom_call" | custom-call | tf_op jit(solution)/shard_map/copies/pallas_call | solution.py:166
  8.6 0.0 copy-start.2
  8.6 0.0 copy-start.3
  8.6 0.0 copy-start.5
  8.6 11.0 %all-to-all-start = ((bf16[8,16,4224]{2,1,0:T(8,128)(2,1)}), bf16[8,16,4224]{2,1,0:T(8,128)(2,1)S(1)}, u32[]{:S(2)}, u32[]{:S(2)}) async-start(bf16[8,16,4224]{2,1,0:T(8,128)(2,1)} %copies.1), calls=%async_computation | async-start | bytes 2162688 | tf_op jit(solution)/shard_map/all_to_all | solution.py:178
  19.6 0.0 all-gather.2.cloned.1.call-start
  19.7 1.5 %local.1 = (bf16[128,384]{1,0:T(8,128)(2,1)S(1)}, f32[128,128]{1,0:T(8,128)S(1)}, f32[128,256]{1,0:T(8,128)S(1)}) custom-call(bf16[128,128]{1,0:T(8,128)(2,1)S(1)} %copy-done.5, bf16[128,128]{1,0:T(8,128)(2,1)S(1)} %copy-done.6, bf16[128,256]{1,0:T(8,128)(2,1)S(1)} %copy-done.2, f32[128,128]{1,0:T(8,128)S(1)} %copy-done.3), custom_call_target="tpu_custom_call" | custom-call | tf_op jit(solution)/shard_map/local/pallas_call | solution.py:62
  21.2 0.0 copy-start.11
  21.3 16.7 %all-to-all-done = bf16[8,16,4224]{2,1,0:T(8,128)(2,1)S(1)} async-done(((bf16[8,16,4224]{2,1,0:T(8,128)(2,1)}), bf16[8,16,4224]{2,1,0:T(8,128)(2,1)S(1)}, u32[]{:S(2)}, u32[]{:S(2)}) %all-to-all-start) | async-done | bytes 1081376 | tf_op jit(solution)/shard_map/all_to_all | solution.py:178
  38.0 1.0 copy-done.12
  39.0 0.0 all-gather.2.cloned.1.call-update
  39.0 4.4 %collective-permute-start = (bf16[256,2048]{1,0:T(8,128)(2,1)S(1)}, bf16[256,2048]{1,0:T(8,128)(2,1)S(1)}, u32[]{:S(2)}, u32[]{:S(2)}) collective-permute-start(bf16[256,2048]{1,0:T(8,128)(2,1)S(1)} %copy-done), channel_id=1, source_target_pairs={{0,4},{1,5},{2,6},{3,7},{4,0},{5,1},{6,2},{7,3},{8,12},{9,13},{10,... | collective-permute-start | bytes 3145736 | tf_op jit(solution)/shard_map/ppermute | solution.py:217
  43.5 2.2 %collective-permute-start.1 = (bf16[256,2048]{1,0:T(8,128)(2,1)S(1)}, bf16[256,2048]{1,0:T(8,128)(2,1)S(1)}, u32[]{:S(2)}, u32[]{:S(2)}) collective-permute-start(bf16[256,2048]{1,0:T(8,128)(2,1)S(1)} %copy-done), channel_id=1, source_target_pairs={{0,2},{1,3},{2,4},{3,5},{4,6},{5,7},{6,0},{7,1},{8,10},{9,11},{10,... | collective-permute-start | bytes 3145736 | tf_op jit(solution)/shard_map/ppermute | solution.py:217
  45.7 4.3 %collective-permute-start.2 = (bf16[256,2048]{1,0:T(8,128)(2,1)S(1)}, bf16[256,2048]{1,0:T(8,128)(2,1)}, u32[]{:S(2)}, u32[]{:S(2)}) collective-permute-start(bf16[256,2048]{1,0:T(8,128)(2,1)S(1)} %copy-done), channel_id=1, source_target_pairs={{0,6},{1,7},{2,0},{3,1},{4,2},{5,3},{6,4},{7,5},{8,14},{9,15},{10,... | collective-permute-start | bytes 3145736 | tf_op jit(solution)/shard_map/ppermute | solution.py:217
  50.0 19.7 %all_to_all.30 = bf16[64,2,384]{2,1,0:T(2,128)(2,1)S(1)} all-to-all(bf16[64,2,384]{2,1,0:T(2,128)(2,1)S(1)} %reshape.21), channel_id=1, replica_groups=mesh['sp_0'=8,'sp_1'=8,'tp'=8] {'sp_0','sp_1'}, dimensions={0} | all-to-all | bytes 196608 | tf_op jit(solution)/shard_map/all_to_all | solution.py:351
  69.6 1.2 prefix.1
  70.8 15.7 %all_to_all.31 = bf16[64,2,256]{2,1,0:T(2,128)(2,1)} all-to-all(bf16[64,2,256]{2,1,0:T(2,128)(2,1)S(1)} %reshape.24), channel_id=1, replica_groups=mesh['sp_0'=8,'sp_1'=8,'tp'=8] {'sp_0','sp_1'}, dimensions={0} | all-to-all | bytes 131072 | tf_op jit(solution)/shard_map/all_to_all | solution.py:115
  86.6 0.9 reshape.25.state_ref
  87.4 2.7 %collective-permute-done.1.refs_2_ = bf16[256,2048]{1,0:T(8,128)(2,1)S(1)} collective-permute-done((bf16[256,2048]{1,0:T(8,128)(2,1)S(1)}, bf16[256,2048]{1,0:T(8,128)(2,1)S(1)}, u32[]{:S(2)}, u32[]{:S(2)}) %collective-permute-start.1) | collective-permute-done | bytes 1048608 | tf_op jit(solution)/shard_map/ppermute | solution.py:217
  90.2 0.4 gate.1
  90.5 8.4 %all_to_all.32.gated_ref = bf16[4,128,256]{2,1,0:T(8,128)(2,1)S(1)} all-to-all(bf16[4,128,256]{2,1,0:T(8,128)(2,1)S(1)} %gate.1), channel_id=1, replica_groups={{0,2,4,6},{1,3,5,7},{8,10,12,14},{9,11,13,15},{16,18,20,22},{17,19,21,2..., dimensions={0} | all-to-all | bytes 524288 | tf_op jit(solution)/shard_map/all_to_all | solution.py:267
  99.0 2.0 %project.1.own_ref = bf16[128,2048]{1,0:T(8,128)(2,1)S(1)} custom-call(s32[1]{0:T(128)} %bitcast.2.place_ref, bf16[4,128,256]{2,1,0:T(8,128)(2,1)S(1)} %all_to_all.32.gated_ref, bf16[256,2048]{1,0:T(8,128)(2,1)S(1)} %copy-done, bf16[256,2048]{1,0:T(8,128)(2,1)S(1)} %collective-permute-done.refs_1_, bf16[256,2048]{1,0:T(8,128)(2,1)S(1)} %collective-permute-done.1.refs_2_, ...), custom_call_target="tpu_custom_call" | custom-call | tf_op jit(solution)/shard_map/project/pallas_call | solution.py:276
  101.0 5.3 %collective-permute-start.3 = (bf16[128,2048]{1,0:T(8,128)(2,1)S(1)}, bf16[128,2048]{1,0:T(8,128)(2,1)S(1)}, u32[]{:S(2)}, u32[]{:S(2)}) collective-permute-start(bf16[128,2048]{1,0:T(8,128)(2,1)S(1)} %project.1.own_ref), channel_id=1, source_target_pairs={{0,1},{1,0},{2,3},{3,2},{4,5},{5,4},{6,7},{7,6},{8,9},{9,8},{10,11... | collective-permute-start | bytes 1572872 | tf_op jit(solution)/shard_map/ppermute | solution.py:284
  106.3 1.5 %collective-permute-done.3.other_ref = bf16[128,2048]{1,0:T(8,128)(2,1)S(1)} collective-permute-done((bf16[128,2048]{1,0:T(8,128)(2,1)S(1)}, bf16[128,2048]{1,0:T(8,128)(2,1)S(1)}, u32[]{:S(2)}, u32[]{:S(2)}) %collective-permute-start.3) | collective-permute-done | bytes 524320 | tf_op jit(solution)/shard_map/ppermute | solution.py:284
  107.8 1.7 %middle.1 = (bf16[128,2048]{1,0:T(8,128)(2,1)S(1)}, bf16[16,2048]{1,0:T(8,128)(2,1)S(1)}) custom-call(s32[1]{0:T(128)} %bitcast.2.place_ref, bf16[128,2048]{1,0:T(8,128)(2,1)S(1)} %project.1.own_ref, bf16[128,2048]{1,0:T(8,128)(2,1)S(1)} %collective-permute-done.3.other_ref, bf16[128,2048]{1,0:T(8,128)(2,1)S(1)} %copy-done.1, f32[1,2048]{1,0:T(1,128)S(1)} %bitcast.14, ...), custom_call_target="tpu_custom_call" | custom-call | tf_op jit(solution)/shard_map/middle/pallas_call | solution.py:285
  109.5 0.0 all-gather.2.cloned.1.call-done.weights_ref
  109.5 0.0 copy-start.9
  109.6 4.8 %mix_channels.1 = bf16[128,2048]{1,0:T(8,128)(2,1)S(1)} custom-call(bf16[128,2048]{1,0:T(8,128)(2,1)S(1)} %get-tuple-element.28.mid_ref, bf16[1024,4224]{1,0:T(8,128)(2,1)} %all-gather.2.cloned.1.call-done.weights_ref), custom_call_target="tpu_custom_call" | custom-call | flops 1107296256 | bytes 8650752 | tf_op jit(solution)/shard_map/mix_channels/pallas_call | solution.py:409
  114.4 11.7 %all_to_all.33.arrived_ref = bf16[8,16,2048]{2,1,0:T(8,128)(2,1)S(1)} all-to-all(bf16[8,16,2048]{2,1,0:T(8,128)(2,1)S(1)} %bitcast.12), channel_id=1, replica_groups=mesh['sp_0'=8,'sp_1'=8,'tp'=8] {'tp'}, dimensions={0} | all-to-all | bytes 1048576 | tf_op jit(solution)/shard_map/all_to_all | solution.py:329
  126.1 0.8 settle.1
  126.9 12.8 %all_to_all.34 = bf16[8,16,2048]{2,1,0:T(8,128)(2,1)S(1)} all-to-all(bf16[8,16,2048]{2,1,0:T(8,128)(2,1)S(1)} %settle.1), channel_id=1, replica_groups=mesh['sp_0'=8,'sp_1'=8,'tp'=8] {'tp'}, dimensions={0} | all-to-all | bytes 1048576 | tf_op jit(solution)/shard_map/all_to_all | solution.py:329
  139.7 0.8 copy.18
  (25 shorter events, 0.1 us)
Async XLA Ops:
  8.6 11.1 %copy-start.2 = (bf16[128,256]{1,0:T(8,128)(2,1)S(1)}, bf16[128,256]{1,0:T(8,128)(2,1)}, u32[]{:S(2)}) copy-start(bf16[128,256]{1,0:T(8,128)(2,1)} %values_ref.1) | copy-start | bytes 196612
  8.6 11.1 %copy-start.3 = (f32[128,128]{1,0:T(8,128)S(1)}, f32[128,128]{1,0:T(8,128)}, u32[]{:S(2)}) copy-start(f32[128,128]{1,0:T(8,128)} %decay_ref.1) | copy-start | bytes 196612
  8.6 11.1 %copy-start.5 = (bf16[128,128]{1,0:T(8,128)(2,1)S(1)}, bf16[128,128]{1,0:T(8,128)(2,1)}, u32[]{:S(2)}) copy-start(bf16[128,128]{1,0:T(8,128)(2,1)} %queries_ref.1) | copy-start | bytes 98308
  8.6 11.1 %copy-start.6 = (bf16[128,128]{1,0:T(8,128)(2,1)S(1)}, bf16[128,128]{1,0:T(8,128)(2,1)}, u32[]{:S(2)}) copy-start(bf16[128,128]{1,0:T(8,128)(2,1)} %keys_ref.1) | copy-start | bytes 98308
  8.6 29.4 %all-to-all-start = ((bf16[8,16,4224]{2,1,0:T(8,128)(2,1)}), bf16[8,16,4224]{2,1,0:T(8,128)(2,1)S(1)}, u32[]{:S(2)}, u32[]{:S(2)}) async-start(bf16[8,16,4224]{2,1,0:T(8,128)(2,1)} %copies.1), calls=%async_computation | async-start | bytes 2162688 | tf_op jit(solution)/shard_map/all_to_all | solution.py:178
  19.6 19.4 %copy-start = (bf16[256,2048]{1,0:T(8,128)(2,1)S(1)}, bf16[256,2048]{1,0:T(8,128)(2,1)}, u32[]{:S(2)}) copy-start(bf16[256,2048]{1,0:T(8,128)(2,1)} %refs_0_) | copy-start | bytes 3145732
  19.6 89.9 %all-gather.2.cloned.1.call-start = ((), (), s32[]{:S(2)}) async-start(), calls=%async_computation.6 | async-start | bytes 9732096 | tf_op jit(solution)/shard_map/all_gather | solution.py:190
  21.2 69.0 %copy-start.4 = (bf16[128,256]{1,0:T(8,128)(2,1)S(1)}, bf16[128,256]{1,0:T(8,128)(2,1)}, u32[]{:S(2)}) copy-start(bf16[128,256]{1,0:T(8,128)(2,1)} %gate_ref.3) | copy-start | bytes 196612
  21.2 69.0 %copy-start.11 = (f32[256]{0:T(256)S(1)}, f32[256]{0:T(256)}, u32[]{:S(2)}) copy-start(f32[256]{0:T(256)} %param.21) | copy-start | bytes 3076
  38.0 1.0 copy-start.12
  39.0 48.4 %collective-permute-start = (bf16[256,2048]{1,0:T(8,128)(2,1)S(1)}, bf16[256,2048]{1,0:T(8,128)(2,1)S(1)}, u32[]{:S(2)}, u32[]{:S(2)}) collective-permute-start(bf16[256,2048]{1,0:T(8,128)(2,1)S(1)} %copy-done), channel_id=1, source_target_pairs={{0,4},{1,5},{2,6},{3,7},{4,0},{5,1},{6,2},{7,3},{8,12},{9,13},{10,... | collective-permute-start | bytes 3145736 | tf_op jit(solution)/shard_map/ppermute | solution.py:217
  43.5 46.7 %collective-permute-start.1 = (bf16[256,2048]{1,0:T(8,128)(2,1)S(1)}, bf16[256,2048]{1,0:T(8,128)(2,1)S(1)}, u32[]{:S(2)}, u32[]{:S(2)}) collective-permute-start(bf16[256,2048]{1,0:T(8,128)(2,1)S(1)} %copy-done), channel_id=1, source_target_pairs={{0,2},{1,3},{2,4},{3,5},{4,6},{5,7},{6,0},{7,1},{8,10},{9,11},{10,... | collective-permute-start | bytes 3145736 | tf_op jit(solution)/shard_map/ppermute | solution.py:217
  45.7 44.5 %collective-permute-start.2 = (bf16[256,2048]{1,0:T(8,128)(2,1)S(1)}, bf16[256,2048]{1,0:T(8,128)(2,1)}, u32[]{:S(2)}, u32[]{:S(2)}) collective-permute-start(bf16[256,2048]{1,0:T(8,128)(2,1)S(1)} %copy-done), channel_id=1, source_target_pairs={{0,6},{1,7},{2,0},{3,1},{4,2},{5,3},{6,4},{7,5},{8,14},{9,15},{10,... | collective-permute-start | bytes 3145736 | tf_op jit(solution)/shard_map/ppermute | solution.py:217
  99.0 8.9 %copy-start.1 = (bf16[128,2048]{1,0:T(8,128)(2,1)S(1)}, bf16[128,2048]{1,0:T(8,128)(2,1)}, u32[]{:S(2)}) copy-start(bf16[128,2048]{1,0:T(8,128)(2,1)} %before_ref.1) | copy-start | bytes 1572868
  99.0 8.9 %copy-start.7 = (f32[2048]{0:T(1024)S(1)}, f32[2048]{0:T(1024)}, u32[]{:S(2)}) copy-start(f32[2048]{0:T(1024)} %param.23) | copy-start | bytes 24580
  99.0 8.9 %copy-start.8 = (f32[2048]{0:T(1024)S(1)}, f32[2048]{0:T(1024)}, u32[]{:S(2)}) copy-start(f32[2048]{0:T(1024)} %param.24) | copy-start | bytes 24580
  101.0 6.8 %collective-permute-start.3 = (bf16[128,2048]{1,0:T(8,128)(2,1)S(1)}, bf16[128,2048]{1,0:T(8,128)(2,1)S(1)}, u32[]{:S(2)}, u32[]{:S(2)}) collective-permute-start(bf16[128,2048]{1,0:T(8,128)(2,1)S(1)} %project.1.own_ref), channel_id=1, source_target_pairs={{0,1},{1,0},{2,3},{3,2},{4,5},{5,4},{6,7},{7,6},{8,9},{9,8},{10,11... | collective-permute-start | bytes 1572872 | tf_op jit(solution)/shard_map/ppermute | solution.py:284
  109.5 16.6 %copy-start.9 = (f32[2048]{0:T(1024)S(1)}, f32[2048]{0:T(1024)}, u32[]{:S(2)}) copy-start(f32[2048]{0:T(1024)} %param.28) | copy-start | bytes 24580
  109.6 16.6 %copy-start.10 = (f32[2048]{0:T(1024)S(1)}, f32[2048]{0:T(1024)}, u32[]{:S(2)}) copy-start(f32[2048]{0:T(1024)} %param.29) | copy-start | bytes 24580
Sparse Core Ops, SparseCore 0:
  39.1 59.3 all-gather.1
